TPU v7x, 512 devices: a 8x2x16 block of a 8x16x16 slice. The times are simulated.
512 devices in a mesh: grp: 2 (over y), sp: 16 (over z), tp: 16 (over x, core).
Axes of the slice: x: 8, y: 2, z: 16, core: 2. Of those that a mesh axis runs over, the one named last changes fastest.
The devices are a block of a 8x16x16 slice.
Arguments:
- tokens: bfloat16 [8192, 2048], P(('grp', 'sp'), 'tp'), parts along dimension 0, may hold values from -40 to 40
- norm_gain: float32 [2, 2048], replicated, may hold values from 0.1 to 1.9
- value_proj: bfloat16 [2, 1024, 2048], P(None, 'tp', 'sp'), may hold values from -0.125 to 0.125
- gate_proj: bfloat16 [2, 1024, 2048], P(None, 'tp', 'sp'), may hold values from -0.125 to 0.125
- conv_taps: float32 [2, 4, 1024], P(None, None, 'tp'), may hold values from -3 to 3
- recur_map: bfloat16 [2, 16, 64, 64], P(None, 'tp'), may hold values from -0.75 to 0.75
- input_map: bfloat16 [2, 16, 64, 64], P(None, 'tp'), may hold values from -0.75 to 0.75
- decay_param: float32 [2, 1024], P(None, 'tp'), may hold values from 3 to 16
- decay_offset: float32 [2, 1024, 4096], P(None, 'tp', 'sp'), may hold values from -3 to 0
- mix_proj: bfloat16 [2, 1024, 2048], P(None, 'sp', 'tp'), may hold values from -0.1875 to 0.1875
Outputs:
- mixed_out: bfloat16 [8192, 2048], P(('grp', 'sp'), 'tp'), parts along dimension 0
There are 2 independent parts, one for each index of `grp`. A program takes and returns all parts, laid end to end along the dimension named above; an argument that names none is the same for every part. Nothing has to cross between parts.
All inputs are finite; a program needn't handle non-finite values.
Results may differ from a plain program's by a relative error of at most 0.013.
Values may be sent and summed in bfloat16 or wider, within the bound.
No kernel may reach another device: no remote copies, remote signals or barrier semaphores. Data moves between devices by JAX's collectives and lax.ppermute only.
A program may use at most 64 MiB of HBM per device.

v0:
```python
import jax
import jax.numpy as jnp
from jax import lax
from jax.experimental import pallas as pl
from jax.experimental.pallas import tpu as pltpu
from jax.sharding import Mesh, PartitionSpec as P


LAYERS = 2
EPS = 1e-06
RATE_SCALE = 8.0
LANES = 128


def one_minus_exp(u):
    series = 1.0
    for n in range(9, 1, -1):
        series = 1.0 + u * series * (1.0 / n)
    return jnp.where(u > -0.5, -u * series, 1.0 - jnp.exp(u))


def scan_kernel(value_ref, before_ref, consts_ref, maps_ref, offset_ref, cum_ref, state_ref, msg_ref):
    channels, tok = value_ref.shape
    taps = 4
    value = value_ref[...].astype(jnp.float32)
    full = jnp.concatenate([before_ref[...].astype(jnp.float32), value], axis=1)
    smoothed = consts_ref[:, taps - 1 : taps] * value
    for back in range(1, taps):
        shifted = pltpu.roll(full, back, axis=1)[:, LANES:]
        smoothed = smoothed + consts_ref[:, taps - 1 - back : taps - back] * shifted
    half = smoothed.astype(jnp.bfloat16)
    gates = lax.dot_general(
        maps_ref[...], half, (((1,), (0,)), ((), ())), preferred_element_type=jnp.float32
    )
    gates = 1.0 / (1.0 + jnp.exp(-gates))
    recur, inputs = gates[:channels], gates[channels:]
    log_decay = consts_ref[:, taps : taps + 1] * recur + offset_ref[...]
    a = jnp.exp(log_decay)
    b = jnp.sqrt(one_minus_exp(2.0 * log_decay)) * inputs * smoothed
    lane = lax.broadcasted_iota(jnp.int32, (channels, tok), 1)
    step = 1
    while step < tok:
        inside = lane >= step
        b = jnp.where(inside, a * pltpu.roll(b, step, axis=1), 0.0) + b
        a = jnp.where(inside, pltpu.roll(a, step, axis=1), 1.0) * a
        step *= 2
    cum_ref[...] = a
    state_ref[...] = b
    last = jnp.concatenate([a[:, tok - LANES :], b[:, tok - LANES :]], axis=0)
    row = last.T[LANES - 1 : LANES, :]
    msg_ref[...] = jnp.broadcast_to(row[None], msg_ref.shape)


def close_kernel(pos_ref, msgs_ref, cum_ref, state_ref, gate_ref, out_ref):
    channels, tok = cum_ref.shape
    count = msgs_ref.shape[0]
    position = pos_ref[0]
    carry = jnp.zeros((1, channels), jnp.float32)
    for s in range(count - 1):
        line = msgs_ref[s]
        step = line[:, :channels] * carry + line[:, channels:]
        carry = jnp.where(s < position, step, carry)
    wide = jnp.broadcast_to(carry, (LANES, channels)).T
    wide = jnp.concatenate([wide] * (tok // LANES), axis=1)
    hidden = state_ref[...] + cum_ref[...] * wide
    gate = gate_ref[...].astype(jnp.float32)
    branch = (hidden * (gate / (1.0 + jnp.exp(-gate)))).astype(jnp.bfloat16)
    out_ref[...] = jnp.broadcast_to(branch[None], out_ref.shape)


def project_kernel(ids_ref, mine_ref, theirs_ref, gain_ref, weight_ref, value_ref, gate_ref):
    chips, tok, width = mine_ref.shape
    channels = value_ref.shape[0]
    product = jnp.zeros((2 * channels, tok), jnp.float32)
    squares = jnp.zeros((tok, width), jnp.float32)
    for side, piece_ref in enumerate((mine_ref, theirs_ref)):
        for chip in range(chips):
            at = side * chips + chip
            wide = piece_ref[chip].astype(jnp.float32)
            squares += wide * wide
            scaled = (wide * gain_ref[ids_ref[0, at]]).astype(jnp.bfloat16)
            weight = weight_ref[ids_ref[1, at], : 2 * channels, :]
            product += lax.dot_general(
                weight, scaled, (((1,), (1,)), ((), ())), preferred_element_type=jnp.float32
            )
    mean = jnp.sum(squares.T, axis=0, keepdims=True) * (1.0 / (2 * chips * width))
    rows = (product * lax.rsqrt(mean + EPS)).astype(jnp.bfloat16)
    value_ref[...] = rows[:channels]
    gate_ref[...] = rows[channels:]


def mix_kernel(ids_ref, mine_ref, theirs_ref, weight_ref, residual_ref, out_ref):
    chips, channels, _ = mine_ref.shape
    first = weight_ref.shape[1] - channels
    mixed = residual_ref[...].astype(jnp.float32)
    for chip in range(chips):
        branch = jnp.concatenate([mine_ref[chip], theirs_ref[chip]], axis=0)
        weight = jnp.concatenate(
            [weight_ref[ids_ref[1, side * chips + chip], first:, :] for side in range(2)], axis=0
        )
        mixed += lax.dot_general(
            branch, weight, (((0,), (0,)), ((), ())), preferred_element_type=jnp.float32
        )
    mixed = mixed.astype(jnp.bfloat16)
    if len(out_ref.shape) == 3:
        mixed = jnp.broadcast_to(mixed[None], out_ref.shape)
    out_ref[...] = mixed


def vmem(n):
    return [pl.BlockSpec(memory_space=pltpu.VMEM)] * n


def smem(n):
    return [pl.BlockSpec(memory_space=pltpu.SMEM)] * n


def project_call(ids, mine, theirs, gains, weights):
    _, tok, _ = mine.shape
    channels = weights.shape[1] // 3
    rows = jax.ShapeDtypeStruct((channels, tok), jnp.bfloat16)
    return pl.pallas_call(
        project_kernel,
        out_shape=(rows, rows),
        in_specs=smem(1) + vmem(4),
        out_specs=tuple(vmem(2)),
        name="project",
    )(ids, mine, theirs, gains, weights)


def mix_call(ids, mine, theirs, weights, residual, copies):
    return pl.pallas_call(
        mix_kernel,
        out_shape=jax.ShapeDtypeStruct(copies + residual.shape, jnp.bfloat16),
        in_specs=smem(1) + vmem(4),
        out_specs=vmem(1)[0],
        name="mix",
    )(ids, mine, theirs, weights, residual)


def scan_call(value, before, consts, maps, offset, count):
    channels, tok = value.shape
    return pl.pallas_call(
        scan_kernel,
        out_shape=(
            jax.ShapeDtypeStruct((channels, tok), jnp.float32),
            jax.ShapeDtypeStruct((channels, tok), jnp.float32),
            jax.ShapeDtypeStruct((count, 1, 2 * channels), jnp.float32),
        ),
        in_specs=vmem(5),
        out_specs=tuple(vmem(3)),
        name="scan",
    )(value, before, consts, maps, offset)


def close_call(position, msgs, cum, state, gate, copies):
    channels, tok = cum.shape
    return pl.pallas_call(
        close_kernel,
        out_shape=jax.ShapeDtypeStruct((copies, channels, tok), jnp.bfloat16),
        in_specs=smem(1) + vmem(4),
        out_specs=vmem(1)[0],
        name="close",
    )(position, msgs, cum, state, gate)


def exchange(copies, axis):
    return lax.all_to_all(copies, axis, split_axis=0, concat_axis=0, tiled=True)


def shift(array, axis, steps):
    count = lax.axis_size(axis)
    return lax.ppermute(array, axis, [(i, (i + steps) % count) for i in range(count)])


NEAR = (-2, -1, 0, 1)


def far_hops(array, axis):
    far = lax.axis_size(axis) // len(NEAR)
    return jnp.stack([array] + [shift(array, axis, len(NEAR) * q) for q in range(1, far)])


def near_hops(held, axis):
    return jnp.concatenate([shift(held, axis, n) if n else held for n in NEAR])


def slot_of(behind, count):
    at = (behind - NEAR[0]) % count
    return at % len(NEAR) * (count // len(NEAR)) + at // len(NEAR)


def local(
    tokens,
    norm_gain,
    value_proj,
    gate_proj,
    conv_taps,
    recur_map,
    input_map,
    decay_param,
    decay_offset,
    mix_proj,
):
    tok_rows, own_cols = tokens.shape
    chips, cores, count = lax.axis_size("x"), lax.axis_size("core"), lax.axis_size("sp")
    chip, core, place = lax.axis_index("x"), lax.axis_index("core"), lax.axis_index("sp")

    def swap(array):
        return shift(array, "core", 1)

    rates = -RATE_SCALE * jax.nn.softplus(-decay_param)
    consts = jnp.concatenate([conv_taps.transpose(0, 2, 1), rates[:, :, None]], axis=2)
    consts = jnp.pad(consts, ((0, 0), (0, 0), (0, LANES - consts.shape[2])))
    maps = jnp.concatenate([recur_map[:, 0], input_map[:, 0]], axis=2).transpose(0, 2, 1)
    gains = norm_gain.reshape(LAYERS, chips * cores, 1, own_cols)
    shards = jnp.concatenate([value_proj, gate_proj, mix_proj], axis=1)

    slots = jnp.arange(chips)
    far = chips // len(NEAR)
    behind = slots % far * len(NEAR) + slots // far + NEAR[0]
    sides = jnp.stack([core, 1 - core])[:, None]
    by_slot = (cores * ((chip - behind) % chips)[None, :] + sides).reshape(-1)
    by_chip = (cores * slots[None, :] + sides).reshape(-1)
    by_hops = slot_of(place - by_chip, count)
    first_ids = jnp.stack([by_slot, by_slot]).astype(jnp.int32)
    plain_ids = jnp.stack([by_chip, by_chip]).astype(jnp.int32)
    hop_ids = jnp.stack([by_chip, by_hops]).astype(jnp.int32)

    first_weights = exchange(jnp.broadcast_to(shards[0], (count, *shards[0].shape)), "sp")
    first_tokens = near_hops(far_hops(tokens, "x"), "x")
    residual = tokens
    for layer in range(LAYERS):
        if layer == 0:
            mine, weights, ids, mix_ids = first_tokens, first_weights, first_ids, plain_ids
        else:
            mine, ids, mix_ids = None, hop_ids, hop_ids
        if mine is None:
            _, held = lax.optimization_barrier((copies, held))
            mine = exchange(copies, "x")
            weights = near_hops(held, "sp")
        theirs = swap(mine)
        value_rows, gate_rows = project_call(ids, mine, theirs, gains[layer], weights)
        before = lax.ppermute(
            value_rows[:, tok_rows - LANES :], "sp", [(i, i + 1) for i in range(count - 1)]
        )
        cum, state, msg = scan_call(
            value_rows, before, consts[layer], maps[layer], decay_offset[layer], count
        )
        msgs = exchange(msg, "sp")
        sent = close_call(place.reshape(1), msgs, cum, state, gate_rows, chips)
        if layer + 1 < LAYERS:
            _, shard = lax.optimization_barrier((sent, shards[layer + 1]))
        mine = exchange(sent, "x")
        if layer + 1 < LAYERS:
            held = far_hops(shard, "sp")
        theirs = swap(mine)
        if layer + 1 < LAYERS:
            copies = mix_call(mix_ids, mine, theirs, weights, residual, (chips,))
            residual = copies[0]
        else:
            residual = mix_call(mix_ids, mine, theirs, weights, residual, ())
    return residual


def solution(mesh):
    grid = mesh.devices
    split = Mesh(grid.reshape(*grid.shape[:2], grid.shape[2] // 2, 2), ("grp", "sp", "x", "core"))
    tp = ("x", "core")
    in_specs = (
        P(("grp", "sp"), tp),
        P(),
        P(None, tp, "sp"),
        P(None, tp, "sp"),
        P(None, None, tp),
        P(None, tp, None, None),
        P(None, tp, None, None),
        P(None, tp),
        P(None, tp, "sp"),
        P(None, "sp", tp),
    )
    return jax.shard_map(
        local, mesh=split, in_specs=in_specs, out_specs=P(("grp", "sp"), tp), check_vma=False
    )
```

profile of v0, /device:TPU:80, one launch (start us, length us, event | category | flops | bytes accessed | tf_op | source)
XLA Modules:
  0.0 251.2 jit_solution(3401343351962870790)
XLA Ops:
  2.6 43.8 %all-to-all-start = ((bf16[16,192,128]{2,1,0:T(8,128)(2,1)}), bf16[16,192,128]{2,1,0:T(8,128)(2,1)S(1)}, u32[]{:S(2)}, u32[]{:S(2)}) async-start(bf16[16,192,128]{2,1,0:T(8,128)(2,1)} %broadcast_in_dim.4), calls=%async_computation | async-start | bytes 1572864 | tf_op jit(solution)/shard_map/all_to_all | solution.py:168
  46.5 8.0 %collective-permute-start = (bf16[256,128]{1,0:T(8,128)(2,1)S(1)}, bf16[256,128]{1,0:T(8,128)(2,1)S(1)}, u32[]{:S(2)}, u32[]{:S(2)}) collective-permute-start(bf16[256,128]{1,0:T(8,128)(2,1)S(1)} %copy-done.6), channel_id=1, source_target_pairs={{0,8},{2,10},{4,12},{6,14},{8,0},{10,2},{12,4},{14,6},{1,9},{3,11}... | collective-permute-start | bytes 196616 | tf_op jit(solution)/shard_map/ppermute | solution.py:173
  57.2 6.6 %collective-permute-start.1 = (bf16[2,256,128]{2,1,0:T(8,128)(2,1)S(1)}, bf16[2,256,128]{2,1,0:T(8,128)(2,1)S(1)}, u32[]{:S(2)}, u32[]{:S(2)}) collective-permute-start(bf16[2,256,128]{2,1,0:T(8,128)(2,1)S(1)} %pad_maximum_fusion.1), channel_id=1, source_target_pairs={{0,12},{2,14},{4,0},{6,2},{8,4},{10,6},{12,8},{14,10},{1,13},{3,15... | collective-permute-start | bytes 393224 | tf_op jit(solution)/shard_map/ppermute | solution.py:173
  64.5 2.9 %collective-permute-start.2 = (bf16[2,256,128]{2,1,0:T(8,128)(2,1)S(1)}, bf16[2,256,128]{2,1,0:T(8,128)(2,1)S(1)}, u32[]{:S(2)}, u32[]{:S(2)}) collective-permute-start(bf16[2,256,128]{2,1,0:T(8,128)(2,1)S(1)} %pad_maximum_fusion.1), channel_id=1, source_target_pairs={{0,14},{2,0},{4,2},{6,4},{8,6},{10,8},{12,10},{14,12},{1,15},{3,1}... | collective-permute-start | bytes 393224 | tf_op jit(solution)/shard_map/ppermute | solution.py:173
  67.6 3.0 %collective-permute-start.3 = (bf16[2,256,128]{2,1,0:T(8,128)(2,1)S(1)}, bf16[2,256,128]{2,1,0:T(8,128)(2,1)S(1)}, u32[]{:S(2)}, u32[]{:S(2)}) collective-permute-start(bf16[2,256,128]{2,1,0:T(8,128)(2,1)S(1)} %pad_maximum_fusion.1), channel_id=1, source_target_pairs={{0,2},{2,4},{4,6},{6,8},{8,10},{10,12},{12,14},{14,0},{1,3},{3,5},... | collective-permute-start | bytes 393224 | tf_op jit(solution)/shard_map/ppermute | solution.py:173
  71.8 3.8 %collective-permute-done.3 = bf16[2,256,128]{2,1,0:T(8,128)(2,1)S(1)} collective-permute-done((bf16[2,256,128]{2,1,0:T(8,128)(2,1)S(1)}, bf16[2,256,128]{2,1,0:T(8,128)(2,1)S(1)}, u32[]{:S(2)}, u32[]{:S(2)}) %collective-permute-start.3) | collective-permute-done | bytes 131104 | tf_op jit(solution)/shard_map/ppermute | solution.py:173
  79.7 5.7 %all-to-all-done.weight_ref = bf16[16,192,128]{2,1,0:T(8,128)(2,1)S(1)} async-done(((bf16[16,192,128]{2,1,0:T(8,128)(2,1)}), bf16[16,192,128]{2,1,0:T(8,128)(2,1)S(1)}, u32[]{:S(2)}, u32[]{:S(2)}) %all-to-all-start) | async-done | bytes 786464 | tf_op jit(solution)/shard_map/all_to_all | solution.py:168
  86.2 2.6 %project.2 = (bf16[64,256]{1,0:T(8,128)(2,1)}, bf16[64,256]{1,0:T(8,128)(2,1)}) custom-call(s32[2,16]{1,0:T(2,128)} %pad_add_fusion.2.ids_ref, bf16[8,256,128]{2,1,0:T(8,128)(2,1)} %copy-done.5, bf16[8,256,128]{2,1,0:T(8,128)(2,1)} %copy-done.8, f32[16,1,128]{2,1,0:T(1,128)} %get-tuple-element.38.gain_ref, bf16[16,192,128]{2,1,0:T(8,128)(2,1)} %copy-done), custom_call_target="tpu_custom_call" | custom-call | tf_op jit(solution)/shard_map/project/pallas_call | solution.py:122
  89.5 4.0 %collective-permute-start.5 = (bf16[64,128]{1,0:T(8,128)(2,1)S(1)}, bf16[64,128]{1,0:T(8,128)(2,1)S(1)}, u32[]{:S(2)}, u32[]{:S(2)}) collective-permute-start(bf16[64,128]{1,0:T(8,128)(2,1)S(1)} %slice.43), channel_id=1, source_target_pairs={{0,16},{16,32},{32,48},{48,64},{64,80},{80,96},{96,112},{112,128},... | collective-permute-start | bytes 49160 | tf_op jit(solution)/shard_map/ppermute | solution.py:244
  98.1 9.3 %all-to-all-start.1 = ((f32[16,1,128]{2,1,0:T(1,128)}), f32[16,1,128]{2,1,0:T(1,128)S(1)}, u32[]{:S(2)}, u32[]{:S(2)}) async-start(f32[16,1,128]{2,1,0:T(1,128)} %get-tuple-element.18), calls=%async_computation.1 | async-start | bytes 16384 | tf_op jit(solution)/shard_map/all_to_all | solution.py:168
  107.4 12.2 %all-to-all-done.1.msgs_ref = f32[16,1,128]{2,1,0:T(1,128)S(1)} async-done(((f32[16,1,128]{2,1,0:T(1,128)}), f32[16,1,128]{2,1,0:T(1,128)S(1)}, u32[]{:S(2)}, u32[]{:S(2)}) %all-to-all-start.1) | async-done | bytes 8224 | tf_op jit(solution)/shard_map/all_to_all | solution.py:168
  122.0 7.3 %all-to-all-start.2 = ((bf16[8,64,256]{2,1,0:T(8,128)(2,1)}), bf16[8,64,256]{2,1,0:T(8,128)(2,1)S(1)}, u32[]{:S(2)}, u32[]{:S(2)}) async-start(bf16[8,64,256]{2,1,0:T(8,128)(2,1)} %close.2), calls=%async_computation.2 | async-start | bytes 524288 | tf_op jit(solution)/shard_map/all_to_all | solution.py:168
  129.4 10.4 %all-to-all-done.2.mine_ref = bf16[8,64,256]{2,1,0:T(8,128)(2,1)S(1)} async-done(((bf16[8,64,256]{2,1,0:T(8,128)(2,1)}), bf16[8,64,256]{2,1,0:T(8,128)(2,1)S(1)}, u32[]{:S(2)}, u32[]{:S(2)}) %all-to-all-start.2) | async-done | bytes 262176 | tf_op jit(solution)/shard_map/all_to_all | solution.py:168
  146.3 3.7 %all-to-all-start.3 = ((bf16[8,256,128]{2,1,0:T(8,128)(2,1)}), bf16[8,256,128]{2,1,0:T(8,128)(2,1)S(1)}, u32[]{:S(2)}, u32[]{:S(2)}) async-start(bf16[8,256,128]{2,1,0:T(8,128)(2,1)} %mix.2), calls=%async_computation.3 | async-start | bytes 1048576 | tf_op jit(solution)/shard_map/all_to_all | solution.py:168
  150.0 2.6 %collective-permute-start.8 = (bf16[192,128]{1,0:T(8,128)(2,1)S(1)}, bf16[192,128]{1,0:T(8,128)(2,1)S(1)}, u32[]{:S(2)}, u32[]{:S(2)}) collective-permute-start(bf16[192,128]{1,0:T(8,128)(2,1)S(1)} %get-tuple-element.22), channel_id=1, source_target_pairs={{0,64},{16,80},{32,96},{48,112},{64,128},{80,144},{96,160},{112,17... | collective-permute-start | bytes 147464 | tf_op jit(solution)/shard_map/ppermute | solution.py:173
  152.6 7.4 %collective-permute-start.9 = (bf16[192,128]{1,0:T(8,128)(2,1)S(1)}, bf16[192,128]{1,0:T(8,128)(2,1)S(1)}, u32[]{:S(2)}, u32[]{:S(2)}) collective-permute-start(bf16[192,128]{1,0:T(8,128)(2,1)S(1)} %get-tuple-element.22), channel_id=1, source_target_pairs={{0,128},{16,144},{32,160},{48,176},{64,192},{80,208},{96,224},{112... | collective-permute-start | bytes 147464 | tf_op jit(solution)/shard_map/ppermute | solution.py:173
  162.5 4.9 %collective-permute-done.9 = bf16[192,128]{1,0:T(8,128)(2,1)S(1)} collective-permute-done((bf16[192,128]{1,0:T(8,128)(2,1)S(1)}, bf16[192,128]{1,0:T(8,128)(2,1)S(1)}, u32[]{:S(2)}, u32[]{:S(2)}) %collective-permute-start.9) | collective-permute-done | bytes 49184 | tf_op jit(solution)/shard_map/ppermute | solution.py:173
  167.4 6.7 %collective-permute-done.10 = bf16[192,128]{1,0:T(8,128)(2,1)S(1)} collective-permute-done((bf16[192,128]{1,0:T(8,128)(2,1)S(1)}, bf16[192,128]{1,0:T(8,128)(2,1)S(1)}, u32[]{:S(2)}, u32[]{:S(2)}) %collective-permute-start.10) | collective-permute-done | bytes 49184 | tf_op jit(solution)/shard_map/ppermute | solution.py:173
  180.2 4.0 %collective-permute-start.13 = (bf16[4,192,128]{2,1,0:T(8,128)(2,1)S(1)}, bf16[4,192,128]{2,1,0:T(8,128)(2,1)S(1)}, u32[]{:S(2)}, u32[]{:S(2)}) collective-permute-start(bf16[4,192,128]{2,1,0:T(8,128)(2,1)S(1)} %pad_maximum_fusion), channel_id=1, source_target_pairs={{0,16},{16,32},{32,48},{48,64},{64,80},{80,96},{96,112},{112,128},... | collective-permute-start | bytes 589832 | tf_op jit(solution)/shard_map/ppermute | solution.py:173
  184.1 2.6 %collective-permute-done.11 = bf16[4,192,128]{2,1,0:T(8,128)(2,1)S(1)} collective-permute-done((bf16[4,192,128]{2,1,0:T(8,128)(2,1)S(1)}, bf16[4,192,128]{2,1,0:T(8,128)(2,1)S(1)}, u32[]{:S(2)}, u32[]{:S(2)}) %collective-permute-start.11) | collective-permute-done | bytes 196640 | tf_op jit(solution)/shard_map/ppermute | solution.py:173
  191.8 2.6 %project.3 = (bf16[64,256]{1,0:T(8,128)(2,1)}, bf16[64,256]{1,0:T(8,128)(2,1)}) custom-call(s32[2,16]{1,0:T(2,128)} %get-tuple-element.42.ids_ref, bf16[8,256,128]{2,1,0:T(8,128)(2,1)} %copy-done.2, bf16[8,256,128]{2,1,0:T(8,128)(2,1)} %copy-done.7, f32[16,1,128]{2,1,0:T(1,128)} %get-tuple-element.37.gain_ref, bf16[16,192,128]{2,1,0:T(8,128)(2,1)} %copy-done.1), custom_call_target="tpu_custom_call" | custom-call | tf_op jit(solution)/shard_map/project/pallas_call | solution.py:122
  195.1 3.2 %collective-permute-start.14 = (bf16[64,128]{1,0:T(8,128)(2,1)S(1)}, bf16[64,128]{1,0:T(8,128)(2,1)S(1)}, u32[]{:S(2)}, u32[]{:S(2)}) collective-permute-start(bf16[64,128]{1,0:T(8,128)(2,1)S(1)} %slice.49), channel_id=1, source_target_pairs={{0,16},{16,32},{32,48},{48,64},{64,80},{80,96},{96,112},{112,128},... | collective-permute-start | bytes 49160 | tf_op jit(solution)/shard_map/ppermute | solution.py:244
  202.9 22.9 %all_to_all.30.msgs_ref = f32[16,1,128]{2,1,0:T(1,128)} all-to-all(f32[16,1,128]{2,1,0:T(1,128)} %get-tuple-element.25), channel_id=1, replica_groups=mesh['grp'=2,'sp'=16,'x'=8,'core'=2] {'sp'}, dimensions={0} | all-to-all | bytes 16384 | tf_op jit(solution)/shard_map/all_to_all | solution.py:168
  227.5 17.2 %all_to_all.31.mine_ref = bf16[8,64,256]{2,1,0:T(8,128)(2,1)S(1)} all-to-all(bf16[8,64,256]{2,1,0:T(8,128)(2,1)} %close.3), channel_id=1, replica_groups=mesh['grp'=2,'sp'=16,'x'=8,'core'=2] {'x'}, dimensions={0} | all-to-all | bytes 524288 | tf_op jit(solution)/shard_map/all_to_all | solution.py:168
  (108 shorter events, 53.7 us)
Async XLA Ops:
  2.6 43.8 %copy-start.6 = (bf16[256,128]{1,0:T(8,128)(2,1)S(1)}, bf16[256,128]{1,0:T(8,128)(2,1)}, u32[]{:S(2)}) copy-start(bf16[256,128]{1,0:T(8,128)(2,1)} %residual_ref.1) | copy-start | bytes 196612
  2.6 52.0 %copy-start.17 = (f32[2,2048]{1,0:T(2,128)S(1)}, f32[2,2048]{1,0:T(2,128)}, u32[]{:S(2)}) copy-start(f32[2,2048]{1,0:T(2,128)} %param.11) | copy-start | bytes 49156
  2.6 82.7 %all-to-all-start = ((bf16[16,192,128]{2,1,0:T(8,128)(2,1)}), bf16[16,192,128]{2,1,0:T(8,128)(2,1)S(1)}, u32[]{:S(2)}, u32[]{:S(2)}) async-start(bf16[16,192,128]{2,1,0:T(8,128)(2,1)} %broadcast_in_dim.4), calls=%async_computation | async-start | bytes 1572864 | tf_op jit(solution)/shard_map/all_to_all | solution.py:168
  46.5 10.7 %collective-permute-start = (bf16[256,128]{1,0:T(8,128)(2,1)S(1)}, bf16[256,128]{1,0:T(8,128)(2,1)S(1)}, u32[]{:S(2)}, u32[]{:S(2)}) collective-permute-start(bf16[256,128]{1,0:T(8,128)(2,1)S(1)} %copy-done.6), channel_id=1, source_target_pairs={{0,8},{2,10},{4,12},{6,14},{8,0},{10,2},{12,4},{14,6},{1,9},{3,11}... | collective-permute-start | bytes 196616 | tf_op jit(solution)/shard_map/ppermute | solution.py:173
  57.2 13.4 %collective-permute-start.1 = (bf16[2,256,128]{2,1,0:T(8,128)(2,1)S(1)}, bf16[2,256,128]{2,1,0:T(8,128)(2,1)S(1)}, u32[]{:S(2)}, u32[]{:S(2)}) collective-permute-start(bf16[2,256,128]{2,1,0:T(8,128)(2,1)S(1)} %pad_maximum_fusion.1), channel_id=1, source_target_pairs={{0,12},{2,14},{4,0},{6,2},{8,4},{10,6},{12,8},{14,10},{1,13},{3,15... | collective-permute-start | bytes 393224 | tf_op jit(solution)/shard_map/ppermute | solution.py:173
  64.5 7.3 %collective-permute-start.2 = (bf16[2,256,128]{2,1,0:T(8,128)(2,1)S(1)}, bf16[2,256,128]{2,1,0:T(8,128)(2,1)S(1)}, u32[]{:S(2)}, u32[]{:S(2)}) collective-permute-start(bf16[2,256,128]{2,1,0:T(8,128)(2,1)S(1)} %pad_maximum_fusion.1), channel_id=1, source_target_pairs={{0,14},{2,0},{4,2},{6,4},{8,6},{10,8},{12,10},{14,12},{1,15},{3,1}... | collective-permute-start | bytes 393224 | tf_op jit(solution)/shard_map/ppermute | solution.py:173
  67.6 8.1 %collective-permute-start.3 = (bf16[2,256,128]{2,1,0:T(8,128)(2,1)S(1)}, bf16[2,256,128]{2,1,0:T(8,128)(2,1)S(1)}, u32[]{:S(2)}, u32[]{:S(2)}) collective-permute-start(bf16[2,256,128]{2,1,0:T(8,128)(2,1)S(1)} %pad_maximum_fusion.1), channel_id=1, source_target_pairs={{0,2},{2,4},{4,6},{6,8},{8,10},{10,12},{12,14},{14,0},{1,3},{3,5},... | collective-permute-start | bytes 393224 | tf_op jit(solution)/shard_map/ppermute | solution.py:173
  75.7 9.7 %copy-start.5 = (bf16[8,256,128]{2,1,0:T(8,128)(2,1)}, bf16[8,256,128]{2,1,0:T(8,128)(2,1)S(1)}, u32[]{:S(2)}) copy-start(bf16[8,256,128]{2,1,0:T(8,128)(2,1)S(1)} %constant_dynamic-update-slice_fusion.mine_ref) | copy-start | bytes 1572868
  75.7 4.0 %collective-permute-start.4 = (bf16[8,256,128]{2,1,0:T(8,128)(2,1)S(1)}, bf16[8,256,128]{2,1,0:T(8,128)(2,1)S(1)}, u32[]{:S(2)}, u32[]{:S(2)}) collective-permute-start(bf16[8,256,128]{2,1,0:T(8,128)(2,1)S(1)} %constant_dynamic-update-slice_fusion.mine_ref), channel_id=1, source_target_pairs={{0,1},{1,0},{2,3},{3,2},{4,5},{5,4},{6,7},{7,6},{8,9},{9,8},{10,11... | collective-permute-start | bytes 1572872 | tf_op jit(solution)/shard_map/ppermute | solution.py:173
  89.5 5.4 %collective-permute-start.5 = (bf16[64,128]{1,0:T(8,128)(2,1)S(1)}, bf16[64,128]{1,0:T(8,128)(2,1)S(1)}, u32[]{:S(2)}, u32[]{:S(2)}) collective-permute-start(bf16[64,128]{1,0:T(8,128)(2,1)S(1)} %slice.43), channel_id=1, source_target_pairs={{0,16},{16,32},{32,48},{48,64},{64,80},{80,96},{96,112},{112,128},... | collective-permute-start | bytes 49160 | tf_op jit(solution)/shard_map/ppermute | solution.py:244
  98.1 21.5 %all-to-all-start.1 = ((f32[16,1,128]{2,1,0:T(1,128)}), f32[16,1,128]{2,1,0:T(1,128)S(1)}, u32[]{:S(2)}, u32[]{:S(2)}) async-start(f32[16,1,128]{2,1,0:T(1,128)} %get-tuple-element.18), calls=%async_computation.1 | async-start | bytes 16384 | tf_op jit(solution)/shard_map/all_to_all | solution.py:168
  122.0 17.8 %all-to-all-start.2 = ((bf16[8,64,256]{2,1,0:T(8,128)(2,1)}), bf16[8,64,256]{2,1,0:T(8,128)(2,1)S(1)}, u32[]{:S(2)}, u32[]{:S(2)}) async-start(bf16[8,64,256]{2,1,0:T(8,128)(2,1)} %close.2), calls=%async_computation.2 | async-start | bytes 524288 | tf_op jit(solution)/shard_map/all_to_all | solution.py:168
  139.8 3.4 %collective-permute-start.6 = (bf16[8,64,256]{2,1,0:T(8,128)(2,1)S(1)}, bf16[8,64,256]{2,1,0:T(8,128)(2,1)S(1)}, u32[]{:S(2)}, u32[]{:S(2)}) collective-permute-start(bf16[8,64,256]{2,1,0:T(8,128)(2,1)S(1)} %all-to-all-done.2.mine_ref), channel_id=1, source_target_pairs={{0,1},{1,0},{2,3},{3,2},{4,5},{5,4},{6,7},{7,6},{8,9},{9,8},{10,11... | collective-permute-start | bytes 786440 | tf_op jit(solution)/shard_map/ppermute | solution.py:173
  146.3 31.9 %all-to-all-start.3 = ((bf16[8,256,128]{2,1,0:T(8,128)(2,1)}), bf16[8,256,128]{2,1,0:T(8,128)(2,1)S(1)}, u32[]{:S(2)}, u32[]{:S(2)}) async-start(bf16[8,256,128]{2,1,0:T(8,128)(2,1)} %mix.2), calls=%async_computation.3 | async-start | bytes 1048576 | tf_op jit(solution)/shard_map/all_to_all | solution.py:168
  150.0 12.4 %collective-permute-start.8 = (bf16[192,128]{1,0:T(8,128)(2,1)S(1)}, bf16[192,128]{1,0:T(8,128)(2,1)S(1)}, u32[]{:S(2)}, u32[]{:S(2)}) collective-permute-start(bf16[192,128]{1,0:T(8,128)(2,1)S(1)} %get-tuple-element.22), channel_id=1, source_target_pairs={{0,64},{16,80},{32,96},{48,112},{64,128},{80,144},{96,160},{112,17... | collective-permute-start | bytes 147464 | tf_op jit(solution)/shard_map/ppermute | solution.py:173
  152.6 14.7 %collective-permute-start.9 = (bf16[192,128]{1,0:T(8,128)(2,1)S(1)}, bf16[192,128]{1,0:T(8,128)(2,1)S(1)}, u32[]{:S(2)}, u32[]{:S(2)}) collective-permute-start(bf16[192,128]{1,0:T(8,128)(2,1)S(1)} %get-tuple-element.22), channel_id=1, source_target_pairs={{0,128},{16,144},{32,160},{48,176},{64,192},{80,208},{96,224},{112... | collective-permute-start | bytes 147464 | tf_op jit(solution)/shard_map/ppermute | solution.py:173
  160.0 14.1 %collective-permute-start.10 = (bf16[192,128]{1,0:T(8,128)(2,1)S(1)}, bf16[192,128]{1,0:T(8,128)(2,1)S(1)}, u32[]{:S(2)}, u32[]{:S(2)}) collective-permute-start(bf16[192,128]{1,0:T(8,128)(2,1)S(1)} %get-tuple-element.22), channel_id=1, source_target_pairs={{0,192},{16,208},{32,224},{48,240},{64,0},{80,16},{96,32},{112,48}... | collective-permute-start | bytes 147464 | tf_op jit(solution)/shard_map/ppermute | solution.py:173
  174.1 12.6 %collective-permute-start.11 = (bf16[4,192,128]{2,1,0:T(8,128)(2,1)S(1)}, bf16[4,192,128]{2,1,0:T(8,128)(2,1)S(1)}, u32[]{:S(2)}, u32[]{:S(2)}) collective-permute-start(bf16[4,192,128]{2,1,0:T(8,128)(2,1)S(1)} %pad_maximum_fusion), channel_id=1, source_target_pairs={{0,224},{16,240},{32,0},{48,16},{64,32},{80,48},{96,64},{112,80},{... | collective-permute-start | bytes 589832 | tf_op jit(solution)/shard_map/ppermute | solution.py:173
  176.2 13.1 %collective-permute-start.12 = (bf16[4,192,128]{2,1,0:T(8,128)(2,1)S(1)}, bf16[4,192,128]{2,1,0:T(8,128)(2,1)S(1)}, u32[]{:S(2)}, u32[]{:S(2)}) collective-permute-start(bf16[4,192,128]{2,1,0:T(8,128)(2,1)S(1)} %pad_maximum_fusion), channel_id=1, source_target_pairs={{0,240},{16,0},{32,16},{48,32},{64,48},{80,64},{96,80},{112,96},{1... | collective-permute-start | bytes 589832 | tf_op jit(solution)/shard_map/ppermute | solution.py:173
  178.2 11.2 %copy-start.2 = (bf16[8,256,128]{2,1,0:T(8,128)(2,1)}, bf16[8,256,128]{2,1,0:T(8,128)(2,1)S(1)}, u32[]{:S(2)}) copy-start(bf16[8,256,128]{2,1,0:T(8,128)(2,1)S(1)} %all-to-all-done.3.mine_ref) | copy-start | bytes 1572868
  178.2 12.6 %collective-permute-start.7 = (bf16[8,256,128]{2,1,0:T(8,128)(2,1)S(1)}, bf16[8,256,128]{2,1,0:T(8,128)(2,1)S(1)}, u32[]{:S(2)}, u32[]{:S(2)}) collective-permute-start(bf16[8,256,128]{2,1,0:T(8,128)(2,1)S(1)} %all-to-all-done.3.mine_ref), channel_id=1, source_target_pairs={{0,1},{1,0},{2,3},{3,2},{4,5},{5,4},{6,7},{7,6},{8,9},{9,8},{10,11... | collective-permute-start | bytes 1572872 | tf_op jit(solution)/shard_map/ppermute | solution.py:173
  180.2 10.6 %collective-permute-start.13 = (bf16[4,192,128]{2,1,0:T(8,128)(2,1)S(1)}, bf16[4,192,128]{2,1,0:T(8,128)(2,1)S(1)}, u32[]{:S(2)}, u32[]{:S(2)}) collective-permute-start(bf16[4,192,128]{2,1,0:T(8,128)(2,1)S(1)} %pad_maximum_fusion), channel_id=1, source_target_pairs={{0,16},{16,32},{32,48},{48,64},{64,80},{80,96},{96,112},{112,128},... | collective-permute-start | bytes 589832 | tf_op jit(solution)/shard_map/ppermute | solution.py:173
  195.1 4.6 %collective-permute-start.14 = (bf16[64,128]{1,0:T(8,128)(2,1)S(1)}, bf16[64,128]{1,0:T(8,128)(2,1)S(1)}, u32[]{:S(2)}, u32[]{:S(2)}) collective-permute-start(bf16[64,128]{1,0:T(8,128)(2,1)S(1)} %slice.49), channel_id=1, source_target_pairs={{0,16},{16,32},{32,48},{48,64},{64,80},{80,96},{96,112},{112,128},... | collective-permute-start | bytes 49160 | tf_op jit(solution)/shard_map/ppermute | solution.py:244
  244.8 3.4 %collective-permute-start.15 = (bf16[8,64,256]{2,1,0:T(8,128)(2,1)S(1)}, bf16[8,64,256]{2,1,0:T(8,128)(2,1)S(1)}, u32[]{:S(2)}, u32[]{:S(2)}) collective-permute-start(bf16[8,64,256]{2,1,0:T(8,128)(2,1)S(1)} %all_to_all.31.mine_ref), channel_id=1, source_target_pairs={{0,1},{1,0},{2,3},{3,2},{4,5},{5,4},{6,7},{7,6},{8,9},{9,8},{10,11... | collective-permute-start | bytes 786440 | tf_op jit(solution)/shard_map/ppermute | solution.py:173
  (18 other events, 34.4 us)
where the time goes:
time: 254 us; the launch traced here: 251 us
  starting transfers between devices  120 us (47%)
  waiting for transfers between devices  55.6 us (22%)
  blocking collectives  40.1 us (16%)
  Pallas kernels  18.5 us (7%)
  local copies, waits for them, and re-layouts  15.2 us (6%)
    all_to_all x4, starting transfers between devices, exchange(): return lax.all_to_all(copies, axis, split_axis=0, concat_axis=0, tiled=True)  64.1 us
    ppermute x14, starting transfers between devices, shift(): lax.ppermute(array, axis, [(i, (i + steps) % count) for i in range(count)])  48.8 us
    all_to_all x2, blocking collectives, exchange(): return lax.all_to_all(copies, axis, split_axis=0, concat_axis=0, tiled=True)  40.1 us
    all_to_all x4, waiting for transfers between devices, exchange(): return lax.all_to_all(copies, axis, split_axis=0, concat_axis=0, tiled=True)  28.3 us
    ppermute x14, waiting for transfers between devices, shift(): lax.ppermute(array, axis, [(i, (i + steps) % count) for i in range(count)])  25.1 us
    unnamed x56, local copies, waits for them, and re-layouts  8.36 us
    ppermute x2, starting transfers between devices, local(): lax.ppermute(value_rows[:, tok_rows - LANES:], 'sp', [(i, i + 1) for i in...  7.15 us
    pallas_call x2, Pallas kernels, project_call(): pl.pallas_call(project_kernel, out_shape=(rows, rows), in_specs=smem(1) +...  5.16 us
  transfers between devices with their start and end apart: 20, of which 14 were waited for; matrix products, arithmetic and copies ran while one was open for 2% of the time, Pallas kernels for 0%

commit v1 on v0

--- a/solution.py
+++ b/solution.py
@@ -1,3 +1,5 @@
+import functools
+
 import jax
 import jax.numpy as jnp
 from jax import lax
@@ -19,22 +21,25 @@
     return jnp.where(u > -0.5, -u * series, 1.0 - jnp.exp(u))
 
 
-def scan_kernel(value_ref, before_ref, consts_ref, maps_ref, offset_ref, cum_ref, state_ref, msg_ref):
+def scan_kernel(
+    layer, value_ref, before_ref, consts_ref, maps_ref, offset_ref, cum_ref, state_ref, msg_ref
+):
     channels, tok = value_ref.shape
     taps = 4
     value = value_ref[...].astype(jnp.float32)
     full = jnp.concatenate([before_ref[...].astype(jnp.float32), value], axis=1)
-    smoothed = consts_ref[:, taps - 1 : taps] * value
+    consts = consts_ref[layer]
+    smoothed = consts[:, taps - 1 : taps] * value
     for back in range(1, taps):
         shifted = pltpu.roll(full, back, axis=1)[:, LANES:]
-        smoothed = smoothed + consts_ref[:, taps - 1 - back : taps - back] * shifted
+        smoothed = smoothed + consts[:, taps - 1 - back : taps - back] * shifted
     half = smoothed.astype(jnp.bfloat16)
     gates = lax.dot_general(
-        maps_ref[...], half, (((1,), (0,)), ((), ())), preferred_element_type=jnp.float32
+        maps_ref[layer], half, (((1,), (0,)), ((), ())), preferred_element_type=jnp.float32
     )
     gates = 1.0 / (1.0 + jnp.exp(-gates))
     recur, inputs = gates[:channels], gates[channels:]
-    log_decay = consts_ref[:, taps : taps + 1] * recur + offset_ref[...]
+    log_decay = consts[:, taps : taps + 1] * recur + offset_ref[layer]
     a = jnp.exp(log_decay)
     b = jnp.sqrt(one_minus_exp(2.0 * log_decay)) * inputs * smoothed
     lane = lax.broadcasted_iota(jnp.int32, (channels, tok), 1)
@@ -68,7 +73,9 @@
     out_ref[...] = jnp.broadcast_to(branch[None], out_ref.shape)
 
 
-def project_kernel(ids_ref, mine_ref, theirs_ref, gain_ref, weight_ref, value_ref, gate_ref):
+def project_kernel(
+    layer, ids_ref, mine_ref, theirs_ref, gain_ref, weight_ref, value_ref, gate_ref, tail_ref
+):
     chips, tok, width = mine_ref.shape
     channels = value_ref.shape[0]
     product = jnp.zeros((2 * channels, tok), jnp.float32)
@@ -78,7 +85,7 @@
             at = side * chips + chip
             wide = piece_ref[chip].astype(jnp.float32)
             squares += wide * wide
-            scaled = (wide * gain_ref[ids_ref[0, at]]).astype(jnp.bfloat16)
+            scaled = (wide * gain_ref[layer, ids_ref[0, at]]).astype(jnp.bfloat16)
             weight = weight_ref[ids_ref[1, at], : 2 * channels, :]
             product += lax.dot_general(
                 weight, scaled, (((1,), (1,)), ((), ())), preferred_element_type=jnp.float32
@@ -87,9 +94,10 @@
     rows = (product * lax.rsqrt(mean + EPS)).astype(jnp.bfloat16)
     value_ref[...] = rows[:channels]
     gate_ref[...] = rows[channels:]
-
-
-def mix_kernel(ids_ref, mine_ref, theirs_ref, weight_ref, residual_ref, out_ref):
+    tail_ref[...] = rows[:channels, tok - LANES :]
+
+
+def mix_kernel(ids_ref, mine_ref, theirs_ref, weight_ref, residual_ref, out_ref, *copies_ref):
     chips, channels, _ = mine_ref.shape
     first = weight_ref.shape[1] - channels
     mixed = residual_ref[...].astype(jnp.float32)
@@ -102,9 +110,9 @@
             branch, weight, (((0,), (0,)), ((), ())), preferred_element_type=jnp.float32
         )
     mixed = mixed.astype(jnp.bfloat16)
-    if len(out_ref.shape) == 3:
-        mixed = jnp.broadcast_to(mixed[None], out_ref.shape)
     out_ref[...] = mixed
+    for ref in copies_ref:
+        ref[...] = jnp.broadcast_to(mixed[None], ref.shape)
 
 
 def vmem(n):
@@ -115,33 +123,34 @@
     return [pl.BlockSpec(memory_space=pltpu.SMEM)] * n
 
 
-def project_call(ids, mine, theirs, gains, weights):
+def project_call(layer, ids, mine, theirs, gains, weights):
     _, tok, _ = mine.shape
     channels = weights.shape[1] // 3
     rows = jax.ShapeDtypeStruct((channels, tok), jnp.bfloat16)
     return pl.pallas_call(
-        project_kernel,
-        out_shape=(rows, rows),
+        functools.partial(project_kernel, layer),
+        out_shape=(rows, rows, jax.ShapeDtypeStruct((channels, LANES), jnp.bfloat16)),
         in_specs=smem(1) + vmem(4),
-        out_specs=tuple(vmem(2)),
+        out_specs=tuple(vmem(3)),
         name="project",
     )(ids, mine, theirs, gains, weights)
 
 
 def mix_call(ids, mine, theirs, weights, residual, copies):
+    shapes = [residual.shape] + ([(copies, *residual.shape)] if copies else [])
     return pl.pallas_call(
         mix_kernel,
-        out_shape=jax.ShapeDtypeStruct(copies + residual.shape, jnp.bfloat16),
+        out_shape=[jax.ShapeDtypeStruct(shape, jnp.bfloat16) for shape in shapes],
         in_specs=smem(1) + vmem(4),
-        out_specs=vmem(1)[0],
+        out_specs=vmem(len(shapes)),
         name="mix",
     )(ids, mine, theirs, weights, residual)
 
 
-def scan_call(value, before, consts, maps, offset, count):
+def scan_call(layer, value, before, consts, maps, offset, count):
     channels, tok = value.shape
     return pl.pallas_call(
-        scan_kernel,
+        functools.partial(scan_kernel, layer),
         out_shape=(
             jax.ShapeDtypeStruct((channels, tok), jnp.float32),
             jax.ShapeDtypeStruct((channels, tok), jnp.float32),
@@ -162,6 +171,22 @@
         out_specs=vmem(1)[0],
         name="close",
     )(position, msgs, cum, state, gate)
+
+
+def tick_kernel(ids_ref, out_ref):
+    for side in range(ids_ref.shape[0]):
+        for at in range(ids_ref.shape[1]):
+            out_ref[side, at] = ids_ref[side, at]
+
+
+def tick_call(ids):
+    return pl.pallas_call(
+        tick_kernel,
+        out_shape=jax.ShapeDtypeStruct(ids.shape, ids.dtype),
+        in_specs=smem(1),
+        out_specs=smem(1)[0],
+        name="copy_ids",
+    )(ids)
 
 
 def exchange(copies, axis):
@@ -202,7 +227,7 @@
     decay_offset,
     mix_proj,
 ):
-    tok_rows, own_cols = tokens.shape
+    _, own_cols = tokens.shape
     chips, cores, count = lax.axis_size("x"), lax.axis_size("core"), lax.axis_size("sp")
     chip, core, place = lax.axis_index("x"), lax.axis_index("core"), lax.axis_index("sp")
 
@@ -225,7 +250,8 @@
     by_hops = slot_of(place - by_chip, count)
     first_ids = jnp.stack([by_slot, by_slot]).astype(jnp.int32)
     plain_ids = jnp.stack([by_chip, by_chip]).astype(jnp.int32)
-    hop_ids = jnp.stack([by_chip, by_hops]).astype(jnp.int32)
+    hop_ids = tick_call(jnp.stack([by_chip, by_hops]).astype(jnp.int32))
+    hop_ids = tick_call(hop_ids)
 
     first_weights = exchange(jnp.broadcast_to(shards[0], (count, *shards[0].shape)), "sp")
     first_tokens = near_hops(far_hops(tokens, "x"), "x")
@@ -234,32 +260,28 @@
         if layer == 0:
             mine, weights, ids, mix_ids = first_tokens, first_weights, first_ids, plain_ids
         else:
-            mine, ids, mix_ids = None, hop_ids, hop_ids
+            mine, weights, ids, mix_ids = None, later_weights, hop_ids, hop_ids
         if mine is None:
-            _, held = lax.optimization_barrier((copies, held))
-            mine = exchange(copies, "x")
-            weights = near_hops(held, "sp")
+            mine = exchange(copies[0], "x")
         theirs = swap(mine)
-        value_rows, gate_rows = project_call(ids, mine, theirs, gains[layer], weights)
-        before = lax.ppermute(
-            value_rows[:, tok_rows - LANES :], "sp", [(i, i + 1) for i in range(count - 1)]
+        value_rows, gate_rows, tail = project_call(
+            layer, ids, mine, theirs, gains, weights
         )
-        cum, state, msg = scan_call(
-            value_rows, before, consts[layer], maps[layer], decay_offset[layer], count
-        )
+        before = lax.ppermute(tail, "sp", [(i, i + 1) for i in range(count - 1)])
+        cum, state, msg = scan_call(layer, value_rows, before, consts, maps, decay_offset, count)
         msgs = exchange(msg, "sp")
+        if layer + 1 < LAYERS:
+            _, shard = lax.optimization_barrier((msg, shards[layer + 1]))
+            held = far_hops(shard, "sp")
         sent = close_call(place.reshape(1), msgs, cum, state, gate_rows, chips)
-        if layer + 1 < LAYERS:
-            _, shard = lax.optimization_barrier((sent, shards[layer + 1]))
         mine = exchange(sent, "x")
         if layer + 1 < LAYERS:
-            held = far_hops(shard, "sp")
+            _, held = lax.optimization_barrier((sent, held))
+            later_weights = near_hops(held, "sp")
         theirs = swap(mine)
-        if layer + 1 < LAYERS:
-            copies = mix_call(mix_ids, mine, theirs, weights, residual, (chips,))
-            residual = copies[0]
-        else:
-            residual = mix_call(mix_ids, mine, theirs, weights, residual, ())
+        residual, *copies = mix_call(
+            mix_ids, mine, theirs, weights, residual, chips if layer + 1 < LAYERS else 0
+        )
     return residual
 
 

time: 254 us -> 256 us (level)
  local copies, waits for them, and re-layouts: 15.2 us -> 11 us
  waiting for transfers between devices: 55.6 us -> 58.6 us
  Pallas kernels: 18.5 us -> 21.3 us
    squeeze x6 -> x1, local copies, waits for them, and re-layouts: 3.99 us -> 0.01 us  [local(): _, shard = lax.optimization_barrier((msg, shards[layer + 1]))]
    ppermute x14, waiting for transfers between devices: 25.1 us -> 28.2 us  [shift(): lax.ppermute(array, axis, [(i, (i + steps) % count) for i in range(count)])]
    pallas_call x6 -> x8, Pallas kernels: 14.9 us -> 17.7 us  [the longest x2 5.26 us: scan_call(): pl.pallas_call(functools.partial(scan_kernel, layer), out_shape=(jax.Shap...]
    unnamed x56 -> x54, local copies, waits for them, and re-layouts: 8.36 us -> 8.38 us
  transfers between devices with their start and end apart: 20 -> 20, of which waited for: 14 -> 15; matrix products, arithmetic and copies ran while one was open for 2% -> 2% of each run, Pallas kernels for 0% -> 1%
where the time goes in v1:
time: 256 us; the launch traced here: 254 us
  starting transfers between devices  120 us (47%)
  waiting for transfers between devices  58.6 us (23%)
  blocking collectives  40.5 us (16%)
  Pallas kernels  21.3 us (8%)
  local copies, waits for them, and re-layouts  11 us (4%)
    all_to_all x4, starting transfers between devices, exchange(): return lax.all_to_all(copies, axis, split_axis=0, concat_axis=0, tiled=True)  64.1 us
    ppermute x14, starting transfers between devices, shift(): lax.ppermute(array, axis, [(i, (i + steps) % count) for i in range(count)])  48.9 us
    all_to_all x2, blocking collectives, exchange(): return lax.all_to_all(copies, axis, split_axis=0, concat_axis=0, tiled=True)  40.5 us
    ppermute x14, waiting for transfers between devices, shift(): lax.ppermute(array, axis, [(i, (i + steps) % count) for i in range(count)])  28.2 us
    all_to_all x4, waiting for transfers between devices, exchange(): return lax.all_to_all(copies, axis, split_axis=0, concat_axis=0, tiled=True)  28 us
    unnamed x54, local copies, waits for them, and re-layouts  8.38 us
    ppermute x2, starting transfers between devices, local(): before = lax.ppermute(tail, 'sp', [(i, i + 1) for i in range(count - 1)])  6.7 us
    pallas_call x2, Pallas kernels, scan_call(): pl.pallas_call(functools.partial(scan_kernel, layer), out_shape=(jax.Shap...  5.26 us
  transfers between devices with their start and end apart: 20, of which 15 were waited for; matrix products, arithmetic and copies ran while one was open for 2% of the time, Pallas kernels for 1%

profile of v1, /device:TPU:80, one launch (start us, length us, event | category | flops | bytes accessed | tf_op | source)
XLA Modules:
  0.0 253.6 jit_solution(10856540390104928464)
XLA Ops:
  2.6 43.8 %all-to-all-start = ((bf16[16,192,128]{2,1,0:T(8,128)(2,1)}), bf16[16,192,128]{2,1,0:T(8,128)(2,1)S(1)}, u32[]{:S(2)}, u32[]{:S(2)}) async-start(bf16[16,192,128]{2,1,0:T(8,128)(2,1)} %broadcast_in_dim.4), calls=%async_computation | async-start | bytes 1572864 | tf_op jit(solution)/shard_map/all_to_all | solution.py:193
  46.4 8.0 %collective-permute-start = (bf16[256,128]{1,0:T(8,128)(2,1)S(1)}, bf16[256,128]{1,0:T(8,128)(2,1)S(1)}, u32[]{:S(2)}, u32[]{:S(2)}) collective-permute-start(bf16[256,128]{1,0:T(8,128)(2,1)S(1)} %copy-done.6), channel_id=1, source_target_pairs={{0,8},{2,10},{4,12},{6,14},{8,0},{10,2},{12,4},{14,6},{1,9},{3,11}... | collective-permute-start | bytes 196616 | tf_op jit(solution)/shard_map/ppermute | solution.py:198
  54.4 2.8 %collective-permute-done = bf16[256,128]{1,0:T(8,128)(2,1)S(1)} collective-permute-done((bf16[256,128]{1,0:T(8,128)(2,1)S(1)}, bf16[256,128]{1,0:T(8,128)(2,1)S(1)}, u32[]{:S(2)}, u32[]{:S(2)}) %collective-permute-start) | collective-permute-done | bytes 65568 | tf_op jit(solution)/shard_map/ppermute | solution.py:198
  57.2 6.6 %collective-permute-start.1 = (bf16[2,256,128]{2,1,0:T(8,128)(2,1)S(1)}, bf16[2,256,128]{2,1,0:T(8,128)(2,1)S(1)}, u32[]{:S(2)}, u32[]{:S(2)}) collective-permute-start(bf16[2,256,128]{2,1,0:T(8,128)(2,1)S(1)} %pad_maximum_fusion.1), channel_id=1, source_target_pairs={{0,12},{2,14},{4,0},{6,2},{8,4},{10,6},{12,8},{14,10},{1,13},{3,15... | collective-permute-start | bytes 393224 | tf_op jit(solution)/shard_map/ppermute | solution.py:198
  63.8 2.9 %collective-permute-start.2 = (bf16[2,256,128]{2,1,0:T(8,128)(2,1)S(1)}, bf16[2,256,128]{2,1,0:T(8,128)(2,1)S(1)}, u32[]{:S(2)}, u32[]{:S(2)}) collective-permute-start(bf16[2,256,128]{2,1,0:T(8,128)(2,1)S(1)} %pad_maximum_fusion.1), channel_id=1, source_target_pairs={{0,14},{2,0},{4,2},{6,4},{8,6},{10,8},{12,10},{14,12},{1,15},{3,1}... | collective-permute-start | bytes 393224 | tf_op jit(solution)/shard_map/ppermute | solution.py:198
  66.7 3.0 %collective-permute-start.3 = (bf16[2,256,128]{2,1,0:T(8,128)(2,1)S(1)}, bf16[2,256,128]{2,1,0:T(8,128)(2,1)S(1)}, u32[]{:S(2)}, u32[]{:S(2)}) collective-permute-start(bf16[2,256,128]{2,1,0:T(8,128)(2,1)S(1)} %pad_maximum_fusion.1), channel_id=1, source_target_pairs={{0,2},{2,4},{4,6},{6,8},{8,10},{10,12},{12,14},{14,0},{1,3},{3,5},... | collective-permute-start | bytes 393224 | tf_op jit(solution)/shard_map/ppermute | solution.py:198
  71.8 3.0 %collective-permute-done.3 = bf16[2,256,128]{2,1,0:T(8,128)(2,1)S(1)} collective-permute-done((bf16[2,256,128]{2,1,0:T(8,128)(2,1)S(1)}, bf16[2,256,128]{2,1,0:T(8,128)(2,1)S(1)}, u32[]{:S(2)}, u32[]{:S(2)}) %collective-permute-start.3) | collective-permute-done | bytes 131104 | tf_op jit(solution)/shard_map/ppermute | solution.py:198
  80.0 5.3 %all-to-all-done.weight_ref = bf16[16,192,128]{2,1,0:T(8,128)(2,1)S(1)} async-done(((bf16[16,192,128]{2,1,0:T(8,128)(2,1)}), bf16[16,192,128]{2,1,0:T(8,128)(2,1)S(1)}, u32[]{:S(2)}, u32[]{:S(2)}) %all-to-all-start) | async-done | bytes 786464 | tf_op jit(solution)/shard_map/all_to_all | solution.py:193
  88.8 4.0 %collective-permute-start.5 = (bf16[64,128]{1,0:T(8,128)(2,1)}, bf16[64,128]{1,0:T(8,128)(2,1)S(1)}, u32[]{:S(2)}, u32[]{:S(2)}) collective-permute-start(bf16[64,128]{1,0:T(8,128)(2,1)} %get-tuple-element.22), channel_id=1, source_target_pairs={{0,16},{16,32},{32,48},{48,64},{64,80},{80,96},{96,112},{112,128},... | collective-permute-start | bytes 49160 | tf_op jit(solution)/shard_map/ppermute | solution.py:270
  95.0 2.6 %scan.2 = (f32[64,256]{1,0:T(8,128)}, f32[64,256]{1,0:T(8,128)}, f32[16,1,128]{2,1,0:T(1,128)}) custom-call(bf16[64,256]{1,0:T(8,128)(2,1)} %get-tuple-element.21.value_ref, bf16[64,128]{1,0:T(8,128)(2,1)} %copy-done.16, f32[2,64,128]{2,1,0:T(8,128)} %pad.4.consts_ref, bf16[2,128,64]{2,1,0:T(8,128)(2,1)} %maximum_bitcast_fusion.maps_ref, ...), custom_call_target="tpu_custom_call" | custom-call | tf_op jit(solution)/shard_map/scan/pallas_call | solution.py:152
  97.6 9.3 %all-to-all-start.1 = ((f32[16,1,128]{2,1,0:T(1,128)}), f32[16,1,128]{2,1,0:T(1,128)S(1)}, u32[]{:S(2)}, u32[]{:S(2)}) async-start(f32[16,1,128]{2,1,0:T(1,128)} %get-tuple-element.23), calls=%async_computation.1 | async-start | bytes 16384 | tf_op jit(solution)/shard_map/all_to_all | solution.py:193
  106.9 12.2 %all-to-all-done.1.msgs_ref = f32[16,1,128]{2,1,0:T(1,128)S(1)} async-done(((f32[16,1,128]{2,1,0:T(1,128)}), f32[16,1,128]{2,1,0:T(1,128)S(1)}, u32[]{:S(2)}, u32[]{:S(2)}) %all-to-all-start.1) | async-done | bytes 8224 | tf_op jit(solution)/shard_map/all_to_all | solution.py:193
  121.5 7.3 %all-to-all-start.2 = ((bf16[8,64,256]{2,1,0:T(8,128)(2,1)}), bf16[8,64,256]{2,1,0:T(8,128)(2,1)S(1)}, u32[]{:S(2)}, u32[]{:S(2)}) async-start(bf16[8,64,256]{2,1,0:T(8,128)(2,1)} %close.2), calls=%async_computation.2 | async-start | bytes 524288 | tf_op jit(solution)/shard_map/all_to_all | solution.py:193
  128.9 10.4 %all-to-all-done.2.mine_ref = bf16[8,64,256]{2,1,0:T(8,128)(2,1)S(1)} async-done(((bf16[8,64,256]{2,1,0:T(8,128)(2,1)}), bf16[8,64,256]{2,1,0:T(8,128)(2,1)S(1)}, u32[]{:S(2)}, u32[]{:S(2)}) %all-to-all-start.2) | async-done | bytes 262176 | tf_op jit(solution)/shard_map/all_to_all | solution.py:193
  145.9 3.7 %all-to-all-start.3 = ((bf16[8,256,128]{2,1,0:T(8,128)(2,1)}), bf16[8,256,128]{2,1,0:T(8,128)(2,1)S(1)}, u32[]{:S(2)}, u32[]{:S(2)}) async-start(bf16[8,256,128]{2,1,0:T(8,128)(2,1)} %get-tuple-element.27), calls=%async_computation.3 | async-start | bytes 1048576 | tf_op jit(solution)/shard_map/all_to_all | solution.py:193
  152.2 7.3 %collective-permute-start.9 = (bf16[192,128]{1,0:T(8,128)(2,1)S(1)}, bf16[192,128]{1,0:T(8,128)(2,1)S(1)}, u32[]{:S(2)}, u32[]{:S(2)}) collective-permute-start(bf16[192,128]{1,0:T(8,128)(2,1)S(1)} %get-tuple-element.28), channel_id=1, source_target_pairs={{0,128},{16,144},{32,160},{48,176},{64,192},{80,208},{96,224},{112... | collective-permute-start | bytes 147464 | tf_op jit(solution)/shard_map/ppermute | solution.py:198
  162.1 4.8 %collective-permute-done.9 = bf16[192,128]{1,0:T(8,128)(2,1)S(1)} collective-permute-done((bf16[192,128]{1,0:T(8,128)(2,1)S(1)}, bf16[192,128]{1,0:T(8,128)(2,1)S(1)}, u32[]{:S(2)}, u32[]{:S(2)}) %collective-permute-start.9) | collective-permute-done | bytes 49184 | tf_op jit(solution)/shard_map/ppermute | solution.py:198
  166.9 6.8 %collective-permute-done.10 = bf16[192,128]{1,0:T(8,128)(2,1)S(1)} collective-permute-done((bf16[192,128]{1,0:T(8,128)(2,1)S(1)}, bf16[192,128]{1,0:T(8,128)(2,1)S(1)}, u32[]{:S(2)}, u32[]{:S(2)}) %collective-permute-start.10) | collective-permute-done | bytes 49184 | tf_op jit(solution)/shard_map/ppermute | solution.py:198
  182.5 4.0 %collective-permute-start.13 = (bf16[4,192,128]{2,1,0:T(8,128)(2,1)S(1)}, bf16[4,192,128]{2,1,0:T(8,128)(2,1)S(1)}, u32[]{:S(2)}, u32[]{:S(2)}) collective-permute-start(bf16[4,192,128]{2,1,0:T(8,128)(2,1)S(1)} %pad_maximum_fusion), channel_id=1, source_target_pairs={{0,16},{16,32},{32,48},{48,64},{64,80},{80,96},{96,112},{112,128},... | collective-permute-start | bytes 589832 | tf_op jit(solution)/shard_map/ppermute | solution.py:198
  188.9 4.0 %collective-permute-done.13 = bf16[4,192,128]{2,1,0:T(8,128)(2,1)S(1)} collective-permute-done((bf16[4,192,128]{2,1,0:T(8,128)(2,1)S(1)}, bf16[4,192,128]{2,1,0:T(8,128)(2,1)S(1)}, u32[]{:S(2)}, u32[]{:S(2)}) %collective-permute-start.13) | collective-permute-done | bytes 196640 | tf_op jit(solution)/shard_map/ppermute | solution.py:198
  197.3 2.7 %collective-permute-start.14 = (bf16[64,128]{1,0:T(8,128)(2,1)}, bf16[64,128]{1,0:T(8,128)(2,1)S(1)}, u32[]{:S(2)}, u32[]{:S(2)}) collective-permute-start(bf16[64,128]{1,0:T(8,128)(2,1)} %get-tuple-element.31), channel_id=1, source_target_pairs={{0,16},{16,32},{32,48},{48,64},{64,80},{80,96},{96,112},{112,128},... | collective-permute-start | bytes 49160 | tf_op jit(solution)/shard_map/ppermute | solution.py:270
  202.2 2.6 %scan.3 = (f32[64,256]{1,0:T(8,128)}, f32[64,256]{1,0:T(8,128)}, f32[16,1,128]{2,1,0:T(1,128)}) custom-call(bf16[64,256]{1,0:T(8,128)(2,1)} %get-tuple-element.30.value_ref, bf16[64,128]{1,0:T(8,128)(2,1)} %copy-done.17, f32[2,64,128]{2,1,0:T(8,128)} %pad.4.consts_ref, bf16[2,128,64]{2,1,0:T(8,128)(2,1)} %maximum_bitcast_fusion.maps_ref, ...), custom_call_target="tpu_custom_call" | custom-call | tf_op jit(solution)/shard_map/scan/pallas_call | solution.py:152
  204.9 23.3 %all_to_all.30.msgs_ref = f32[16,1,128]{2,1,0:T(1,128)} all-to-all(f32[16,1,128]{2,1,0:T(1,128)} %get-tuple-element.32), channel_id=1, replica_groups=mesh['grp'=2,'sp'=16,'x'=8,'core'=2] {'sp'}, dimensions={0} | all-to-all | bytes 16384 | tf_op jit(solution)/shard_map/all_to_all | solution.py:193
  229.9 17.2 %all_to_all.31.mine_ref = bf16[8,64,256]{2,1,0:T(8,128)(2,1)S(1)} all-to-all(bf16[8,64,256]{2,1,0:T(8,128)(2,1)} %close.3), channel_id=1, replica_groups=mesh['grp'=2,'sp'=16,'x'=8,'core'=2] {'x'}, dimensions={0} | all-to-all | bytes 524288 | tf_op jit(solution)/shard_map/all_to_all | solution.py:193
  (103 shorter events, 55.5 us)
Async XLA Ops:
  2.6 43.8 %copy-start.6 = (bf16[256,128]{1,0:T(8,128)(2,1)S(1)}, bf16[256,128]{1,0:T(8,128)(2,1)}, u32[]{:S(2)}) copy-start(bf16[256,128]{1,0:T(8,128)(2,1)} %residual_ref.1) | copy-start | bytes 196612
  2.6 82.7 %all-to-all-start = ((bf16[16,192,128]{2,1,0:T(8,128)(2,1)}), bf16[16,192,128]{2,1,0:T(8,128)(2,1)S(1)}, u32[]{:S(2)}, u32[]{:S(2)}) async-start(bf16[16,192,128]{2,1,0:T(8,128)(2,1)} %broadcast_in_dim.4), calls=%async_computation | async-start | bytes 1572864 | tf_op jit(solution)/shard_map/all_to_all | solution.py:193
  46.4 10.7 %collective-permute-start = (bf16[256,128]{1,0:T(8,128)(2,1)S(1)}, bf16[256,128]{1,0:T(8,128)(2,1)S(1)}, u32[]{:S(2)}, u32[]{:S(2)}) collective-permute-start(bf16[256,128]{1,0:T(8,128)(2,1)S(1)} %copy-done.6), channel_id=1, source_target_pairs={{0,8},{2,10},{4,12},{6,14},{8,0},{10,2},{12,4},{14,6},{1,9},{3,11}... | collective-permute-start | bytes 196616 | tf_op jit(solution)/shard_map/ppermute | solution.py:198
  57.2 12.6 %collective-permute-start.1 = (bf16[2,256,128]{2,1,0:T(8,128)(2,1)S(1)}, bf16[2,256,128]{2,1,0:T(8,128)(2,1)S(1)}, u32[]{:S(2)}, u32[]{:S(2)}) collective-permute-start(bf16[2,256,128]{2,1,0:T(8,128)(2,1)S(1)} %pad_maximum_fusion.1), channel_id=1, source_target_pairs={{0,12},{2,14},{4,0},{6,2},{8,4},{10,6},{12,8},{14,10},{1,13},{3,15... | collective-permute-start | bytes 393224 | tf_op jit(solution)/shard_map/ppermute | solution.py:198
  63.8 8.0 %collective-permute-start.2 = (bf16[2,256,128]{2,1,0:T(8,128)(2,1)S(1)}, bf16[2,256,128]{2,1,0:T(8,128)(2,1)S(1)}, u32[]{:S(2)}, u32[]{:S(2)}) collective-permute-start(bf16[2,256,128]{2,1,0:T(8,128)(2,1)S(1)} %pad_maximum_fusion.1), channel_id=1, source_target_pairs={{0,14},{2,0},{4,2},{6,4},{8,6},{10,8},{12,10},{14,12},{1,15},{3,1}... | collective-permute-start | bytes 393224 | tf_op jit(solution)/shard_map/ppermute | solution.py:198
  66.7 8.1 %collective-permute-start.3 = (bf16[2,256,128]{2,1,0:T(8,128)(2,1)S(1)}, bf16[2,256,128]{2,1,0:T(8,128)(2,1)S(1)}, u32[]{:S(2)}, u32[]{:S(2)}) collective-permute-start(bf16[2,256,128]{2,1,0:T(8,128)(2,1)S(1)} %pad_maximum_fusion.1), channel_id=1, source_target_pairs={{0,2},{2,4},{4,6},{6,8},{8,10},{10,12},{12,14},{14,0},{1,3},{3,5},... | collective-permute-start | bytes 393224 | tf_op jit(solution)/shard_map/ppermute | solution.py:198
  74.9 10.5 %copy-start.5 = (bf16[8,256,128]{2,1,0:T(8,128)(2,1)}, bf16[8,256,128]{2,1,0:T(8,128)(2,1)S(1)}, u32[]{:S(2)}) copy-start(bf16[8,256,128]{2,1,0:T(8,128)(2,1)S(1)} %constant_dynamic-update-slice_fusion.mine_ref) | copy-start | bytes 1572868
  74.9 5.1 %collective-permute-start.4 = (bf16[8,256,128]{2,1,0:T(8,128)(2,1)S(1)}, bf16[8,256,128]{2,1,0:T(8,128)(2,1)S(1)}, u32[]{:S(2)}, u32[]{:S(2)}) collective-permute-start(bf16[8,256,128]{2,1,0:T(8,128)(2,1)S(1)} %constant_dynamic-update-slice_fusion.mine_ref), channel_id=1, source_target_pairs={{0,1},{1,0},{2,3},{3,2},{4,5},{5,4},{6,7},{7,6},{8,9},{9,8},{10,11... | collective-permute-start | bytes 1572872 | tf_op jit(solution)/shard_map/ppermute | solution.py:198
  80.0 5.4 %copy-start.8 = (bf16[8,256,128]{2,1,0:T(8,128)(2,1)}, bf16[8,256,128]{2,1,0:T(8,128)(2,1)S(1)}, u32[]{:S(2)}) copy-start(bf16[8,256,128]{2,1,0:T(8,128)(2,1)S(1)} %collective-permute-done.4.theirs_ref) | copy-start | bytes 1572868
  88.8 5.6 %collective-permute-start.5 = (bf16[64,128]{1,0:T(8,128)(2,1)}, bf16[64,128]{1,0:T(8,128)(2,1)S(1)}, u32[]{:S(2)}, u32[]{:S(2)}) collective-permute-start(bf16[64,128]{1,0:T(8,128)(2,1)} %get-tuple-element.22), channel_id=1, source_target_pairs={{0,16},{16,32},{32,48},{48,64},{64,80},{80,96},{96,112},{112,128},... | collective-permute-start | bytes 49160 | tf_op jit(solution)/shard_map/ppermute | solution.py:270
  97.6 21.5 %all-to-all-start.1 = ((f32[16,1,128]{2,1,0:T(1,128)}), f32[16,1,128]{2,1,0:T(1,128)S(1)}, u32[]{:S(2)}, u32[]{:S(2)}) async-start(f32[16,1,128]{2,1,0:T(1,128)} %get-tuple-element.23), calls=%async_computation.1 | async-start | bytes 16384 | tf_op jit(solution)/shard_map/all_to_all | solution.py:193
  121.5 17.8 %all-to-all-start.2 = ((bf16[8,64,256]{2,1,0:T(8,128)(2,1)}), bf16[8,64,256]{2,1,0:T(8,128)(2,1)S(1)}, u32[]{:S(2)}, u32[]{:S(2)}) async-start(bf16[8,64,256]{2,1,0:T(8,128)(2,1)} %close.2), calls=%async_computation.2 | async-start | bytes 524288 | tf_op jit(solution)/shard_map/all_to_all | solution.py:193
  139.3 3.4 %collective-permute-start.6 = (bf16[8,64,256]{2,1,0:T(8,128)(2,1)S(1)}, bf16[8,64,256]{2,1,0:T(8,128)(2,1)S(1)}, u32[]{:S(2)}, u32[]{:S(2)}) collective-permute-start(bf16[8,64,256]{2,1,0:T(8,128)(2,1)S(1)} %all-to-all-done.2.mine_ref), channel_id=1, source_target_pairs={{0,1},{1,0},{2,3},{3,2},{4,5},{5,4},{6,7},{7,6},{8,9},{9,8},{10,11... | collective-permute-start | bytes 786440 | tf_op jit(solution)/shard_map/ppermute | solution.py:198
  145.9 32.0 %all-to-all-start.3 = ((bf16[8,256,128]{2,1,0:T(8,128)(2,1)}), bf16[8,256,128]{2,1,0:T(8,128)(2,1)S(1)}, u32[]{:S(2)}, u32[]{:S(2)}) async-start(bf16[8,256,128]{2,1,0:T(8,128)(2,1)} %get-tuple-element.27), calls=%async_computation.3 | async-start | bytes 1048576 | tf_op jit(solution)/shard_map/all_to_all | solution.py:193
  149.6 12.4 %collective-permute-start.8 = (bf16[192,128]{1,0:T(8,128)(2,1)S(1)}, bf16[192,128]{1,0:T(8,128)(2,1)S(1)}, u32[]{:S(2)}, u32[]{:S(2)}) collective-permute-start(bf16[192,128]{1,0:T(8,128)(2,1)S(1)} %get-tuple-element.28), channel_id=1, source_target_pairs={{0,64},{16,80},{32,96},{48,112},{64,128},{80,144},{96,160},{112,17... | collective-permute-start | bytes 147464 | tf_op jit(solution)/shard_map/ppermute | solution.py:198
  152.2 14.7 %collective-permute-start.9 = (bf16[192,128]{1,0:T(8,128)(2,1)S(1)}, bf16[192,128]{1,0:T(8,128)(2,1)S(1)}, u32[]{:S(2)}, u32[]{:S(2)}) collective-permute-start(bf16[192,128]{1,0:T(8,128)(2,1)S(1)} %get-tuple-element.28), channel_id=1, source_target_pairs={{0,128},{16,144},{32,160},{48,176},{64,192},{80,208},{96,224},{112... | collective-permute-start | bytes 147464 | tf_op jit(solution)/shard_map/ppermute | solution.py:198
  159.5 14.2 %collective-permute-start.10 = (bf16[192,128]{1,0:T(8,128)(2,1)S(1)}, bf16[192,128]{1,0:T(8,128)(2,1)S(1)}, u32[]{:S(2)}, u32[]{:S(2)}) collective-permute-start(bf16[192,128]{1,0:T(8,128)(2,1)S(1)} %get-tuple-element.28), channel_id=1, source_target_pairs={{0,192},{16,208},{32,224},{48,240},{64,0},{80,16},{96,32},{112,48}... | collective-permute-start | bytes 147464 | tf_op jit(solution)/shard_map/ppermute | solution.py:198
  173.7 12.9 %collective-permute-start.11 = (bf16[4,192,128]{2,1,0:T(8,128)(2,1)S(1)}, bf16[4,192,128]{2,1,0:T(8,128)(2,1)S(1)}, u32[]{:S(2)}, u32[]{:S(2)}) collective-permute-start(bf16[4,192,128]{2,1,0:T(8,128)(2,1)S(1)} %pad_maximum_fusion), channel_id=1, source_target_pairs={{0,224},{16,240},{32,0},{48,16},{64,32},{80,48},{96,64},{112,80},{... | collective-permute-start | bytes 589832 | tf_op jit(solution)/shard_map/ppermute | solution.py:198
  176.0 12.8 %collective-permute-start.12 = (bf16[4,192,128]{2,1,0:T(8,128)(2,1)S(1)}, bf16[4,192,128]{2,1,0:T(8,128)(2,1)S(1)}, u32[]{:S(2)}, u32[]{:S(2)}) collective-permute-start(bf16[4,192,128]{2,1,0:T(8,128)(2,1)S(1)} %pad_maximum_fusion), channel_id=1, source_target_pairs={{0,240},{16,0},{32,16},{48,32},{64,48},{80,64},{96,80},{112,96},{1... | collective-permute-start | bytes 589832 | tf_op jit(solution)/shard_map/ppermute | solution.py:198
  178.0 10.9 %copy-start.2 = (bf16[8,256,128]{2,1,0:T(8,128)(2,1)}, bf16[8,256,128]{2,1,0:T(8,128)(2,1)S(1)}, u32[]{:S(2)}) copy-start(bf16[8,256,128]{2,1,0:T(8,128)(2,1)S(1)} %all-to-all-done.3.mine_ref) | copy-start | bytes 1572868
  178.0 15.0 %collective-permute-start.7 = (bf16[8,256,128]{2,1,0:T(8,128)(2,1)S(1)}, bf16[8,256,128]{2,1,0:T(8,128)(2,1)S(1)}, u32[]{:S(2)}, u32[]{:S(2)}) collective-permute-start(bf16[8,256,128]{2,1,0:T(8,128)(2,1)S(1)} %all-to-all-done.3.mine_ref), channel_id=1, source_target_pairs={{0,1},{1,0},{2,3},{3,2},{4,5},{5,4},{6,7},{7,6},{8,9},{9,8},{10,11... | collective-permute-start | bytes 1572872 | tf_op jit(solution)/shard_map/ppermute | solution.py:198
  182.5 10.4 %collective-permute-start.13 = (bf16[4,192,128]{2,1,0:T(8,128)(2,1)S(1)}, bf16[4,192,128]{2,1,0:T(8,128)(2,1)S(1)}, u32[]{:S(2)}, u32[]{:S(2)}) collective-permute-start(bf16[4,192,128]{2,1,0:T(8,128)(2,1)S(1)} %pad_maximum_fusion), channel_id=1, source_target_pairs={{0,16},{16,32},{32,48},{48,64},{64,80},{80,96},{96,112},{112,128},... | collective-permute-start | bytes 589832 | tf_op jit(solution)/shard_map/ppermute | solution.py:198
  197.3 4.4 %collective-permute-start.14 = (bf16[64,128]{1,0:T(8,128)(2,1)}, bf16[64,128]{1,0:T(8,128)(2,1)S(1)}, u32[]{:S(2)}, u32[]{:S(2)}) collective-permute-start(bf16[64,128]{1,0:T(8,128)(2,1)} %get-tuple-element.31), channel_id=1, source_target_pairs={{0,16},{16,32},{32,48},{48,64},{64,80},{80,96},{96,112},{112,128},... | collective-permute-start | bytes 49160 | tf_op jit(solution)/shard_map/ppermute | solution.py:270
  247.2 3.4 %collective-permute-start.15 = (bf16[8,64,256]{2,1,0:T(8,128)(2,1)S(1)}, bf16[8,64,256]{2,1,0:T(8,128)(2,1)S(1)}, u32[]{:S(2)}, u32[]{:S(2)}) collective-permute-start(bf16[8,64,256]{2,1,0:T(8,128)(2,1)S(1)} %all_to_all.31.mine_ref), channel_id=1, source_target_pairs={{0,1},{1,0},{2,3},{3,2},{4,5},{5,4},{6,7},{7,6},{8,9},{9,8},{10,11... | collective-permute-start | bytes 786440 | tf_op jit(solution)/shard_map/ppermute | solution.py:198
  (17 other events, 21.6 us)

commit v2 on v1

v2 whole, which is shorter than its diff:
```python
import functools

import jax
import jax.numpy as jnp
from jax import lax
from jax.experimental import pallas as pl
from jax.experimental.pallas import tpu as pltpu
from jax.sharding import Mesh, PartitionSpec as P


LAYERS = 2
EPS = 1e-06
RATE_SCALE = 8.0
LANES = 128
NEAR = (-2, -1, 0, 1)


def one_minus_exp(u):
    series = 1.0
    for n in range(9, 1, -1):
        series = 1.0 + u * series * (1.0 / n)
    return jnp.where(u > -0.5, -u * series, 1.0 - jnp.exp(u))


def scan_kernel(
    layer, value_ref, before_ref, consts_ref, maps_ref, offset_ref, cum_ref, state_ref, msg_ref
):
    channels, tok = value_ref.shape
    taps = 4
    value = value_ref[...].astype(jnp.float32)
    full = jnp.concatenate([before_ref[...].astype(jnp.float32), value], axis=1)
    consts = consts_ref[layer]
    smoothed = consts[:, taps - 1 : taps] * value
    for back in range(1, taps):
        shifted = pltpu.roll(full, back, axis=1)[:, LANES:]
        smoothed = smoothed + consts[:, taps - 1 - back : taps - back] * shifted
    half = smoothed.astype(jnp.bfloat16)
    gates = lax.dot_general(
        maps_ref[layer], half, (((1,), (0,)), ((), ())), preferred_element_type=jnp.float32
    )
    gates = 1.0 / (1.0 + jnp.exp(-gates))
    recur, inputs = gates[:channels], gates[channels:]
    log_decay = consts[:, taps : taps + 1] * recur + offset_ref[layer]
    a = jnp.exp(log_decay)
    b = jnp.sqrt(one_minus_exp(2.0 * log_decay)) * inputs * smoothed
    lane = lax.broadcasted_iota(jnp.int32, (channels, tok), 1)
    step = 1
    while step < tok:
        inside = lane >= step
        b = jnp.where(inside, a * pltpu.roll(b, step, axis=1), 0.0) + b
        a = jnp.where(inside, pltpu.roll(a, step, axis=1), 1.0) * a
        step *= 2
    cum_ref[...] = a
    state_ref[...] = b
    last = jnp.concatenate([a[:, tok - LANES :], b[:, tok - LANES :]], axis=0)
    row = last.T[LANES - 1 : LANES, :]
    msg_ref[...] = jnp.broadcast_to(row[None], msg_ref.shape)


def close_kernel(msgs_ref, cum_ref, state_ref, gate_ref, out_ref):
    channels, tok = cum_ref.shape
    count = msgs_ref.shape[0]
    position = lax.axis_index("sp")
    carry = jnp.zeros((1, channels), jnp.float32)
    for s in range(count - 1):
        line = msgs_ref[s]
        step = line[:, :channels] * carry + line[:, channels:]
        carry = jnp.where(s < position, step, carry)
    wide = jnp.broadcast_to(carry, (LANES, channels)).T
    wide = jnp.concatenate([wide] * (tok // LANES), axis=1)
    hidden = state_ref[...] + cum_ref[...] * wide
    gate = gate_ref[...].astype(jnp.float32)
    branch = (hidden * (gate / (1.0 + jnp.exp(-gate)))).astype(jnp.bfloat16)
    out_ref[...] = jnp.broadcast_to(branch[None], out_ref.shape)


def blocks_of(chips, count, hopped, slotted=False):
    chip, core, place = (lax.axis_index(name) for name in ("x", "core", "sp"))
    far = chips // len(NEAR)
    for side in range(2):
        for slot in range(chips):
            source = slot
            if slotted:
                behind = slot % far * len(NEAR) + slot // far + NEAR[0]
                source = lax.rem(chip + chips - behind, chips)
            block = 2 * source + (core if side == 0 else 1 - core)
            held = block
            if hopped:
                at = lax.rem(place + 2 * count - block - NEAR[0], count)
                held = lax.rem(at, len(NEAR)) * (count // len(NEAR)) + lax.div(at, len(NEAR))
            yield side, slot, block, held


def project_kernel(
    slotted, hopped, mine_ref, theirs_ref, gain_ref, weight_ref, value_ref, gate_ref, tail_ref
):
    chips, tok, width = mine_ref.shape
    channels = value_ref.shape[0]
    product = jnp.zeros((2 * channels, tok), jnp.float32)
    squares = jnp.zeros((tok, width), jnp.float32)
    pieces = (mine_ref, theirs_ref)
    for side, slot, block, held in blocks_of(chips, weight_ref.shape[0], hopped, slotted):
        wide = pieces[side][slot].astype(jnp.float32)
        squares += wide * wide
        scaled = (wide * gain_ref[block]).astype(jnp.bfloat16)
        product += lax.dot_general(
            weight_ref[held, : 2 * channels, :],
            scaled,
            (((1,), (1,)), ((), ())),
            preferred_element_type=jnp.float32,
        )
    mean = jnp.sum(squares.T, axis=0, keepdims=True) * (1.0 / (2 * chips * width))
    rows = (product * lax.rsqrt(mean + EPS)).astype(jnp.bfloat16)
    value_ref[...] = rows[:channels]
    gate_ref[...] = rows[channels:]
    tail_ref[...] = rows[:channels, tok - LANES :]


def mix_kernel(hopped, mine_ref, theirs_ref, weight_ref, residual_ref, out_ref, *copies_ref):
    chips, channels, _ = mine_ref.shape
    first = weight_ref.shape[1] - channels
    held = {(side, slot): w for side, slot, _, w in blocks_of(chips, weight_ref.shape[0], hopped)}
    mixed = residual_ref[...].astype(jnp.float32)
    for slot in range(chips):
        branch = jnp.concatenate([mine_ref[slot], theirs_ref[slot]], axis=0)
        weight = jnp.concatenate(
            [weight_ref[held[side, slot], first:, :] for side in range(2)], axis=0
        )
        mixed += lax.dot_general(
            branch, weight, (((0,), (0,)), ((), ())), preferred_element_type=jnp.float32
        )
    mixed = mixed.astype(jnp.bfloat16)
    out_ref[...] = mixed
    for ref in copies_ref:
        ref[...] = jnp.broadcast_to(mixed[None], ref.shape)


def pack_kernel(value_ref, gate_ref, mix_ref, *out_refs):
    for layer, out_ref in enumerate(out_refs):
        rows = jnp.concatenate([value_ref[layer], gate_ref[layer], mix_ref[layer]], axis=0)
        if len(out_ref.shape) == 3:
            rows = jnp.broadcast_to(rows[None], out_ref.shape)
        out_ref[...] = rows


def vmem(n):
    return [pl.BlockSpec(memory_space=pltpu.VMEM)] * n


def kernel_call(kernel, out_shape, *operands):
    return pl.pallas_call(
        kernel, out_shape=out_shape, in_specs=vmem(len(operands)), out_specs=vmem(len(out_shape))
    )(*(pltpu.with_memory_space_constraint(a, pltpu.VMEM) for a in operands))


def pack_call(value_proj, gate_proj, mix_proj, count):
    layers, channels, width = value_proj.shape
    rows = (3 * channels, width)
    out = [pltpu.VMEM((count, *rows), value_proj.dtype)]
    out += [pltpu.VMEM(rows, value_proj.dtype)] * (layers - 1)
    return kernel_call(pack_kernel, out, value_proj, gate_proj, mix_proj)


def project_call(slotted, hopped, mine, theirs, gains, weights):
    _, tok, _ = mine.shape
    channels = weights.shape[1] // 3
    out = [pltpu.VMEM((channels, n), jnp.bfloat16) for n in (tok, tok, LANES)]
    kernel = functools.partial(project_kernel, slotted, hopped)
    return kernel_call(kernel, out, mine, theirs, gains, weights)


def mix_call(hopped, mine, theirs, weights, residual, copies):
    shape, dtype = residual.shape, jnp.bfloat16
    if copies:
        out = [pltpu.VMEM(shape, dtype), pltpu.VMEM((copies, *shape), dtype)]
    else:
        out = [jax.ShapeDtypeStruct(shape, dtype)]
    kernel = functools.partial(mix_kernel, hopped)
    return kernel_call(kernel, out, mine, theirs, weights, residual)


def scan_call(layer, value, before, consts, maps, offset, count):
    channels, tok = value.shape
    out = [
        pltpu.VMEM((channels, tok), jnp.float32),
        pltpu.VMEM((channels, tok), jnp.float32),
        pltpu.VMEM((count, 1, 2 * channels), jnp.float32),
    ]
    kernel = functools.partial(scan_kernel, layer)
    return kernel_call(kernel, out, value, before, consts, maps, offset)


def close_call(msgs, cum, state, gate, copies):
    out = [pltpu.VMEM((copies, *cum.shape), jnp.bfloat16)]
    return kernel_call(close_kernel, out, msgs, cum, state, gate)[0]


def copy_kernel(in_ref, out_ref):
    out_ref[...] = in_ref[...]


def copy_call(array):
    return kernel_call(copy_kernel, [pltpu.VMEM(array.shape, array.dtype)], array)[0]


def exchange(copies, axis):
    return lax.all_to_all(copies, axis, split_axis=0, concat_axis=0, tiled=True)


def shift(array, axis, steps):
    count = lax.axis_size(axis)
    return lax.ppermute(array, axis, [(i, (i + steps) % count) for i in range(count)])


def far_hop(array, axis, hops=1):
    return shift(array, axis, len(NEAR) * hops)


def near_hops(held, axis):
    return jnp.concatenate([shift(held, axis, n) if n else held for n in NEAR])


def local(
    tokens,
    norm_gain,
    value_proj,
    gate_proj,
    conv_taps,
    recur_map,
    input_map,
    decay_param,
    decay_offset,
    mix_proj,
):
    own_cols = tokens.shape[1]
    chips, cores, count = (lax.axis_size(name) for name in ("x", "core", "sp"))

    def swap(array):
        return shift(array, "core", 1)

    first, shard = pack_call(value_proj, gate_proj, mix_proj, count)
    weights = exchange(first, "sp")
    held = jnp.stack([tokens, far_hop(tokens, "x")])
    mine = near_hops(held, "x")
    rates = -RATE_SCALE * jax.nn.softplus(-decay_param)
    consts = jnp.concatenate([conv_taps.transpose(0, 2, 1), rates[:, :, None]], axis=2)
    consts = jnp.pad(consts, ((0, 0), (0, 0), (0, LANES - consts.shape[2])))
    maps = jnp.concatenate([recur_map[:, 0], input_map[:, 0]], axis=2).transpose(0, 2, 1)
    gains = [gain.reshape(chips * cores, 1, own_cols) for gain in norm_gain]
    gains[1] = copy_call(gains[1])
    gains[1] = copy_call(gains[1])

    residual = tokens
    for layer in range(LAYERS):
        more = layer + 1 < LAYERS
        if layer:
            mine = exchange(copies[0], "x")
            weights = later_weights
        theirs = swap(mine)
        value_rows, gate_rows, tail = project_call(
            layer == 0, layer > 0, mine, theirs, gains[layer], weights
        )
        before = lax.ppermute(tail, "sp", [(i, i + 1) for i in range(count - 1)])
        cum, state, msg = scan_call(layer, value_rows, before, consts, maps, decay_offset, count)
        msgs = exchange(msg, "sp")
        if more:
            _, shard = lax.optimization_barrier((msg, shard))
            hop_one = far_hop(shard, "sp")
        sent = close_call(msgs, cum, state, gate_rows, chips)
        mine = exchange(sent, "x")
        if more:
            _, shard, hop_one = lax.optimization_barrier((sent, shard, hop_one))
            hop_back = far_hop(shard, "sp", -1)
            hop_two = far_hop(hop_one, "sp")
        theirs = swap(mine)
        residual, *copies = mix_call(
            layer > 0, mine, theirs, weights, residual, chips if more else 0
        )
        if more:
            _, *held = lax.optimization_barrier((copies[0], shard, hop_one, hop_two, hop_back))
            later_weights = near_hops(jnp.stack(held), "sp")
    return residual


def solution(mesh):
    grid = mesh.devices
    split = Mesh(grid.reshape(*grid.shape[:2], grid.shape[2] // 2, 2), ("grp", "sp", "x", "core"))
    tp = ("x", "core")
    in_specs = (
        P(("grp", "sp"), tp),
        P(),
        P(None, tp, "sp"),
        P(None, tp, "sp"),
        P(None, None, tp),
        P(None, tp, None, None),
        P(None, tp, None, None),
        P(None, tp),
        P(None, tp, "sp"),
        P(None, "sp", tp),
    )
    return jax.shard_map(
        local, mesh=split, in_specs=in_specs, out_specs=P(("grp", "sp"), tp), check_vma=False
    )
```

time: 256 us -> 229 us (0.89)
  blocking collectives: 40.5 us -> 75.1 us
  waiting for transfers between devices: 58.6 us -> 35.9 us
  starting transfers between devices: 120 us -> 105 us
  Pallas kernels: 21.3 us -> 6.58 us
  local copies, waits for them, and re-layouts: 11 us -> 4.14 us
    all_to_all x2 -> x4, blocking collectives: 40.5 us -> 75.1 us  [exchange(): return lax.all_to_all(copies, axis, split_axis=0, concat_axis=0, tiled=True)]
    all_to_all x4 -> x2, waiting for transfers between devices: 28 us -> 5.82 us  [exchange(): return lax.all_to_all(copies, axis, split_axis=0, concat_axis=0, tiled=True)]
    all_to_all x4 -> x2, starting transfers between devices: 64.1 us -> 47.5 us  [exchange(): return lax.all_to_all(copies, axis, split_axis=0, concat_axis=0, tiled=True)]
    pallas_call x10 -> x11, Pallas kernels: 21.3 us -> 6.58 us  [kernel_call(): pl.pallas_call(kernel, out_shape=out_shape, in_specs=vmem(len(operands)),...]
    unnamed x54 -> x33, local copies, waits for them, and re-layouts: 8.38 us -> 3.96 us
    ppermute x14, starting transfers between devices: 48.9 us -> 51.6 us  [shift(): lax.ppermute(array, axis, [(i, (i + steps) % count) for i in range(count)])]
  transfers between devices with their start and end apart: 20 -> 18, of which waited for: 15 -> 12; matrix products, arithmetic and copies ran while one was open for 2% -> 0% of each run, Pallas kernels for 1% -> 1%
where the time goes in v2:
time: 229 us; the launch traced here: 227 us
  starting transfers between devices  105 us (46%)
  blocking collectives  75.1 us (33%)
  waiting for transfers between devices  35.9 us (16%)
  Pallas kernels  6.58 us (3%)
  local copies, waits for them, and re-layouts  4.14 us (2%)
    all_to_all x4, blocking collectives, exchange(): return lax.all_to_all(copies, axis, split_axis=0, concat_axis=0, tiled=True)  75.1 us
    ppermute x14, starting transfers between devices, shift(): lax.ppermute(array, axis, [(i, (i + steps) % count) for i in range(count)])  51.6 us
    all_to_all x2, starting transfers between devices, exchange(): return lax.all_to_all(copies, axis, split_axis=0, concat_axis=0, tiled=True)  47.5 us
    ppermute x14, waiting for transfers between devices, shift(): lax.ppermute(array, axis, [(i, (i + steps) % count) for i in range(count)])  27.4 us
    pallas_call x11, Pallas kernels, kernel_call(): pl.pallas_call(kernel, out_shape=out_shape, in_specs=vmem(len(operands)),...  6.58 us
    all_to_all x2, waiting for transfers between devices, exchange(): return lax.all_to_all(copies, axis, split_axis=0, concat_axis=0, tiled=True)  5.82 us
    ppermute x2, starting transfers between devices, local(): before = lax.ppermute(tail, 'sp', [(i, i + 1) for i in range(count - 1)])  5.6 us
  transfers between devices with their start and end apart: 18, of which 12 were waited for; matrix products, arithmetic and copies ran while one was open for 0% of the time, Pallas kernels for 1%

profile of v2, /device:TPU:80, one launch (start us, length us, event | category | flops | bytes accessed | tf_op | source)
XLA Modules:
  0.0 227.0 jit_solution(8756193445178571098)
XLA Ops:
  3.3 43.8 %all-to-all-start = ((bf16[16,192,128]{2,1,0:T(8,128)(2,1)}), bf16[16,192,128]{2,1,0:T(8,128)(2,1)S(1)}, u32[]{:S(2)}, u32[]{:S(2)}) async-start(bf16[16,192,128]{2,1,0:T(8,128)(2,1)} %get-tuple-element.28), calls=%async_computation | async-start | bytes 1572864 | tf_op jit(solution)/shard_map/all_to_all | solution.py:207
  47.2 8.0 %collective-permute-start = (bf16[256,128]{1,0:T(8,128)(2,1)S(1)}, bf16[256,128]{1,0:T(8,128)(2,1)S(1)}, u32[]{:S(2)}, u32[]{:S(2)}) collective-permute-start(bf16[256,128]{1,0:T(8,128)(2,1)S(1)} %copy-done), channel_id=1, source_target_pairs={{0,8},{2,10},{4,12},{6,14},{8,0},{10,2},{12,4},{14,6},{1,9},{3,11}... | collective-permute-start | bytes 196616 | tf_op jit(solution)/shard_map/ppermute | solution.py:212
  55.1 2.8 %collective-permute-done = bf16[256,128]{1,0:T(8,128)(2,1)S(1)} collective-permute-done((bf16[256,128]{1,0:T(8,128)(2,1)S(1)}, bf16[256,128]{1,0:T(8,128)(2,1)S(1)}, u32[]{:S(2)}, u32[]{:S(2)}) %collective-permute-start) | collective-permute-done | bytes 65568 | tf_op jit(solution)/shard_map/ppermute | solution.py:212
  57.9 6.6 %collective-permute-start.1 = (bf16[2,256,128]{2,1,0:T(8,128)(2,1)S(1)}, bf16[2,256,128]{2,1,0:T(8,128)(2,1)S(1)}, u32[]{:S(2)}, u32[]{:S(2)}) collective-permute-start(bf16[2,256,128]{2,1,0:T(8,128)(2,1)S(1)} %pad_maximum_fusion.1), channel_id=1, source_target_pairs={{0,12},{2,14},{4,0},{6,2},{8,4},{10,6},{12,8},{14,10},{1,13},{3,15... | collective-permute-start | bytes 393224 | tf_op jit(solution)/shard_map/ppermute | solution.py:212
  64.5 2.9 %collective-permute-start.2 = (bf16[2,256,128]{2,1,0:T(8,128)(2,1)S(1)}, bf16[2,256,128]{2,1,0:T(8,128)(2,1)S(1)}, u32[]{:S(2)}, u32[]{:S(2)}) collective-permute-start(bf16[2,256,128]{2,1,0:T(8,128)(2,1)S(1)} %pad_maximum_fusion.1), channel_id=1, source_target_pairs={{0,14},{2,0},{4,2},{6,4},{8,6},{10,8},{12,10},{14,12},{1,15},{3,1}... | collective-permute-start | bytes 393224 | tf_op jit(solution)/shard_map/ppermute | solution.py:212
  68.3 3.0 %collective-permute-start.3 = (bf16[2,256,128]{2,1,0:T(8,128)(2,1)S(1)}, bf16[2,256,128]{2,1,0:T(8,128)(2,1)S(1)}, u32[]{:S(2)}, u32[]{:S(2)}) collective-permute-start(bf16[2,256,128]{2,1,0:T(8,128)(2,1)S(1)} %pad_maximum_fusion.1), channel_id=1, source_target_pairs={{0,2},{2,4},{4,6},{6,8},{8,10},{10,12},{12,14},{14,0},{1,3},{3,5},... | collective-permute-start | bytes 393224 | tf_op jit(solution)/shard_map/ppermute | solution.py:212
  72.5 3.8 %collective-permute-done.3 = bf16[2,256,128]{2,1,0:T(8,128)(2,1)S(1)} collective-permute-done((bf16[2,256,128]{2,1,0:T(8,128)(2,1)S(1)}, bf16[2,256,128]{2,1,0:T(8,128)(2,1)S(1)}, u32[]{:S(2)}, u32[]{:S(2)}) %collective-permute-start.3) | collective-permute-done | bytes 131104 | tf_op jit(solution)/shard_map/ppermute | solution.py:212
  76.4 2.0 collective-permute-start.4
  80.2 5.8 %all-to-all-done.weight_ref = bf16[16,192,128]{2,1,0:T(8,128)(2,1)S(1)} async-done(((bf16[16,192,128]{2,1,0:T(8,128)(2,1)}), bf16[16,192,128]{2,1,0:T(8,128)(2,1)S(1)}, u32[]{:S(2)}, u32[]{:S(2)}) %all-to-all-start) | async-done | bytes 786464 | tf_op jit(solution)/shard_map/all_to_all | solution.py:207
  86.6 4.1 %collective-permute-start.5 = (bf16[64,128]{1,0:T(8,128)(2,1)S(1)}, bf16[64,128]{1,0:T(8,128)(2,1)S(1)}, u32[]{:S(2)}, u32[]{:S(2)}) collective-permute-start(bf16[64,128]{1,0:T(8,128)(2,1)S(1)} %get-tuple-element.30), channel_id=1, source_target_pairs={{0,16},{16,32},{32,48},{48,64},{64,80},{80,96},{96,112},{112,128},... | collective-permute-start | bytes 49160 | tf_op jit(solution)/shard_map/ppermute | solution.py:263
  93.1 21.3 %all_to_all.30.msgs_ref = f32[16,1,128]{2,1,0:T(1,128)S(1)} all-to-all(f32[16,1,128]{2,1,0:T(1,128)S(1)} %get-tuple-element.31), channel_id=1, replica_groups=mesh['grp'=2,'sp'=16,'x'=8,'core'=2] {'sp'}, dimensions={0} | all-to-all | bytes 16384 | tf_op jit(solution)/shard_map/all_to_all | solution.py:207
  114.7 17.6 %all_to_all.31.mine_ref = bf16[8,64,256]{2,1,0:T(8,128)(2,1)S(1)} all-to-all(bf16[8,64,256]{2,1,0:T(8,128)(2,1)S(1)} %shard_map.103), channel_id=1, replica_groups=mesh['grp'=2,'sp'=16,'x'=8,'core'=2] {'x'}, dimensions={0} | all-to-all | bytes 524288 | tf_op jit(solution)/shard_map/all_to_all | solution.py:207
  134.2 2.5 %collective-permute-start.8 = (bf16[192,128]{1,0:T(8,128)(2,1)S(1)}, bf16[192,128]{1,0:T(8,128)(2,1)S(1)}, u32[]{:S(2)}, u32[]{:S(2)}) collective-permute-start(bf16[192,128]{1,0:T(8,128)(2,1)S(1)} %get-tuple-element.40), channel_id=1, source_target_pairs={{0,64},{16,80},{32,96},{48,112},{64,128},{80,144},{96,160},{112,17... | collective-permute-start | bytes 147464 | tf_op jit(solution)/shard_map/ppermute | solution.py:212
  136.7 7.8 %collective-permute-done.8 = bf16[192,128]{1,0:T(8,128)(2,1)S(1)} collective-permute-done((bf16[192,128]{1,0:T(8,128)(2,1)S(1)}, bf16[192,128]{1,0:T(8,128)(2,1)S(1)}, u32[]{:S(2)}, u32[]{:S(2)}) %collective-permute-start.8) | collective-permute-done | bytes 49184 | tf_op jit(solution)/shard_map/ppermute | solution.py:212
  144.5 2.5 %collective-permute-start.10 = (bf16[192,128]{1,0:T(8,128)(2,1)S(1)}, bf16[192,128]{1,0:T(8,128)(2,1)S(1)}, u32[]{:S(2)}, u32[]{:S(2)}) collective-permute-start(bf16[192,128]{1,0:T(8,128)(2,1)S(1)} %get-tuple-element.40), channel_id=1, source_target_pairs={{0,192},{16,208},{32,224},{48,240},{64,0},{80,16},{96,32},{112,48}... | collective-permute-start | bytes 147464 | tf_op jit(solution)/shard_map/ppermute | solution.py:212
  147.0 7.3 %collective-permute-start.9 = (bf16[192,128]{1,0:T(8,128)(2,1)S(1)}, bf16[192,128]{1,0:T(8,128)(2,1)S(1)}, u32[]{:S(2)}, u32[]{:S(2)}) collective-permute-start(bf16[192,128]{1,0:T(8,128)(2,1)S(1)} %collective-permute-done.8), channel_id=1, source_target_pairs={{0,64},{16,80},{32,96},{48,112},{64,128},{80,144},{96,160},{112,17... | collective-permute-start | bytes 147464 | tf_op jit(solution)/shard_map/ppermute | solution.py:212
  155.5 3.7 %all-to-all-start.3 = ((bf16[8,256,128]{2,1,0:T(8,128)(2,1)}), bf16[8,256,128]{2,1,0:T(8,128)(2,1)S(1)}, u32[]{:S(2)}, u32[]{:S(2)}) async-start(bf16[8,256,128]{2,1,0:T(8,128)(2,1)} %get-tuple-element.35), calls=%async_computation.3 | async-start | bytes 1048576 | tf_op jit(solution)/shard_map/all_to_all | solution.py:207
  159.3 5.2 %collective-permute-start.11 = (bf16[4,192,128]{2,1,0:T(8,128)(2,1)S(1)}, bf16[4,192,128]{2,1,0:T(8,128)(2,1)S(1)}, u32[]{:S(2)}, u32[]{:S(2)}) collective-permute-start(bf16[4,192,128]{2,1,0:T(8,128)(2,1)S(1)} %pad_maximum_fusion), channel_id=1, source_target_pairs={{0,224},{16,240},{32,0},{48,16},{64,32},{80,48},{96,64},{112,80},{... | collective-permute-start | bytes 589832 | tf_op jit(solution)/shard_map/ppermute | solution.py:212
  164.5 2.0 collective-permute-start.12
  166.6 3.9 %collective-permute-start.13 = (bf16[4,192,128]{2,1,0:T(8,128)(2,1)S(1)}, bf16[4,192,128]{2,1,0:T(8,128)(2,1)S(1)}, u32[]{:S(2)}, u32[]{:S(2)}) collective-permute-start(bf16[4,192,128]{2,1,0:T(8,128)(2,1)S(1)} %pad_maximum_fusion), channel_id=1, source_target_pairs={{0,16},{16,32},{32,48},{48,64},{64,80},{80,96},{96,112},{112,128},... | collective-permute-start | bytes 589832 | tf_op jit(solution)/shard_map/ppermute | solution.py:212
  170.5 2.7 %collective-permute-done.11 = bf16[4,192,128]{2,1,0:T(8,128)(2,1)S(1)} collective-permute-done((bf16[4,192,128]{2,1,0:T(8,128)(2,1)S(1)}, bf16[4,192,128]{2,1,0:T(8,128)(2,1)S(1)}, u32[]{:S(2)}, u32[]{:S(2)}) %collective-permute-start.11) | collective-permute-done | bytes 196640 | tf_op jit(solution)/shard_map/ppermute | solution.py:212
  173.1 4.7 %collective-permute-done.12 = bf16[4,192,128]{2,1,0:T(8,128)(2,1)S(1)} collective-permute-done((bf16[4,192,128]{2,1,0:T(8,128)(2,1)S(1)}, bf16[4,192,128]{2,1,0:T(8,128)(2,1)S(1)}, u32[]{:S(2)}, u32[]{:S(2)}) %collective-permute-start.12) | collective-permute-done | bytes 196640 | tf_op jit(solution)/shard_map/ppermute | solution.py:212
  186.2 20.8 %all_to_all.32.msgs_ref = f32[16,1,128]{2,1,0:T(1,128)S(1)} all-to-all(f32[16,1,128]{2,1,0:T(1,128)S(1)} %get-tuple-element.46), channel_id=1, replica_groups=mesh['grp'=2,'sp'=16,'x'=8,'core'=2] {'sp'}, dimensions={0} | all-to-all | bytes 16384 | tf_op jit(solution)/shard_map/all_to_all | solution.py:207
  207.2 15.3 %all_to_all.33.mine_ref = bf16[8,64,256]{2,1,0:T(8,128)(2,1)S(1)} all-to-all(bf16[8,64,256]{2,1,0:T(8,128)(2,1)S(1)} %shard_map.109), channel_id=1, replica_groups=mesh['grp'=2,'sp'=16,'x'=8,'core'=2] {'x'}, dimensions={0} | all-to-all | bytes 524288 | tf_op jit(solution)/shard_map/all_to_all | solution.py:207
  (70 shorter events, 26.4 us)
Async XLA Ops:
  0.0 0.8 copy-start.2
  3.3 43.8 %copy-start = (bf16[256,128]{1,0:T(8,128)(2,1)S(1)}, bf16[256,128]{1,0:T(8,128)(2,1)}, u32[]{:S(2)}) copy-start(bf16[256,128]{1,0:T(8,128)(2,1)} %residual_ref.1) | copy-start | bytes 196612
  3.3 82.7 %all-to-all-start = ((bf16[16,192,128]{2,1,0:T(8,128)(2,1)}), bf16[16,192,128]{2,1,0:T(8,128)(2,1)S(1)}, u32[]{:S(2)}, u32[]{:S(2)}) async-start(bf16[16,192,128]{2,1,0:T(8,128)(2,1)} %get-tuple-element.28), calls=%async_computation | async-start | bytes 1572864 | tf_op jit(solution)/shard_map/all_to_all | solution.py:207
  47.2 10.7 %collective-permute-start = (bf16[256,128]{1,0:T(8,128)(2,1)S(1)}, bf16[256,128]{1,0:T(8,128)(2,1)S(1)}, u32[]{:S(2)}, u32[]{:S(2)}) collective-permute-start(bf16[256,128]{1,0:T(8,128)(2,1)S(1)} %copy-done), channel_id=1, source_target_pairs={{0,8},{2,10},{4,12},{6,14},{8,0},{10,2},{12,4},{14,6},{1,9},{3,11}... | collective-permute-start | bytes 196616 | tf_op jit(solution)/shard_map/ppermute | solution.py:212
  57.9 9.5 %copy-start.8 = (f32[2,4,64]{2,1,0:T(4,128)S(1)}, f32[2,4,64]{2,1,0:T(4,128)}, u32[]{:S(2)}) copy-start(f32[2,4,64]{2,1,0:T(4,128)} %param.14) | copy-start | bytes 6148
  57.9 9.5 %copy-start.5 = (bf16[2,1,64,64]{3,2,1,0:T(8,128)(2,1)S(1)}, bf16[2,1,64,64]{3,2,1,0:T(8,128)(2,1)}, u32[]{:S(2)}) copy-start(bf16[2,1,64,64]{3,2,1,0:T(8,128)(2,1)} %param.15) | copy-start | bytes 49156
  57.9 13.4 %collective-permute-start.1 = (bf16[2,256,128]{2,1,0:T(8,128)(2,1)S(1)}, bf16[2,256,128]{2,1,0:T(8,128)(2,1)S(1)}, u32[]{:S(2)}, u32[]{:S(2)}) collective-permute-start(bf16[2,256,128]{2,1,0:T(8,128)(2,1)S(1)} %pad_maximum_fusion.1), channel_id=1, source_target_pairs={{0,12},{2,14},{4,0},{6,2},{8,4},{10,6},{12,8},{14,10},{1,13},{3,15... | collective-permute-start | bytes 393224 | tf_op jit(solution)/shard_map/ppermute | solution.py:212
  64.5 8.0 %collective-permute-start.2 = (bf16[2,256,128]{2,1,0:T(8,128)(2,1)S(1)}, bf16[2,256,128]{2,1,0:T(8,128)(2,1)S(1)}, u32[]{:S(2)}, u32[]{:S(2)}) collective-permute-start(bf16[2,256,128]{2,1,0:T(8,128)(2,1)S(1)} %pad_maximum_fusion.1), channel_id=1, source_target_pairs={{0,14},{2,0},{4,2},{6,4},{8,6},{10,8},{12,10},{14,12},{1,15},{3,1}... | collective-permute-start | bytes 393224 | tf_op jit(solution)/shard_map/ppermute | solution.py:212
  67.4 0.8 copy-start.6
  68.3 8.1 %collective-permute-start.3 = (bf16[2,256,128]{2,1,0:T(8,128)(2,1)S(1)}, bf16[2,256,128]{2,1,0:T(8,128)(2,1)S(1)}, u32[]{:S(2)}, u32[]{:S(2)}) collective-permute-start(bf16[2,256,128]{2,1,0:T(8,128)(2,1)S(1)} %pad_maximum_fusion.1), channel_id=1, source_target_pairs={{0,2},{2,4},{4,6},{6,8},{8,10},{10,12},{12,14},{14,0},{1,3},{3,5},... | collective-permute-start | bytes 393224 | tf_op jit(solution)/shard_map/ppermute | solution.py:212
  76.4 3.8 %collective-permute-start.4 = (bf16[8,256,128]{2,1,0:T(8,128)(2,1)S(1)}, bf16[8,256,128]{2,1,0:T(8,128)(2,1)S(1)}, u32[]{:S(2)}, u32[]{:S(2)}) collective-permute-start(bf16[8,256,128]{2,1,0:T(8,128)(2,1)S(1)} %constant_dynamic-update-slice_fusion.mine_ref), channel_id=1, source_target_pairs={{0,1},{1,0},{2,3},{3,2},{4,5},{5,4},{6,7},{7,6},{8,9},{9,8},{10,11... | collective-permute-start | bytes 1572872 | tf_op jit(solution)/shard_map/ppermute | solution.py:212
  86.5 5.6 %copy-start.1 = (f32[2,64,256]{2,1,0:T(8,128)S(1)}, f32[2,64,256]{2,1,0:T(8,128)}, u32[]{:S(2)}) copy-start(f32[2,64,256]{2,1,0:T(8,128)} %offset_ref.3) | copy-start | bytes 393220
  86.6 5.5 %collective-permute-start.5 = (bf16[64,128]{1,0:T(8,128)(2,1)S(1)}, bf16[64,128]{1,0:T(8,128)(2,1)S(1)}, u32[]{:S(2)}, u32[]{:S(2)}) collective-permute-start(bf16[64,128]{1,0:T(8,128)(2,1)S(1)} %get-tuple-element.30), channel_id=1, source_target_pairs={{0,16},{16,32},{32,48},{48,64},{64,80},{80,96},{96,112},{112,128},... | collective-permute-start | bytes 49160 | tf_op jit(solution)/shard_map/ppermute | solution.py:263
  132.3 22.1 %collective-permute-start.6 = (bf16[8,64,256]{2,1,0:T(8,128)(2,1)S(1)}, bf16[8,64,256]{2,1,0:T(8,128)(2,1)S(1)}, u32[]{:S(2)}, u32[]{:S(2)}) collective-permute-start(bf16[8,64,256]{2,1,0:T(8,128)(2,1)S(1)} %all_to_all.31.mine_ref), channel_id=1, source_target_pairs={{0,1},{1,0},{2,3},{3,2},{4,5},{5,4},{6,7},{7,6},{8,9},{9,8},{10,11... | collective-permute-start | bytes 786440 | tf_op jit(solution)/shard_map/ppermute | solution.py:212
  134.2 10.3 %collective-permute-start.8 = (bf16[192,128]{1,0:T(8,128)(2,1)S(1)}, bf16[192,128]{1,0:T(8,128)(2,1)S(1)}, u32[]{:S(2)}, u32[]{:S(2)}) collective-permute-start(bf16[192,128]{1,0:T(8,128)(2,1)S(1)} %get-tuple-element.40), channel_id=1, source_target_pairs={{0,64},{16,80},{32,96},{48,112},{64,128},{80,144},{96,160},{112,17... | collective-permute-start | bytes 147464 | tf_op jit(solution)/shard_map/ppermute | solution.py:212
  144.5 14.7 %collective-permute-start.10 = (bf16[192,128]{1,0:T(8,128)(2,1)S(1)}, bf16[192,128]{1,0:T(8,128)(2,1)S(1)}, u32[]{:S(2)}, u32[]{:S(2)}) collective-permute-start(bf16[192,128]{1,0:T(8,128)(2,1)S(1)} %get-tuple-element.40), channel_id=1, source_target_pairs={{0,192},{16,208},{32,224},{48,240},{64,0},{80,16},{96,32},{112,48}... | collective-permute-start | bytes 147464 | tf_op jit(solution)/shard_map/ppermute | solution.py:212
  147.0 12.2 %collective-permute-start.9 = (bf16[192,128]{1,0:T(8,128)(2,1)S(1)}, bf16[192,128]{1,0:T(8,128)(2,1)S(1)}, u32[]{:S(2)}, u32[]{:S(2)}) collective-permute-start(bf16[192,128]{1,0:T(8,128)(2,1)S(1)} %collective-permute-done.8), channel_id=1, source_target_pairs={{0,64},{16,80},{32,96},{48,112},{64,128},{80,144},{96,160},{112,17... | collective-permute-start | bytes 147464 | tf_op jit(solution)/shard_map/ppermute | solution.py:212
  155.5 22.4 %all-to-all-start.3 = ((bf16[8,256,128]{2,1,0:T(8,128)(2,1)}), bf16[8,256,128]{2,1,0:T(8,128)(2,1)S(1)}, u32[]{:S(2)}, u32[]{:S(2)}) async-start(bf16[8,256,128]{2,1,0:T(8,128)(2,1)} %get-tuple-element.35), calls=%async_computation.3 | async-start | bytes 1048576 | tf_op jit(solution)/shard_map/all_to_all | solution.py:207
  159.3 13.8 %collective-permute-start.11 = (bf16[4,192,128]{2,1,0:T(8,128)(2,1)S(1)}, bf16[4,192,128]{2,1,0:T(8,128)(2,1)S(1)}, u32[]{:S(2)}, u32[]{:S(2)}) collective-permute-start(bf16[4,192,128]{2,1,0:T(8,128)(2,1)S(1)} %pad_maximum_fusion), channel_id=1, source_target_pairs={{0,224},{16,240},{32,0},{48,16},{64,32},{80,48},{96,64},{112,80},{... | collective-permute-start | bytes 589832 | tf_op jit(solution)/shard_map/ppermute | solution.py:212
  164.5 13.3 %collective-permute-start.12 = (bf16[4,192,128]{2,1,0:T(8,128)(2,1)S(1)}, bf16[4,192,128]{2,1,0:T(8,128)(2,1)S(1)}, u32[]{:S(2)}, u32[]{:S(2)}) collective-permute-start(bf16[4,192,128]{2,1,0:T(8,128)(2,1)S(1)} %pad_maximum_fusion), channel_id=1, source_target_pairs={{0,240},{16,0},{32,16},{48,32},{64,48},{80,64},{96,80},{112,96},{1... | collective-permute-start | bytes 589832 | tf_op jit(solution)/shard_map/ppermute | solution.py:212
  166.6 13.4 %collective-permute-start.13 = (bf16[4,192,128]{2,1,0:T(8,128)(2,1)S(1)}, bf16[4,192,128]{2,1,0:T(8,128)(2,1)S(1)}, u32[]{:S(2)}, u32[]{:S(2)}) collective-permute-start(bf16[4,192,128]{2,1,0:T(8,128)(2,1)S(1)} %pad_maximum_fusion), channel_id=1, source_target_pairs={{0,16},{16,32},{32,48},{48,64},{64,80},{80,96},{96,112},{112,128},... | collective-permute-start | bytes 589832 | tf_op jit(solution)/shard_map/ppermute | solution.py:212
  177.9 3.8 %collective-permute-start.7 = (bf16[8,256,128]{2,1,0:T(8,128)(2,1)S(1)}, bf16[8,256,128]{2,1,0:T(8,128)(2,1)S(1)}, u32[]{:S(2)}, u32[]{:S(2)}) collective-permute-start(bf16[8,256,128]{2,1,0:T(8,128)(2,1)S(1)} %all-to-all-done.3.mine_ref), channel_id=1, source_target_pairs={{0,1},{1,0},{2,3},{3,2},{4,5},{5,4},{6,7},{7,6},{8,9},{9,8},{10,11... | collective-permute-start | bytes 1572872 | tf_op jit(solution)/shard_map/ppermute | solution.py:212
  182.3 2.9 %collective-permute-start.14 = (bf16[64,128]{1,0:T(8,128)(2,1)S(1)}, bf16[64,128]{1,0:T(8,128)(2,1)S(1)}, u32[]{:S(2)}, u32[]{:S(2)}) collective-permute-start(bf16[64,128]{1,0:T(8,128)(2,1)S(1)} %get-tuple-element.45), channel_id=1, source_target_pairs={{0,16},{16,32},{32,48},{48,64},{64,80},{80,96},{96,112},{112,128},... | collective-permute-start | bytes 49160 | tf_op jit(solution)/shard_map/ppermute | solution.py:263
  222.5 3.4 %collective-permute-start.15 = (bf16[8,64,256]{2,1,0:T(8,128)(2,1)S(1)}, bf16[8,64,256]{2,1,0:T(8,128)(2,1)S(1)}, u32[]{:S(2)}, u32[]{:S(2)}) collective-permute-start(bf16[8,64,256]{2,1,0:T(8,128)(2,1)S(1)} %all_to_all.33.mine_ref), channel_id=1, source_target_pairs={{0,1},{1,0},{2,3},{3,2},{4,5},{5,4},{6,7},{7,6},{8,9},{9,8},{10,11... | collective-permute-start | bytes 786440 | tf_op jit(solution)/shard_map/ppermute | solution.py:212
  (4 other events, 2.9 us)

commit v3 on v2

--- a/solution.py
+++ b/solution.py
@@ -76,18 +76,21 @@
 
 def blocks_of(chips, count, hopped, slotted=False):
     chip, core, place = (lax.axis_index(name) for name in ("x", "core", "sp"))
-    far = chips // len(NEAR)
+    steps = len(NEAR)
+    own_sign = 1 - 2 * core
     for side in range(2):
         for slot in range(chips):
-            source = slot
+            source, sign = slot, own_sign if side == 0 else -own_sign
             if slotted:
-                behind = slot % far * len(NEAR) + slot // far + NEAR[0]
-                source = lax.rem(chip + chips - behind, chips)
+                far = chips // steps
+                behind = slot % far * steps + sign * NEAR[slot // far]
+                source = lax.rem(chip + 2 * chips - behind, chips)
             block = 2 * source + (core if side == 0 else 1 - core)
             held = block
             if hopped:
-                at = lax.rem(place + 2 * count - block - NEAR[0], count)
-                held = lax.rem(at, len(NEAR)) * (count // len(NEAR)) + lax.div(at, len(NEAR))
+                far = count // steps
+                at = lax.rem(own_sign * (place - block) + 2 * count - NEAR[0], count)
+                held = lax.rem(at, steps) * far + lax.rem(own_sign * lax.div(at, steps) + far, far)
             yield side, slot, block, held
 
 
@@ -135,12 +138,23 @@
         ref[...] = jnp.broadcast_to(mixed[None], ref.shape)
 
 
-def pack_kernel(value_ref, gate_ref, mix_ref, *out_refs):
-    for layer, out_ref in enumerate(out_refs):
-        rows = jnp.concatenate([value_ref[layer], gate_ref[layer], mix_ref[layer]], axis=0)
-        if len(out_ref.shape) == 3:
-            rows = jnp.broadcast_to(rows[None], out_ref.shape)
-        out_ref[...] = rows
+def pack_kernel(value_ref, gate_ref, mix_ref, first_ref, *rest_refs):
+    *later_refs, sems = rest_refs
+    channels = value_ref.shape[1]
+    moves = []
+    for layer, rows_ref in enumerate((first_ref.at[0], *later_refs)):
+        for k, shard_ref in enumerate((value_ref, gate_ref, mix_ref)):
+            target = rows_ref.at[pl.ds(k * channels, channels)]
+            moves.append(
+                pltpu.make_async_copy(shard_ref.at[layer], target, sems.at[len(moves)])
+            )
+    for move in moves:
+        move.start()
+    for move in moves:
+        move.wait()
+    rows = first_ref[0]
+    for at in range(1, first_ref.shape[0]):
+        first_ref[at] = rows
 
 
 def vmem(n):
@@ -158,7 +172,14 @@
     rows = (3 * channels, width)
     out = [pltpu.VMEM((count, *rows), value_proj.dtype)]
     out += [pltpu.VMEM(rows, value_proj.dtype)] * (layers - 1)
-    return kernel_call(pack_kernel, out, value_proj, gate_proj, mix_proj)
+    return pl.pallas_call(
+        pack_kernel,
+        out_shape=out,
+        in_specs=[pl.BlockSpec(memory_space=pl.ANY)] * 3,
+        out_specs=vmem(len(out)),
+        scratch_shapes=[pltpu.SemaphoreType.DMA((3 * layers,))],
+        name="pack",
+    )(value_proj, gate_proj, mix_proj)
 
 
 def project_call(slotted, hopped, mine, theirs, gains, weights):
@@ -217,7 +238,17 @@
 
 
 def near_hops(held, axis):
-    return jnp.concatenate([shift(held, axis, n) if n else held for n in NEAR])
+    count, cores = lax.axis_size(axis), lax.axis_size("core")
+
+    def hop(steps):
+        pairs = [
+            (i * cores + c, (i + steps * (1 - 2 * c)) % count * cores + c)
+            for i in range(count)
+            for c in range(cores)
+        ]
+        return lax.ppermute(held, (axis, "core"), pairs)
+
+    return jnp.concatenate([hop(n) if n else held for n in NEAR])
 
 
 def local(
@@ -242,6 +273,8 @@
     weights = exchange(first, "sp")
     held = jnp.stack([tokens, far_hop(tokens, "x")])
     mine = near_hops(held, "x")
+    _, shard = lax.optimization_barrier((mine, shard))
+    hop_one = far_hop(shard, "sp")
     rates = -RATE_SCALE * jax.nn.softplus(-decay_param)
     consts = jnp.concatenate([conv_taps.transpose(0, 2, 1), rates[:, :, None]], axis=2)
     consts = jnp.pad(consts, ((0, 0), (0, 0), (0, LANES - consts.shape[2])))
@@ -263,9 +296,6 @@
         before = lax.ppermute(tail, "sp", [(i, i + 1) for i in range(count - 1)])
         cum, state, msg = scan_call(layer, value_rows, before, consts, maps, decay_offset, count)
         msgs = exchange(msg, "sp")
-        if more:
-            _, shard = lax.optimization_barrier((msg, shard))
-            hop_one = far_hop(shard, "sp")
         sent = close_call(msgs, cum, state, gate_rows, chips)
         mine = exchange(sent, "x")
         if more:

time: 229 us -> 226 us (0.987)
    ppermute x14 -> x8, starting transfers between devices: 51.6 us -> 28 us  [shift(): lax.ppermute(array, axis, [(i, (i + steps) % count) for i in range(count)])]
    ppermute x0 -> x6, starting transfers between devices: none -> 23.6 us  [hop(): return lax.ppermute(held, (axis, 'core'), pairs)]
    ppermute x14 -> x8, waiting for transfers between devices: 27.4 us -> 15 us  [shift(): lax.ppermute(array, axis, [(i, (i + steps) % count) for i in range(count)])]
    ppermute x0 -> x6, waiting for transfers between devices: none -> 9 us  [hop(): return lax.ppermute(held, (axis, 'core'), pairs)]
    pallas_call x11 -> x10, Pallas kernels: 6.58 us -> 5.53 us  [kernel_call(): pl.pallas_call(kernel, out_shape=out_shape, in_specs=vmem(len(operands)),...]
where the time goes in v3:
time: 226 us; the launch traced here: 224 us
  starting transfers between devices  105 us (46%)
  blocking collectives  74.9 us (33%)
  waiting for transfers between devices  34.3 us (15%)
  Pallas kernels  7.43 us (3%)
    all_to_all x4, blocking collectives, exchange(): return lax.all_to_all(copies, axis, split_axis=0, concat_axis=0, tiled=True)  74.9 us
    all_to_all x2, starting transfers between devices, exchange(): return lax.all_to_all(copies, axis, split_axis=0, concat_axis=0, tiled=True)  47.5 us
    ppermute x8, starting transfers between devices, shift(): lax.ppermute(array, axis, [(i, (i + steps) % count) for i in range(count)])  28 us
    ppermute x6, starting transfers between devices, hop(): return lax.ppermute(held, (axis, 'core'), pairs)  23.6 us
    ppermute x8, waiting for transfers between devices, shift(): lax.ppermute(array, axis, [(i, (i + steps) % count) for i in range(count)])  15 us
    ppermute x6, waiting for transfers between devices, hop(): return lax.ppermute(held, (axis, 'core'), pairs)  9 us
    all_to_all x2, waiting for transfers between devices, exchange(): return lax.all_to_all(copies, axis, split_axis=0, concat_axis=0, tiled=True)  7.53 us
    ppermute x2, starting transfers between devices, local(): before = lax.ppermute(tail, 'sp', [(i, i + 1) for i in range(count - 1)])  5.99 us
  transfers between devices with their start and end apart: 18, of which 12 were waited for; matrix products, arithmetic and copies ran while one was open for 0% of the time, Pallas kernels for 1%

profile of v3, /device:TPU:80, one launch (start us, length us, event | category | flops | bytes accessed | tf_op | source)
XLA Modules:
  0.0 224.1 jit_solution(7594346135326745552)
XLA Ops:
  1.9 43.8 %all-to-all-start = ((bf16[16,192,128]{2,1,0:T(8,128)(2,1)}), bf16[16,192,128]{2,1,0:T(8,128)(2,1)S(1)}, u32[]{:S(2)}, u32[]{:S(2)}) async-start(bf16[16,192,128]{2,1,0:T(8,128)(2,1)} %get-tuple-element.28), calls=%async_computation | async-start | bytes 1572864 | tf_op jit(solution)/shard_map/all_to_all | solution.py:228
  45.8 8.0 %collective-permute-start = (bf16[256,128]{1,0:T(8,128)(2,1)S(1)}, bf16[256,128]{1,0:T(8,128)(2,1)S(1)}, u32[]{:S(2)}, u32[]{:S(2)}) collective-permute-start(bf16[256,128]{1,0:T(8,128)(2,1)S(1)} %copy-done), channel_id=1, source_target_pairs={{0,8},{2,10},{4,12},{6,14},{8,0},{10,2},{12,4},{14,6},{1,9},{3,11}... | collective-permute-start | bytes 196616 | tf_op jit(solution)/shard_map/ppermute | solution.py:233
  53.7 2.8 %collective-permute-done = bf16[256,128]{1,0:T(8,128)(2,1)S(1)} collective-permute-done((bf16[256,128]{1,0:T(8,128)(2,1)S(1)}, bf16[256,128]{1,0:T(8,128)(2,1)S(1)}, u32[]{:S(2)}, u32[]{:S(2)}) %collective-permute-start) | collective-permute-done | bytes 65568 | tf_op jit(solution)/shard_map/ppermute | solution.py:233
  56.5 6.6 %collective-permute-start.1 = (bf16[2,256,128]{2,1,0:T(8,128)(2,1)S(1)}, bf16[2,256,128]{2,1,0:T(8,128)(2,1)S(1)}, u32[]{:S(2)}, u32[]{:S(2)}) collective-permute-start(bf16[2,256,128]{2,1,0:T(8,128)(2,1)S(1)} %pad_maximum_fusion.1), channel_id=1, source_target_pairs={{0,12},{1,5},{2,14},{3,7},{4,0},{5,9},{6,2},{7,11},{8,4},{9,13},{1... | collective-permute-start | bytes 393224 | tf_op jit(solution)/shard_map/ppermute | solution.py:249
  63.1 2.9 %collective-permute-start.2 = (bf16[2,256,128]{2,1,0:T(8,128)(2,1)S(1)}, bf16[2,256,128]{2,1,0:T(8,128)(2,1)S(1)}, u32[]{:S(2)}, u32[]{:S(2)}) collective-permute-start(bf16[2,256,128]{2,1,0:T(8,128)(2,1)S(1)} %pad_maximum_fusion.1), channel_id=1, source_target_pairs={{0,14},{1,3},{2,0},{3,5},{4,2},{5,7},{6,4},{7,9},{8,6},{9,11},{10,... | collective-permute-start | bytes 393224 | tf_op jit(solution)/shard_map/ppermute | solution.py:249
  66.9 3.0 %collective-permute-start.3 = (bf16[2,256,128]{2,1,0:T(8,128)(2,1)S(1)}, bf16[2,256,128]{2,1,0:T(8,128)(2,1)S(1)}, u32[]{:S(2)}, u32[]{:S(2)}) collective-permute-start(bf16[2,256,128]{2,1,0:T(8,128)(2,1)S(1)} %pad_maximum_fusion.1), channel_id=1, source_target_pairs={{0,2},{1,15},{2,4},{3,1},{4,6},{5,3},{6,8},{7,5},{8,10},{9,7},{10,... | collective-permute-start | bytes 393224 | tf_op jit(solution)/shard_map/ppermute | solution.py:249
  70.9 4.0 %collective-permute-done.3 = bf16[2,256,128]{2,1,0:T(8,128)(2,1)S(1)} collective-permute-done((bf16[2,256,128]{2,1,0:T(8,128)(2,1)S(1)}, bf16[2,256,128]{2,1,0:T(8,128)(2,1)S(1)}, u32[]{:S(2)}, u32[]{:S(2)}) %collective-permute-start.3) | collective-permute-done | bytes 131104 | tf_op jit(solution)/shard_map/ppermute | solution.py:249
  75.0 2.0 collective-permute-start.4
  78.8 5.8 %all-to-all-done.weight_ref = bf16[16,192,128]{2,1,0:T(8,128)(2,1)S(1)} async-done(((bf16[16,192,128]{2,1,0:T(8,128)(2,1)}), bf16[16,192,128]{2,1,0:T(8,128)(2,1)S(1)}, u32[]{:S(2)}, u32[]{:S(2)}) %all-to-all-start) | async-done | bytes 786464 | tf_op jit(solution)/shard_map/all_to_all | solution.py:228
  85.2 4.1 %collective-permute-start.5 = (bf16[64,128]{1,0:T(8,128)(2,1)S(1)}, bf16[64,128]{1,0:T(8,128)(2,1)S(1)}, u32[]{:S(2)}, u32[]{:S(2)}) collective-permute-start(bf16[64,128]{1,0:T(8,128)(2,1)S(1)} %get-tuple-element.30), channel_id=1, source_target_pairs={{0,16},{16,32},{32,48},{48,64},{64,80},{80,96},{96,112},{112,128},... | collective-permute-start | bytes 49160 | tf_op jit(solution)/shard_map/ppermute | solution.py:296
  91.7 21.3 %all_to_all.30.msgs_ref = f32[16,1,128]{2,1,0:T(1,128)S(1)} all-to-all(f32[16,1,128]{2,1,0:T(1,128)S(1)} %get-tuple-element.31), channel_id=1, replica_groups=mesh['grp'=2,'sp'=16,'x'=8,'core'=2] {'sp'}, dimensions={0} | all-to-all | bytes 16384 | tf_op jit(solution)/shard_map/all_to_all | solution.py:228
  113.3 17.6 %all_to_all.31.mine_ref = bf16[8,64,256]{2,1,0:T(8,128)(2,1)S(1)} all-to-all(bf16[8,64,256]{2,1,0:T(8,128)(2,1)S(1)} %shard_map.102), channel_id=1, replica_groups=mesh['grp'=2,'sp'=16,'x'=8,'core'=2] {'x'}, dimensions={0} | all-to-all | bytes 524288 | tf_op jit(solution)/shard_map/all_to_all | solution.py:228
  130.9 1.9 collective-permute-start.6
  132.8 2.5 %collective-permute-start.8 = (bf16[192,128]{1,0:T(8,128)(2,1)S(1)}, bf16[192,128]{1,0:T(8,128)(2,1)S(1)}, u32[]{:S(2)}, u32[]{:S(2)}) collective-permute-start(bf16[192,128]{1,0:T(8,128)(2,1)S(1)} %get-tuple-element.40), channel_id=1, source_target_pairs={{0,64},{16,80},{32,96},{48,112},{64,128},{80,144},{96,160},{112,17... | collective-permute-start | bytes 147464 | tf_op jit(solution)/shard_map/ppermute | solution.py:233
  135.3 7.8 %collective-permute-done.8 = bf16[192,128]{1,0:T(8,128)(2,1)S(1)} collective-permute-done((bf16[192,128]{1,0:T(8,128)(2,1)S(1)}, bf16[192,128]{1,0:T(8,128)(2,1)S(1)}, u32[]{:S(2)}, u32[]{:S(2)}) %collective-permute-start.8) | collective-permute-done | bytes 49184 | tf_op jit(solution)/shard_map/ppermute | solution.py:233
  143.2 2.5 %collective-permute-start.10 = (bf16[192,128]{1,0:T(8,128)(2,1)S(1)}, bf16[192,128]{1,0:T(8,128)(2,1)S(1)}, u32[]{:S(2)}, u32[]{:S(2)}) collective-permute-start(bf16[192,128]{1,0:T(8,128)(2,1)S(1)} %get-tuple-element.40), channel_id=1, source_target_pairs={{0,192},{16,208},{32,224},{48,240},{64,0},{80,16},{96,32},{112,48}... | collective-permute-start | bytes 147464 | tf_op jit(solution)/shard_map/ppermute | solution.py:233
  145.7 7.3 %collective-permute-start.9 = (bf16[192,128]{1,0:T(8,128)(2,1)S(1)}, bf16[192,128]{1,0:T(8,128)(2,1)S(1)}, u32[]{:S(2)}, u32[]{:S(2)}) collective-permute-start(bf16[192,128]{1,0:T(8,128)(2,1)S(1)} %collective-permute-done.8), channel_id=1, source_target_pairs={{0,64},{16,80},{32,96},{48,112},{64,128},{80,144},{96,160},{112,17... | collective-permute-start | bytes 147464 | tf_op jit(solution)/shard_map/ppermute | solution.py:233
  154.1 3.7 %all-to-all-start.3 = ((bf16[8,256,128]{2,1,0:T(8,128)(2,1)}), bf16[8,256,128]{2,1,0:T(8,128)(2,1)S(1)}, u32[]{:S(2)}, u32[]{:S(2)}) async-start(bf16[8,256,128]{2,1,0:T(8,128)(2,1)} %get-tuple-element.35), calls=%async_computation.3 | async-start | bytes 1048576 | tf_op jit(solution)/shard_map/all_to_all | solution.py:228
  157.9 5.2 %collective-permute-start.11 = (bf16[4,192,128]{2,1,0:T(8,128)(2,1)S(1)}, bf16[4,192,128]{2,1,0:T(8,128)(2,1)S(1)}, u32[]{:S(2)}, u32[]{:S(2)}) collective-permute-start(bf16[4,192,128]{2,1,0:T(8,128)(2,1)S(1)} %pad_maximum_fusion), channel_id=1, source_target_pairs={{0,224},{1,33},{16,240},{17,49},{32,0},{33,65},{48,16},{49,81},{64... | collective-permute-start | bytes 589832 | tf_op jit(solution)/shard_map/ppermute | solution.py:249
  163.1 2.0 collective-permute-start.12
  165.2 3.9 %collective-permute-start.13 = (bf16[4,192,128]{2,1,0:T(8,128)(2,1)S(1)}, bf16[4,192,128]{2,1,0:T(8,128)(2,1)S(1)}, u32[]{:S(2)}, u32[]{:S(2)}) collective-permute-start(bf16[4,192,128]{2,1,0:T(8,128)(2,1)S(1)} %pad_maximum_fusion), channel_id=1, source_target_pairs={{0,16},{1,241},{16,32},{17,1},{32,48},{33,17},{48,64},{49,33},{64,... | collective-permute-start | bytes 589832 | tf_op jit(solution)/shard_map/ppermute | solution.py:249
  169.1 4.0 %collective-permute-done.12 = bf16[4,192,128]{2,1,0:T(8,128)(2,1)S(1)} collective-permute-done((bf16[4,192,128]{2,1,0:T(8,128)(2,1)S(1)}, bf16[4,192,128]{2,1,0:T(8,128)(2,1)S(1)}, u32[]{:S(2)}, u32[]{:S(2)}) %collective-permute-start.12) | collective-permute-done | bytes 196640 | tf_op jit(solution)/shard_map/ppermute | solution.py:249
  183.6 21.2 %all_to_all.32.msgs_ref = f32[16,1,128]{2,1,0:T(1,128)S(1)} all-to-all(f32[16,1,128]{2,1,0:T(1,128)S(1)} %get-tuple-element.46), channel_id=1, replica_groups=mesh['grp'=2,'sp'=16,'x'=8,'core'=2] {'sp'}, dimensions={0} | all-to-all | bytes 16384 | tf_op jit(solution)/shard_map/all_to_all | solution.py:228
  205.0 14.7 %all_to_all.33.mine_ref = bf16[8,64,256]{2,1,0:T(8,128)(2,1)S(1)} all-to-all(bf16[8,64,256]{2,1,0:T(8,128)(2,1)S(1)} %shard_map.108), channel_id=1, replica_groups=mesh['grp'=2,'sp'=16,'x'=8,'core'=2] {'x'}, dimensions={0} | all-to-all | bytes 524288 | tf_op jit(solution)/shard_map/all_to_all | solution.py:228
  (64 shorter events, 24.9 us)
Async XLA Ops:
  1.9 43.8 %copy-start = (bf16[256,128]{1,0:T(8,128)(2,1)S(1)}, bf16[256,128]{1,0:T(8,128)(2,1)}, u32[]{:S(2)}) copy-start(bf16[256,128]{1,0:T(8,128)(2,1)} %residual_ref.1) | copy-start | bytes 196612
  1.9 82.7 %all-to-all-start = ((bf16[16,192,128]{2,1,0:T(8,128)(2,1)}), bf16[16,192,128]{2,1,0:T(8,128)(2,1)S(1)}, u32[]{:S(2)}, u32[]{:S(2)}) async-start(bf16[16,192,128]{2,1,0:T(8,128)(2,1)} %get-tuple-element.28), calls=%async_computation | async-start | bytes 1572864 | tf_op jit(solution)/shard_map/all_to_all | solution.py:228
  45.8 10.7 %collective-permute-start = (bf16[256,128]{1,0:T(8,128)(2,1)S(1)}, bf16[256,128]{1,0:T(8,128)(2,1)S(1)}, u32[]{:S(2)}, u32[]{:S(2)}) collective-permute-start(bf16[256,128]{1,0:T(8,128)(2,1)S(1)} %copy-done), channel_id=1, source_target_pairs={{0,8},{2,10},{4,12},{6,14},{8,0},{10,2},{12,4},{14,6},{1,9},{3,11}... | collective-permute-start | bytes 196616 | tf_op jit(solution)/shard_map/ppermute | solution.py:233
  56.5 9.5 %copy-start.5 = (f32[2,4,64]{2,1,0:T(4,128)S(1)}, f32[2,4,64]{2,1,0:T(4,128)}, u32[]{:S(2)}) copy-start(f32[2,4,64]{2,1,0:T(4,128)} %param.14) | copy-start | bytes 6148
  56.5 9.5 %copy-start.2 = (bf16[2,1,64,64]{3,2,1,0:T(8,128)(2,1)S(1)}, bf16[2,1,64,64]{3,2,1,0:T(8,128)(2,1)}, u32[]{:S(2)}) copy-start(bf16[2,1,64,64]{3,2,1,0:T(8,128)(2,1)} %param.15) | copy-start | bytes 49156
  56.5 13.4 %collective-permute-start.1 = (bf16[2,256,128]{2,1,0:T(8,128)(2,1)S(1)}, bf16[2,256,128]{2,1,0:T(8,128)(2,1)S(1)}, u32[]{:S(2)}, u32[]{:S(2)}) collective-permute-start(bf16[2,256,128]{2,1,0:T(8,128)(2,1)S(1)} %pad_maximum_fusion.1), channel_id=1, source_target_pairs={{0,12},{1,5},{2,14},{3,7},{4,0},{5,9},{6,2},{7,11},{8,4},{9,13},{1... | collective-permute-start | bytes 393224 | tf_op jit(solution)/shard_map/ppermute | solution.py:249
  63.1 7.8 %collective-permute-start.2 = (bf16[2,256,128]{2,1,0:T(8,128)(2,1)S(1)}, bf16[2,256,128]{2,1,0:T(8,128)(2,1)S(1)}, u32[]{:S(2)}, u32[]{:S(2)}) collective-permute-start(bf16[2,256,128]{2,1,0:T(8,128)(2,1)S(1)} %pad_maximum_fusion.1), channel_id=1, source_target_pairs={{0,14},{1,3},{2,0},{3,5},{4,2},{5,7},{6,4},{7,9},{8,6},{9,11},{10,... | collective-permute-start | bytes 393224 | tf_op jit(solution)/shard_map/ppermute | solution.py:249
  66.0 0.8 copy-start.3
  66.9 8.1 %collective-permute-start.3 = (bf16[2,256,128]{2,1,0:T(8,128)(2,1)S(1)}, bf16[2,256,128]{2,1,0:T(8,128)(2,1)S(1)}, u32[]{:S(2)}, u32[]{:S(2)}) collective-permute-start(bf16[2,256,128]{2,1,0:T(8,128)(2,1)S(1)} %pad_maximum_fusion.1), channel_id=1, source_target_pairs={{0,2},{1,15},{2,4},{3,1},{4,6},{5,3},{6,8},{7,5},{8,10},{9,7},{10,... | collective-permute-start | bytes 393224 | tf_op jit(solution)/shard_map/ppermute | solution.py:249
  75.0 3.8 %collective-permute-start.4 = (bf16[8,256,128]{2,1,0:T(8,128)(2,1)S(1)}, bf16[8,256,128]{2,1,0:T(8,128)(2,1)S(1)}, u32[]{:S(2)}, u32[]{:S(2)}) collective-permute-start(bf16[8,256,128]{2,1,0:T(8,128)(2,1)S(1)} %constant_dynamic-update-slice_fusion.mine_ref), channel_id=1, source_target_pairs={{0,1},{1,0},{2,3},{3,2},{4,5},{5,4},{6,7},{7,6},{8,9},{9,8},{10,11... | collective-permute-start | bytes 1572872 | tf_op jit(solution)/shard_map/ppermute | solution.py:233
  77.0 0.7 copy-start.4
  85.1 5.6 %copy-start.1 = (f32[2,64,256]{2,1,0:T(8,128)S(1)}, f32[2,64,256]{2,1,0:T(8,128)}, u32[]{:S(2)}) copy-start(f32[2,64,256]{2,1,0:T(8,128)} %offset_ref.3) | copy-start | bytes 393220
  85.2 5.5 %collective-permute-start.5 = (bf16[64,128]{1,0:T(8,128)(2,1)S(1)}, bf16[64,128]{1,0:T(8,128)(2,1)S(1)}, u32[]{:S(2)}, u32[]{:S(2)}) collective-permute-start(bf16[64,128]{1,0:T(8,128)(2,1)S(1)} %get-tuple-element.30), channel_id=1, source_target_pairs={{0,16},{16,32},{32,48},{48,64},{64,80},{80,96},{96,112},{112,128},... | collective-permute-start | bytes 49160 | tf_op jit(solution)/shard_map/ppermute | solution.py:296
  130.9 22.1 %collective-permute-start.6 = (bf16[8,64,256]{2,1,0:T(8,128)(2,1)S(1)}, bf16[8,64,256]{2,1,0:T(8,128)(2,1)S(1)}, u32[]{:S(2)}, u32[]{:S(2)}) collective-permute-start(bf16[8,64,256]{2,1,0:T(8,128)(2,1)S(1)} %all_to_all.31.mine_ref), channel_id=1, source_target_pairs={{0,1},{1,0},{2,3},{3,2},{4,5},{5,4},{6,7},{7,6},{8,9},{9,8},{10,11... | collective-permute-start | bytes 786440 | tf_op jit(solution)/shard_map/ppermute | solution.py:233
  132.8 10.3 %collective-permute-start.8 = (bf16[192,128]{1,0:T(8,128)(2,1)S(1)}, bf16[192,128]{1,0:T(8,128)(2,1)S(1)}, u32[]{:S(2)}, u32[]{:S(2)}) collective-permute-start(bf16[192,128]{1,0:T(8,128)(2,1)S(1)} %get-tuple-element.40), channel_id=1, source_target_pairs={{0,64},{16,80},{32,96},{48,112},{64,128},{80,144},{96,160},{112,17... | collective-permute-start | bytes 147464 | tf_op jit(solution)/shard_map/ppermute | solution.py:233
  143.2 14.7 %collective-permute-start.10 = (bf16[192,128]{1,0:T(8,128)(2,1)S(1)}, bf16[192,128]{1,0:T(8,128)(2,1)S(1)}, u32[]{:S(2)}, u32[]{:S(2)}) collective-permute-start(bf16[192,128]{1,0:T(8,128)(2,1)S(1)} %get-tuple-element.40), channel_id=1, source_target_pairs={{0,192},{16,208},{32,224},{48,240},{64,0},{80,16},{96,32},{112,48}... | collective-permute-start | bytes 147464 | tf_op jit(solution)/shard_map/ppermute | solution.py:233
  145.7 12.2 %collective-permute-start.9 = (bf16[192,128]{1,0:T(8,128)(2,1)S(1)}, bf16[192,128]{1,0:T(8,128)(2,1)S(1)}, u32[]{:S(2)}, u32[]{:S(2)}) collective-permute-start(bf16[192,128]{1,0:T(8,128)(2,1)S(1)} %collective-permute-done.8), channel_id=1, source_target_pairs={{0,64},{16,80},{32,96},{48,112},{64,128},{80,144},{96,160},{112,17... | collective-permute-start | bytes 147464 | tf_op jit(solution)/shard_map/ppermute | solution.py:233
  154.1 20.8 %all-to-all-start.3 = ((bf16[8,256,128]{2,1,0:T(8,128)(2,1)}), bf16[8,256,128]{2,1,0:T(8,128)(2,1)S(1)}, u32[]{:S(2)}, u32[]{:S(2)}) async-start(bf16[8,256,128]{2,1,0:T(8,128)(2,1)} %get-tuple-element.35), calls=%async_computation.3 | async-start | bytes 1048576 | tf_op jit(solution)/shard_map/all_to_all | solution.py:228
  157.9 11.2 %collective-permute-start.11 = (bf16[4,192,128]{2,1,0:T(8,128)(2,1)S(1)}, bf16[4,192,128]{2,1,0:T(8,128)(2,1)S(1)}, u32[]{:S(2)}, u32[]{:S(2)}) collective-permute-start(bf16[4,192,128]{2,1,0:T(8,128)(2,1)S(1)} %pad_maximum_fusion), channel_id=1, source_target_pairs={{0,224},{1,33},{16,240},{17,49},{32,0},{33,65},{48,16},{49,81},{64... | collective-permute-start | bytes 589832 | tf_op jit(solution)/shard_map/ppermute | solution.py:249
  163.1 10.0 %collective-permute-start.12 = (bf16[4,192,128]{2,1,0:T(8,128)(2,1)S(1)}, bf16[4,192,128]{2,1,0:T(8,128)(2,1)S(1)}, u32[]{:S(2)}, u32[]{:S(2)}) collective-permute-start(bf16[4,192,128]{2,1,0:T(8,128)(2,1)S(1)} %pad_maximum_fusion), channel_id=1, source_target_pairs={{0,240},{1,17},{16,0},{17,33},{32,16},{33,49},{48,32},{49,65},{64,... | collective-permute-start | bytes 589832 | tf_op jit(solution)/shard_map/ppermute | solution.py:249
  165.2 11.7 %collective-permute-start.13 = (bf16[4,192,128]{2,1,0:T(8,128)(2,1)S(1)}, bf16[4,192,128]{2,1,0:T(8,128)(2,1)S(1)}, u32[]{:S(2)}, u32[]{:S(2)}) collective-permute-start(bf16[4,192,128]{2,1,0:T(8,128)(2,1)S(1)} %pad_maximum_fusion), channel_id=1, source_target_pairs={{0,16},{1,241},{16,32},{17,1},{32,48},{33,17},{48,64},{49,33},{64,... | collective-permute-start | bytes 589832 | tf_op jit(solution)/shard_map/ppermute | solution.py:249
  174.9 3.8 %collective-permute-start.7 = (bf16[8,256,128]{2,1,0:T(8,128)(2,1)S(1)}, bf16[8,256,128]{2,1,0:T(8,128)(2,1)S(1)}, u32[]{:S(2)}, u32[]{:S(2)}) collective-permute-start(bf16[8,256,128]{2,1,0:T(8,128)(2,1)S(1)} %all-to-all-done.3.mine_ref), channel_id=1, source_target_pairs={{0,1},{1,0},{2,3},{3,2},{4,5},{5,4},{6,7},{7,6},{8,9},{9,8},{10,11... | collective-permute-start | bytes 1572872 | tf_op jit(solution)/shard_map/ppermute | solution.py:233
  179.2 3.3 %collective-permute-start.14 = (bf16[64,128]{1,0:T(8,128)(2,1)S(1)}, bf16[64,128]{1,0:T(8,128)(2,1)S(1)}, u32[]{:S(2)}, u32[]{:S(2)}) collective-permute-start(bf16[64,128]{1,0:T(8,128)(2,1)S(1)} %get-tuple-element.45), channel_id=1, source_target_pairs={{0,16},{16,32},{32,48},{48,64},{64,80},{80,96},{96,112},{112,128},... | collective-permute-start | bytes 49160 | tf_op jit(solution)/shard_map/ppermute | solution.py:296
  219.7 3.4 %collective-permute-start.15 = (bf16[8,64,256]{2,1,0:T(8,128)(2,1)S(1)}, bf16[8,64,256]{2,1,0:T(8,128)(2,1)S(1)}, u32[]{:S(2)}, u32[]{:S(2)}) collective-permute-start(bf16[8,64,256]{2,1,0:T(8,128)(2,1)S(1)} %all_to_all.33.mine_ref), channel_id=1, source_target_pairs={{0,1},{1,0},{2,3},{3,2},{4,5},{5,4},{6,7},{7,6},{8,9},{9,8},{10,11... | collective-permute-start | bytes 786440 | tf_op jit(solution)/shard_map/ppermute | solution.py:233
  (1 other events, 0.7 us)

commit v4 on v3

--- a/solution.py
+++ b/solution.py
@@ -74,24 +74,23 @@
     out_ref[...] = jnp.broadcast_to(branch[None], out_ref.shape)
 
 
-def blocks_of(chips, count, hopped, slotted=False):
-    chip, core, place = (lax.axis_index(name) for name in ("x", "core", "sp"))
-    steps = len(NEAR)
-    own_sign = 1 - 2 * core
-    for side in range(2):
-        for slot in range(chips):
-            source, sign = slot, own_sign if side == 0 else -own_sign
-            if slotted:
-                far = chips // steps
-                behind = slot % far * steps + sign * NEAR[slot // far]
-                source = lax.rem(chip + 2 * chips - behind, chips)
-            block = 2 * source + (core if side == 0 else 1 - core)
-            held = block
-            if hopped:
-                far = count // steps
-                at = lax.rem(own_sign * (place - block) + 2 * count - NEAR[0], count)
-                held = lax.rem(at, steps) * far + lax.rem(own_sign * lax.div(at, steps) + far, far)
-            yield side, slot, block, held
+def weight_slot(block, count, hopped):
+    if not hopped:
+        return block
+    steps, far = len(NEAR), count // len(NEAR)
+    sign = 1 - 2 * lax.axis_index("core")
+    at = lax.rem(sign * (lax.axis_index("sp") - block) + 2 * count - NEAR[0], count)
+    return lax.rem(at, steps) * far + lax.rem(sign * lax.div(at, steps) + far, far)
+
+
+def piece_block(side, slot, chips, slotted):
+    core, source = lax.axis_index("core"), slot
+    core = core if side == 0 else 1 - core
+    if slotted:
+        far = chips // len(NEAR)
+        behind = slot % far * len(NEAR) + (1 - 2 * core) * NEAR[slot // far]
+        source = lax.rem(lax.axis_index("x") + 2 * chips - behind, chips)
+    return 2 * source + core
 
 
 def project_kernel(
@@ -102,16 +101,19 @@
     product = jnp.zeros((2 * channels, tok), jnp.float32)
     squares = jnp.zeros((tok, width), jnp.float32)
     pieces = (mine_ref, theirs_ref)
-    for side, slot, block, held in blocks_of(chips, weight_ref.shape[0], hopped, slotted):
-        wide = pieces[side][slot].astype(jnp.float32)
-        squares += wide * wide
-        scaled = (wide * gain_ref[block]).astype(jnp.bfloat16)
-        product += lax.dot_general(
-            weight_ref[held, : 2 * channels, :],
-            scaled,
-            (((1,), (1,)), ((), ())),
-            preferred_element_type=jnp.float32,
-        )
+    for side in range(2):
+        for slot in range(chips):
+            block = piece_block(side, slot, chips, slotted)
+            held = weight_slot(block, weight_ref.shape[0], hopped)
+            wide = pieces[side][slot].astype(jnp.float32)
+            squares += wide * wide
+            scaled = (wide * gain_ref[block]).astype(jnp.bfloat16)
+            product += lax.dot_general(
+                weight_ref[held, : 2 * channels, :],
+                scaled,
+                (((1,), (1,)), ((), ())),
+                preferred_element_type=jnp.float32,
+            )
     mean = jnp.sum(squares.T, axis=0, keepdims=True) * (1.0 / (2 * chips * width))
     rows = (product * lax.rsqrt(mean + EPS)).astype(jnp.bfloat16)
     value_ref[...] = rows[:channels]
@@ -119,18 +121,18 @@
     tail_ref[...] = rows[:channels, tok - LANES :]
 
 
-def mix_kernel(hopped, mine_ref, theirs_ref, weight_ref, residual_ref, out_ref, *copies_ref):
-    chips, channels, _ = mine_ref.shape
-    first = weight_ref.shape[1] - channels
-    held = {(side, slot): w for side, slot, _, w in blocks_of(chips, weight_ref.shape[0], hopped)}
+def mix_kernel(hopped, branch_ref, weight_ref, residual_ref, out_ref, *copies_ref):
+    blocks, channels, _ = branch_ref.shape
+    count, rows, _ = weight_ref.shape
     mixed = residual_ref[...].astype(jnp.float32)
-    for slot in range(chips):
-        branch = jnp.concatenate([mine_ref[slot], theirs_ref[slot]], axis=0)
-        weight = jnp.concatenate(
-            [weight_ref[held[side, slot], first:, :] for side in range(2)], axis=0
-        )
+    for at in range(0, blocks, 2):
+        pair = (at, at + 1)
+        weight = [weight_ref[weight_slot(b, count, hopped), rows - channels :, :] for b in pair]
         mixed += lax.dot_general(
-            branch, weight, (((0,), (0,)), ((), ())), preferred_element_type=jnp.float32
+            jnp.concatenate([branch_ref[b] for b in pair], axis=0),
+            jnp.concatenate(weight, axis=0),
+            (((0,), (0,)), ((), ())),
+            preferred_element_type=jnp.float32,
         )
     mixed = mixed.astype(jnp.bfloat16)
     out_ref[...] = mixed
@@ -190,14 +192,14 @@
     return kernel_call(kernel, out, mine, theirs, gains, weights)
 
 
-def mix_call(hopped, mine, theirs, weights, residual, copies):
+def mix_call(hopped, branch, weights, residual, copies):
     shape, dtype = residual.shape, jnp.bfloat16
     if copies:
         out = [pltpu.VMEM(shape, dtype), pltpu.VMEM((copies, *shape), dtype)]
     else:
         out = [jax.ShapeDtypeStruct(shape, dtype)]
     kernel = functools.partial(mix_kernel, hopped)
-    return kernel_call(kernel, out, mine, theirs, weights, residual)
+    return kernel_call(kernel, out, branch, weights, residual)
 
 
 def scan_call(layer, value, before, consts, maps, offset, count):
@@ -296,16 +298,13 @@
         before = lax.ppermute(tail, "sp", [(i, i + 1) for i in range(count - 1)])
         cum, state, msg = scan_call(layer, value_rows, before, consts, maps, decay_offset, count)
         msgs = exchange(msg, "sp")
-        sent = close_call(msgs, cum, state, gate_rows, chips)
-        mine = exchange(sent, "x")
+        sent = close_call(msgs, cum, state, gate_rows, chips * cores)
+        branch = exchange(sent, ("x", "core"))
         if more:
             _, shard, hop_one = lax.optimization_barrier((sent, shard, hop_one))
             hop_back = far_hop(shard, "sp", -1)
             hop_two = far_hop(hop_one, "sp")
-        theirs = swap(mine)
-        residual, *copies = mix_call(
-            layer > 0, mine, theirs, weights, residual, chips if more else 0
-        )
+        residual, *copies = mix_call(layer > 0, branch, weights, residual, chips if more else 0)
         if more:
             _, *held = lax.optimization_barrier((copies[0], shard, hop_one, hop_two, hop_back))
             later_weights = near_hops(jnp.stack(held), "sp")

time: 226 us -> 223 us (0.987)
  blocking collectives: 74.9 us -> 64.2 us
  starting transfers between devices: 105 us -> 112 us
    all_to_all x2 -> x3, starting transfers between devices: 47.5 us -> 58.4 us  [exchange(): return lax.all_to_all(copies, axis, split_axis=0, concat_axis=0, tiled=True)]
    all_to_all x4 -> x3, blocking collectives: 74.9 us -> 64.2 us  [exchange(): return lax.all_to_all(copies, axis, split_axis=0, concat_axis=0, tiled=True)]
    ppermute x8 -> x6, starting transfers between devices: 28 us -> 24.2 us  [shift(): lax.ppermute(array, axis, [(i, (i + steps) % count) for i in range(count)])]
    ppermute x8 -> x6, waiting for transfers between devices: 15 us -> 13.4 us  [shift(): lax.ppermute(array, axis, [(i, (i + steps) % count) for i in range(count)])]
    all_to_all x2 -> x3, waiting for transfers between devices: 7.53 us -> 7.11 us  [exchange(): return lax.all_to_all(copies, axis, split_axis=0, concat_axis=0, tiled=True)]
  transfers between devices with their start and end apart: 18 -> 17, of which waited for: 12 -> 11; matrix products, arithmetic and copies ran while one was open for 0% -> 0% of each run, Pallas kernels for 1% -> 1%
where the time goes in v4:
time: 223 us; the launch traced here: 219 us
  starting transfers between devices  112 us (50%)
  blocking collectives  64.2 us (29%)
  waiting for transfers between devices  32.6 us (15%)
  Pallas kernels  8.29 us (4%)
    all_to_all x3, blocking collectives, exchange(): return lax.all_to_all(copies, axis, split_axis=0, concat_axis=0, tiled=True)  64.2 us
    all_to_all x3, starting transfers between devices, exchange(): return lax.all_to_all(copies, axis, split_axis=0, concat_axis=0, tiled=True)  58.4 us
    ppermute x6, starting transfers between devices, shift(): lax.ppermute(array, axis, [(i, (i + steps) % count) for i in range(count)])  24.2 us
    ppermute x6, starting transfers between devices, hop(): return lax.ppermute(held, (axis, 'core'), pairs)  23.3 us
    ppermute x6, waiting for transfers between devices, shift(): lax.ppermute(array, axis, [(i, (i + steps) % count) for i in range(count)])  13.4 us
    ppermute x6, waiting for transfers between devices, hop(): return lax.ppermute(held, (axis, 'core'), pairs)  9.39 us
    all_to_all x3, waiting for transfers between devices, exchange(): return lax.all_to_all(copies, axis, split_axis=0, concat_axis=0, tiled=True)  7.11 us
    pallas_call x10, Pallas kernels, kernel_call(): pl.pallas_call(kernel, out_shape=out_shape, in_specs=vmem(len(operands)),...  6.38 us
  transfers between devices with their start and end apart: 17, of which 11 were waited for; matrix products, arithmetic and copies ran while one was open for 0% of the time, Pallas kernels for 1%

profile of v4, /device:TPU:80, one launch (start us, length us, event | category | flops | bytes accessed | tf_op | source)
XLA Modules:
  0.0 219.2 jit_solution(11041428148747048262)
XLA Ops:
  1.9 43.8 %all-to-all-start = ((bf16[16,192,128]{2,1,0:T(8,128)(2,1)}), bf16[16,192,128]{2,1,0:T(8,128)(2,1)S(1)}, u32[]{:S(2)}, u32[]{:S(2)}) async-start(bf16[16,192,128]{2,1,0:T(8,128)(2,1)} %get-tuple-element.28), calls=%async_computation | async-start | bytes 1572864 | tf_op jit(solution)/shard_map/all_to_all | solution.py:230
  45.8 8.0 %collective-permute-start = (bf16[256,128]{1,0:T(8,128)(2,1)S(1)}, bf16[256,128]{1,0:T(8,128)(2,1)S(1)}, u32[]{:S(2)}, u32[]{:S(2)}) collective-permute-start(bf16[256,128]{1,0:T(8,128)(2,1)S(1)} %copy-done), channel_id=1, source_target_pairs={{0,8},{2,10},{4,12},{6,14},{8,0},{10,2},{12,4},{14,6},{1,9},{3,11}... | collective-permute-start | bytes 196616 | tf_op jit(solution)/shard_map/ppermute | solution.py:235
  53.7 2.8 %collective-permute-done = bf16[256,128]{1,0:T(8,128)(2,1)S(1)} collective-permute-done((bf16[256,128]{1,0:T(8,128)(2,1)S(1)}, bf16[256,128]{1,0:T(8,128)(2,1)S(1)}, u32[]{:S(2)}, u32[]{:S(2)}) %collective-permute-start) | collective-permute-done | bytes 65568 | tf_op jit(solution)/shard_map/ppermute | solution.py:235
  56.5 6.6 %collective-permute-start.1 = (bf16[2,256,128]{2,1,0:T(8,128)(2,1)S(1)}, bf16[2,256,128]{2,1,0:T(8,128)(2,1)S(1)}, u32[]{:S(2)}, u32[]{:S(2)}) collective-permute-start(bf16[2,256,128]{2,1,0:T(8,128)(2,1)S(1)} %pad_maximum_fusion.1), channel_id=1, source_target_pairs={{0,12},{1,5},{2,14},{3,7},{4,0},{5,9},{6,2},{7,11},{8,4},{9,13},{1... | collective-permute-start | bytes 393224 | tf_op jit(solution)/shard_map/ppermute | solution.py:251
  63.1 2.9 %collective-permute-start.2 = (bf16[2,256,128]{2,1,0:T(8,128)(2,1)S(1)}, bf16[2,256,128]{2,1,0:T(8,128)(2,1)S(1)}, u32[]{:S(2)}, u32[]{:S(2)}) collective-permute-start(bf16[2,256,128]{2,1,0:T(8,128)(2,1)S(1)} %pad_maximum_fusion.1), channel_id=1, source_target_pairs={{0,14},{1,3},{2,0},{3,5},{4,2},{5,7},{6,4},{7,9},{8,6},{9,11},{10,... | collective-permute-start | bytes 393224 | tf_op jit(solution)/shard_map/ppermute | solution.py:251
  66.9 3.0 %collective-permute-start.3 = (bf16[2,256,128]{2,1,0:T(8,128)(2,1)S(1)}, bf16[2,256,128]{2,1,0:T(8,128)(2,1)S(1)}, u32[]{:S(2)}, u32[]{:S(2)}) collective-permute-start(bf16[2,256,128]{2,1,0:T(8,128)(2,1)S(1)} %pad_maximum_fusion.1), channel_id=1, source_target_pairs={{0,2},{1,15},{2,4},{3,1},{4,6},{5,3},{6,8},{7,5},{8,10},{9,7},{10,... | collective-permute-start | bytes 393224 | tf_op jit(solution)/shard_map/ppermute | solution.py:251
  70.9 4.0 %collective-permute-done.3 = bf16[2,256,128]{2,1,0:T(8,128)(2,1)S(1)} collective-permute-done((bf16[2,256,128]{2,1,0:T(8,128)(2,1)S(1)}, bf16[2,256,128]{2,1,0:T(8,128)(2,1)S(1)}, u32[]{:S(2)}, u32[]{:S(2)}) %collective-permute-start.3) | collective-permute-done | bytes 131104 | tf_op jit(solution)/shard_map/ppermute | solution.py:251
  75.0 2.0 collective-permute-start.4
  78.8 5.8 %all-to-all-done.weight_ref = bf16[16,192,128]{2,1,0:T(8,128)(2,1)S(1)} async-done(((bf16[16,192,128]{2,1,0:T(8,128)(2,1)}), bf16[16,192,128]{2,1,0:T(8,128)(2,1)S(1)}, u32[]{:S(2)}, u32[]{:S(2)}) %all-to-all-start) | async-done | bytes 786464 | tf_op jit(solution)/shard_map/all_to_all | solution.py:230
  85.2 4.1 %collective-permute-start.5 = (bf16[64,128]{1,0:T(8,128)(2,1)S(1)}, bf16[64,128]{1,0:T(8,128)(2,1)S(1)}, u32[]{:S(2)}, u32[]{:S(2)}) collective-permute-start(bf16[64,128]{1,0:T(8,128)(2,1)S(1)} %get-tuple-element.30), channel_id=1, source_target_pairs={{0,16},{16,32},{32,48},{48,64},{64,80},{80,96},{96,112},{112,128},... | collective-permute-start | bytes 49160 | tf_op jit(solution)/shard_map/ppermute | solution.py:298
  91.7 21.4 %all_to_all.30.msgs_ref = f32[16,1,128]{2,1,0:T(1,128)S(1)} all-to-all(f32[16,1,128]{2,1,0:T(1,128)S(1)} %get-tuple-element.31), channel_id=1, replica_groups=mesh['grp'=2,'sp'=16,'x'=8,'core'=2] {'sp'}, dimensions={0} | all-to-all | bytes 16384 | tf_op jit(solution)/shard_map/all_to_all | solution.py:230
  114.1 7.6 %all-to-all-start.2 = ((bf16[16,64,256]{2,1,0:T(8,128)(2,1)}), bf16[16,64,256]{2,1,0:T(8,128)(2,1)S(1)}, u32[]{:S(2)}, u32[]{:S(2)}) async-start(bf16[16,64,256]{2,1,0:T(8,128)(2,1)} %shard_map.102), calls=%async_computation.2 | async-start | bytes 1048576 | tf_op jit(solution)/shard_map/all_to_all | solution.py:230
  121.7 2.5 %collective-permute-start.7 = (bf16[192,128]{1,0:T(8,128)(2,1)S(1)}, bf16[192,128]{1,0:T(8,128)(2,1)S(1)}, u32[]{:S(2)}, u32[]{:S(2)}) collective-permute-start(bf16[192,128]{1,0:T(8,128)(2,1)S(1)} %get-tuple-element.40), channel_id=1, source_target_pairs={{0,64},{16,80},{32,96},{48,112},{64,128},{80,144},{96,160},{112,17... | collective-permute-start | bytes 147464 | tf_op jit(solution)/shard_map/ppermute | solution.py:235
  124.2 7.7 %collective-permute-done.7 = bf16[192,128]{1,0:T(8,128)(2,1)S(1)} collective-permute-done((bf16[192,128]{1,0:T(8,128)(2,1)S(1)}, bf16[192,128]{1,0:T(8,128)(2,1)S(1)}, u32[]{:S(2)}, u32[]{:S(2)}) %collective-permute-start.7) | collective-permute-done | bytes 49184 | tf_op jit(solution)/shard_map/ppermute | solution.py:235
  131.9 2.2 %collective-permute-start.8 = (bf16[192,128]{1,0:T(8,128)(2,1)S(1)}, bf16[192,128]{1,0:T(8,128)(2,1)S(1)}, u32[]{:S(2)}, u32[]{:S(2)}) collective-permute-start(bf16[192,128]{1,0:T(8,128)(2,1)S(1)} %collective-permute-done.7), channel_id=1, source_target_pairs={{0,64},{16,80},{32,96},{48,112},{64,128},{80,144},{96,160},{112,17... | collective-permute-start | bytes 147464 | tf_op jit(solution)/shard_map/ppermute | solution.py:235
  134.1 7.6 %collective-permute-start.9 = (bf16[192,128]{1,0:T(8,128)(2,1)S(1)}, bf16[192,128]{1,0:T(8,128)(2,1)S(1)}, u32[]{:S(2)}, u32[]{:S(2)}) collective-permute-start(bf16[192,128]{1,0:T(8,128)(2,1)S(1)} %get-tuple-element.40), channel_id=1, source_target_pairs={{0,192},{16,208},{32,224},{48,240},{64,0},{80,16},{96,32},{112,48}... | collective-permute-start | bytes 147464 | tf_op jit(solution)/shard_map/ppermute | solution.py:235
  142.9 6.9 %all-to-all-start.3 = ((bf16[8,256,128]{2,1,0:T(8,128)(2,1)}), bf16[8,256,128]{2,1,0:T(8,128)(2,1)S(1)}, u32[]{:S(2)}, u32[]{:S(2)}) async-start(bf16[8,256,128]{2,1,0:T(8,128)(2,1)} %get-tuple-element.35), calls=%async_computation.3 | async-start | bytes 1048576 | tf_op jit(solution)/shard_map/all_to_all | solution.py:230
  149.8 4.9 %collective-permute-start.10 = (bf16[4,192,128]{2,1,0:T(8,128)(2,1)S(1)}, bf16[4,192,128]{2,1,0:T(8,128)(2,1)S(1)}, u32[]{:S(2)}, u32[]{:S(2)}) collective-permute-start(bf16[4,192,128]{2,1,0:T(8,128)(2,1)S(1)} %pad_maximum_fusion), channel_id=1, source_target_pairs={{0,224},{1,33},{16,240},{17,49},{32,0},{33,65},{48,16},{49,81},{64... | collective-permute-start | bytes 589832 | tf_op jit(solution)/shard_map/ppermute | solution.py:251
  154.7 2.1 collective-permute-start.11
  156.9 3.8 %collective-permute-start.12 = (bf16[4,192,128]{2,1,0:T(8,128)(2,1)S(1)}, bf16[4,192,128]{2,1,0:T(8,128)(2,1)S(1)}, u32[]{:S(2)}, u32[]{:S(2)}) collective-permute-start(bf16[4,192,128]{2,1,0:T(8,128)(2,1)S(1)} %pad_maximum_fusion), channel_id=1, source_target_pairs={{0,16},{1,241},{16,32},{17,1},{32,48},{33,17},{48,64},{49,33},{64,... | collective-permute-start | bytes 589832 | tf_op jit(solution)/shard_map/ppermute | solution.py:251
  160.7 4.4 %collective-permute-done.11 = bf16[4,192,128]{2,1,0:T(8,128)(2,1)S(1)} collective-permute-done((bf16[4,192,128]{2,1,0:T(8,128)(2,1)S(1)}, bf16[4,192,128]{2,1,0:T(8,128)(2,1)S(1)}, u32[]{:S(2)}, u32[]{:S(2)}) %collective-permute-start.11) | collective-permute-done | bytes 196640 | tf_op jit(solution)/shard_map/ppermute | solution.py:251
  166.5 1.9 collective-permute-start.6
  175.2 19.6 %all_to_all.31.msgs_ref = f32[16,1,128]{2,1,0:T(1,128)S(1)} all-to-all(f32[16,1,128]{2,1,0:T(1,128)S(1)} %get-tuple-element.46), channel_id=1, replica_groups=mesh['grp'=2,'sp'=16,'x'=8,'core'=2] {'sp'}, dimensions={0} | all-to-all | bytes 16384 | tf_op jit(solution)/shard_map/all_to_all | solution.py:230
  195.1 23.2 %all_to_all.32.branch_ref = bf16[16,64,256]{2,1,0:T(8,128)(2,1)S(1)} all-to-all(bf16[16,64,256]{2,1,0:T(8,128)(2,1)S(1)} %shard_map.108), channel_id=1, replica_groups=mesh['grp'=2,'sp'=16,'x'=8,'core'=2] {'x','core'}, dimensions={0} | all-to-all | bytes 1048576 | tf_op jit(solution)/shard_map/all_to_all | solution.py:230
  (61 shorter events, 20.1 us)
Async XLA Ops:
  1.9 43.8 %copy-start = (bf16[256,128]{1,0:T(8,128)(2,1)S(1)}, bf16[256,128]{1,0:T(8,128)(2,1)}, u32[]{:S(2)}) copy-start(bf16[256,128]{1,0:T(8,128)(2,1)} %residual_ref.1) | copy-start | bytes 196612
  1.9 82.7 %all-to-all-start = ((bf16[16,192,128]{2,1,0:T(8,128)(2,1)}), bf16[16,192,128]{2,1,0:T(8,128)(2,1)S(1)}, u32[]{:S(2)}, u32[]{:S(2)}) async-start(bf16[16,192,128]{2,1,0:T(8,128)(2,1)} %get-tuple-element.28), calls=%async_computation | async-start | bytes 1572864 | tf_op jit(solution)/shard_map/all_to_all | solution.py:230
  45.8 10.7 %collective-permute-start = (bf16[256,128]{1,0:T(8,128)(2,1)S(1)}, bf16[256,128]{1,0:T(8,128)(2,1)S(1)}, u32[]{:S(2)}, u32[]{:S(2)}) collective-permute-start(bf16[256,128]{1,0:T(8,128)(2,1)S(1)} %copy-done), channel_id=1, source_target_pairs={{0,8},{2,10},{4,12},{6,14},{8,0},{10,2},{12,4},{14,6},{1,9},{3,11}... | collective-permute-start | bytes 196616 | tf_op jit(solution)/shard_map/ppermute | solution.py:235
  56.5 9.5 %copy-start.5 = (f32[2,4,64]{2,1,0:T(4,128)S(1)}, f32[2,4,64]{2,1,0:T(4,128)}, u32[]{:S(2)}) copy-start(f32[2,4,64]{2,1,0:T(4,128)} %param.14) | copy-start | bytes 6148
  56.5 9.5 %copy-start.2 = (bf16[2,1,64,64]{3,2,1,0:T(8,128)(2,1)S(1)}, bf16[2,1,64,64]{3,2,1,0:T(8,128)(2,1)}, u32[]{:S(2)}) copy-start(bf16[2,1,64,64]{3,2,1,0:T(8,128)(2,1)} %param.15) | copy-start | bytes 49156
  56.5 13.4 %collective-permute-start.1 = (bf16[2,256,128]{2,1,0:T(8,128)(2,1)S(1)}, bf16[2,256,128]{2,1,0:T(8,128)(2,1)S(1)}, u32[]{:S(2)}, u32[]{:S(2)}) collective-permute-start(bf16[2,256,128]{2,1,0:T(8,128)(2,1)S(1)} %pad_maximum_fusion.1), channel_id=1, source_target_pairs={{0,12},{1,5},{2,14},{3,7},{4,0},{5,9},{6,2},{7,11},{8,4},{9,13},{1... | collective-permute-start | bytes 393224 | tf_op jit(solution)/shard_map/ppermute | solution.py:251
  63.1 7.8 %collective-permute-start.2 = (bf16[2,256,128]{2,1,0:T(8,128)(2,1)S(1)}, bf16[2,256,128]{2,1,0:T(8,128)(2,1)S(1)}, u32[]{:S(2)}, u32[]{:S(2)}) collective-permute-start(bf16[2,256,128]{2,1,0:T(8,128)(2,1)S(1)} %pad_maximum_fusion.1), channel_id=1, source_target_pairs={{0,14},{1,3},{2,0},{3,5},{4,2},{5,7},{6,4},{7,9},{8,6},{9,11},{10,... | collective-permute-start | bytes 393224 | tf_op jit(solution)/shard_map/ppermute | solution.py:251
  66.0 0.8 copy-start.3
  66.9 8.1 %collective-permute-start.3 = (bf16[2,256,128]{2,1,0:T(8,128)(2,1)S(1)}, bf16[2,256,128]{2,1,0:T(8,128)(2,1)S(1)}, u32[]{:S(2)}, u32[]{:S(2)}) collective-permute-start(bf16[2,256,128]{2,1,0:T(8,128)(2,1)S(1)} %pad_maximum_fusion.1), channel_id=1, source_target_pairs={{0,2},{1,15},{2,4},{3,1},{4,6},{5,3},{6,8},{7,5},{8,10},{9,7},{10,... | collective-permute-start | bytes 393224 | tf_op jit(solution)/shard_map/ppermute | solution.py:251
  75.0 3.8 %collective-permute-start.4 = (bf16[8,256,128]{2,1,0:T(8,128)(2,1)S(1)}, bf16[8,256,128]{2,1,0:T(8,128)(2,1)S(1)}, u32[]{:S(2)}, u32[]{:S(2)}) collective-permute-start(bf16[8,256,128]{2,1,0:T(8,128)(2,1)S(1)} %constant_dynamic-update-slice_fusion.mine_ref), channel_id=1, source_target_pairs={{0,1},{1,0},{2,3},{3,2},{4,5},{5,4},{6,7},{7,6},{8,9},{9,8},{10,11... | collective-permute-start | bytes 1572872 | tf_op jit(solution)/shard_map/ppermute | solution.py:235
  77.0 0.7 copy-start.6
  77.0 0.7 copy-start.4
  85.2 5.6 %copy-start.1 = (f32[2,64,256]{2,1,0:T(8,128)S(1)}, f32[2,64,256]{2,1,0:T(8,128)}, u32[]{:S(2)}) copy-start(f32[2,64,256]{2,1,0:T(8,128)} %offset_ref.3) | copy-start | bytes 393220
  85.2 5.5 %collective-permute-start.5 = (bf16[64,128]{1,0:T(8,128)(2,1)S(1)}, bf16[64,128]{1,0:T(8,128)(2,1)S(1)}, u32[]{:S(2)}, u32[]{:S(2)}) collective-permute-start(bf16[64,128]{1,0:T(8,128)(2,1)S(1)} %get-tuple-element.30), channel_id=1, source_target_pairs={{0,16},{16,32},{32,48},{48,64},{64,80},{80,96},{96,112},{112,128},... | collective-permute-start | bytes 49160 | tf_op jit(solution)/shard_map/ppermute | solution.py:298
  114.1 27.6 %all-to-all-start.2 = ((bf16[16,64,256]{2,1,0:T(8,128)(2,1)}), bf16[16,64,256]{2,1,0:T(8,128)(2,1)S(1)}, u32[]{:S(2)}, u32[]{:S(2)}) async-start(bf16[16,64,256]{2,1,0:T(8,128)(2,1)} %shard_map.102), calls=%async_computation.2 | async-start | bytes 1048576 | tf_op jit(solution)/shard_map/all_to_all | solution.py:230
  121.7 10.2 %collective-permute-start.7 = (bf16[192,128]{1,0:T(8,128)(2,1)S(1)}, bf16[192,128]{1,0:T(8,128)(2,1)S(1)}, u32[]{:S(2)}, u32[]{:S(2)}) collective-permute-start(bf16[192,128]{1,0:T(8,128)(2,1)S(1)} %get-tuple-element.40), channel_id=1, source_target_pairs={{0,64},{16,80},{32,96},{48,112},{64,128},{80,144},{96,160},{112,17... | collective-permute-start | bytes 147464 | tf_op jit(solution)/shard_map/ppermute | solution.py:235
  131.9 17.9 %collective-permute-start.8 = (bf16[192,128]{1,0:T(8,128)(2,1)S(1)}, bf16[192,128]{1,0:T(8,128)(2,1)S(1)}, u32[]{:S(2)}, u32[]{:S(2)}) collective-permute-start(bf16[192,128]{1,0:T(8,128)(2,1)S(1)} %collective-permute-done.7), channel_id=1, source_target_pairs={{0,64},{16,80},{32,96},{48,112},{64,128},{80,144},{96,160},{112,17... | collective-permute-start | bytes 147464 | tf_op jit(solution)/shard_map/ppermute | solution.py:235
  134.1 15.7 %collective-permute-start.9 = (bf16[192,128]{1,0:T(8,128)(2,1)S(1)}, bf16[192,128]{1,0:T(8,128)(2,1)S(1)}, u32[]{:S(2)}, u32[]{:S(2)}) collective-permute-start(bf16[192,128]{1,0:T(8,128)(2,1)S(1)} %get-tuple-element.40), channel_id=1, source_target_pairs={{0,192},{16,208},{32,224},{48,240},{64,0},{80,16},{96,32},{112,48}... | collective-permute-start | bytes 147464 | tf_op jit(solution)/shard_map/ppermute | solution.py:235
  142.9 23.6 %all-to-all-start.3 = ((bf16[8,256,128]{2,1,0:T(8,128)(2,1)}), bf16[8,256,128]{2,1,0:T(8,128)(2,1)S(1)}, u32[]{:S(2)}, u32[]{:S(2)}) async-start(bf16[8,256,128]{2,1,0:T(8,128)(2,1)} %get-tuple-element.35), calls=%async_computation.3 | async-start | bytes 1048576 | tf_op jit(solution)/shard_map/all_to_all | solution.py:230
  149.8 10.8 %collective-permute-start.10 = (bf16[4,192,128]{2,1,0:T(8,128)(2,1)S(1)}, bf16[4,192,128]{2,1,0:T(8,128)(2,1)S(1)}, u32[]{:S(2)}, u32[]{:S(2)}) collective-permute-start(bf16[4,192,128]{2,1,0:T(8,128)(2,1)S(1)} %pad_maximum_fusion), channel_id=1, source_target_pairs={{0,224},{1,33},{16,240},{17,49},{32,0},{33,65},{48,16},{49,81},{64... | collective-permute-start | bytes 589832 | tf_op jit(solution)/shard_map/ppermute | solution.py:251
  154.7 10.4 %collective-permute-start.11 = (bf16[4,192,128]{2,1,0:T(8,128)(2,1)S(1)}, bf16[4,192,128]{2,1,0:T(8,128)(2,1)S(1)}, u32[]{:S(2)}, u32[]{:S(2)}) collective-permute-start(bf16[4,192,128]{2,1,0:T(8,128)(2,1)S(1)} %pad_maximum_fusion), channel_id=1, source_target_pairs={{0,240},{1,17},{16,0},{17,33},{32,16},{33,49},{48,32},{49,65},{64,... | collective-permute-start | bytes 589832 | tf_op jit(solution)/shard_map/ppermute | solution.py:251
  156.9 11.6 %collective-permute-start.12 = (bf16[4,192,128]{2,1,0:T(8,128)(2,1)S(1)}, bf16[4,192,128]{2,1,0:T(8,128)(2,1)S(1)}, u32[]{:S(2)}, u32[]{:S(2)}) collective-permute-start(bf16[4,192,128]{2,1,0:T(8,128)(2,1)S(1)} %pad_maximum_fusion), channel_id=1, source_target_pairs={{0,16},{1,241},{16,32},{17,1},{32,48},{33,17},{48,64},{49,33},{64,... | collective-permute-start | bytes 589832 | tf_op jit(solution)/shard_map/ppermute | solution.py:251
  166.5 3.8 %collective-permute-start.6 = (bf16[8,256,128]{2,1,0:T(8,128)(2,1)S(1)}, bf16[8,256,128]{2,1,0:T(8,128)(2,1)S(1)}, u32[]{:S(2)}, u32[]{:S(2)}) collective-permute-start(bf16[8,256,128]{2,1,0:T(8,128)(2,1)S(1)} %all-to-all-done.3.mine_ref), channel_id=1, source_target_pairs={{0,1},{1,0},{2,3},{3,2},{4,5},{5,4},{6,7},{7,6},{8,9},{9,8},{10,11... | collective-permute-start | bytes 1572872 | tf_op jit(solution)/shard_map/ppermute | solution.py:235
  170.8 3.4 %collective-permute-start.13 = (bf16[64,128]{1,0:T(8,128)(2,1)S(1)}, bf16[64,128]{1,0:T(8,128)(2,1)S(1)}, u32[]{:S(2)}, u32[]{:S(2)}) collective-permute-start(bf16[64,128]{1,0:T(8,128)(2,1)S(1)} %get-tuple-element.45), channel_id=1, source_target_pairs={{0,16},{16,32},{32,48},{48,64},{64,80},{80,96},{96,112},{112,128},... | collective-permute-start | bytes 49160 | tf_op jit(solution)/shard_map/ppermute | solution.py:298

commit v5 on v4

--- a/solution.py
+++ b/solution.py
@@ -121,18 +121,16 @@
     tail_ref[...] = rows[:channels, tok - LANES :]
 
 
-def mix_kernel(hopped, branch_ref, weight_ref, residual_ref, out_ref, *copies_ref):
-    blocks, channels, _ = branch_ref.shape
+def mix_kernel(mine_ref, theirs_ref, weight_ref, residual_ref, out_ref, *copies_ref):
+    chips, channels, _ = mine_ref.shape
     count, rows, _ = weight_ref.shape
     mixed = residual_ref[...].astype(jnp.float32)
-    for at in range(0, blocks, 2):
-        pair = (at, at + 1)
-        weight = [weight_ref[weight_slot(b, count, hopped), rows - channels :, :] for b in pair]
+    for slot in range(chips):
+        held = [weight_slot(piece_block(side, slot, chips, False), count, True) for side in range(2)]
+        branch = jnp.concatenate([mine_ref[slot], theirs_ref[slot]], axis=0)
+        weight = jnp.concatenate([weight_ref[at, rows - channels :, :] for at in held], axis=0)
         mixed += lax.dot_general(
-            jnp.concatenate([branch_ref[b] for b in pair], axis=0),
-            jnp.concatenate(weight, axis=0),
-            (((0,), (0,)), ((), ())),
-            preferred_element_type=jnp.float32,
+            branch, weight, (((0,), (0,)), ((), ())), preferred_element_type=jnp.float32
         )
     mixed = mixed.astype(jnp.bfloat16)
     out_ref[...] = mixed
@@ -140,16 +138,14 @@
         ref[...] = jnp.broadcast_to(mixed[None], ref.shape)
 
 
-def pack_kernel(value_ref, gate_ref, mix_ref, first_ref, *rest_refs):
-    *later_refs, sems = rest_refs
-    channels = value_ref.shape[1]
+def pack_kernel(value_ref, gate_ref, mix_ref, first_ref, later_ref, sems):
+    layers, channels, _ = value_ref.shape
+    shards = [ref.at[layer] for layer in range(layers) for ref in (value_ref, gate_ref, mix_ref)]
     moves = []
-    for layer, rows_ref in enumerate((first_ref.at[0], *later_refs)):
-        for k, shard_ref in enumerate((value_ref, gate_ref, mix_ref)):
-            target = rows_ref.at[pl.ds(k * channels, channels)]
-            moves.append(
-                pltpu.make_async_copy(shard_ref.at[layer], target, sems.at[len(moves)])
-            )
+    for k, shard_ref in enumerate(shards):
+        rows_ref, at = (first_ref.at[0], k) if k < 2 else (later_ref, k - 2)
+        target = rows_ref.at[pl.ds(at * channels, channels)]
+        moves.append(pltpu.make_async_copy(shard_ref, target, sems.at[k]))
     for move in moves:
         move.start()
     for move in moves:
@@ -171,9 +167,11 @@
 
 def pack_call(value_proj, gate_proj, mix_proj, count):
     layers, channels, width = value_proj.shape
-    rows = (3 * channels, width)
-    out = [pltpu.VMEM((count, *rows), value_proj.dtype)]
-    out += [pltpu.VMEM(rows, value_proj.dtype)] * (layers - 1)
+    dtype = value_proj.dtype
+    out = [
+        pltpu.VMEM((count, 2 * channels, width), dtype),
+        pltpu.VMEM(((3 * layers - 2) * channels, width), dtype),
+    ]
     return pl.pallas_call(
         pack_kernel,
         out_shape=out,
@@ -184,22 +182,20 @@
     )(value_proj, gate_proj, mix_proj)
 
 
-def project_call(slotted, hopped, mine, theirs, gains, weights):
+def project_call(slotted, hopped, mine, theirs, gains, weights, channels):
     _, tok, _ = mine.shape
-    channels = weights.shape[1] // 3
     out = [pltpu.VMEM((channels, n), jnp.bfloat16) for n in (tok, tok, LANES)]
     kernel = functools.partial(project_kernel, slotted, hopped)
     return kernel_call(kernel, out, mine, theirs, gains, weights)
 
 
-def mix_call(hopped, branch, weights, residual, copies):
+def mix_call(mine, theirs, weights, residual, copies):
     shape, dtype = residual.shape, jnp.bfloat16
     if copies:
         out = [pltpu.VMEM(shape, dtype), pltpu.VMEM((copies, *shape), dtype)]
     else:
         out = [jax.ShapeDtypeStruct(shape, dtype)]
-    kernel = functools.partial(mix_kernel, hopped)
-    return kernel_call(kernel, out, branch, weights, residual)
+    return kernel_call(mix_kernel, out, mine, theirs, weights, residual)
 
 
 def scan_call(layer, value, before, consts, maps, offset, count):
@@ -265,7 +261,7 @@
     decay_offset,
     mix_proj,
 ):
-    own_cols = tokens.shape[1]
+    own_cols, channels = tokens.shape[1], value_proj.shape[1]
     chips, cores, count = (lax.axis_size(name) for name in ("x", "core", "sp"))
 
     def swap(array):
@@ -274,14 +270,14 @@
     first, shard = pack_call(value_proj, gate_proj, mix_proj, count)
     weights = exchange(first, "sp")
     held = jnp.stack([tokens, far_hop(tokens, "x")])
+    hop_one = far_hop(shard, "sp", -1)
     mine = near_hops(held, "x")
-    _, shard = lax.optimization_barrier((mine, shard))
-    hop_one = far_hop(shard, "sp")
     rates = -RATE_SCALE * jax.nn.softplus(-decay_param)
     consts = jnp.concatenate([conv_taps.transpose(0, 2, 1), rates[:, :, None]], axis=2)
     consts = jnp.pad(consts, ((0, 0), (0, 0), (0, LANES - consts.shape[2])))
     maps = jnp.concatenate([recur_map[:, 0], input_map[:, 0]], axis=2).transpose(0, 2, 1)
     gains = [gain.reshape(chips * cores, 1, own_cols) for gain in norm_gain]
+    gains[1] = copy_call(gains[1])
     gains[1] = copy_call(gains[1])
     gains[1] = copy_call(gains[1])
 
@@ -293,21 +289,28 @@
             weights = later_weights
         theirs = swap(mine)
         value_rows, gate_rows, tail = project_call(
-            layer == 0, layer > 0, mine, theirs, gains[layer], weights
+            layer == 0, layer > 0, mine, theirs, gains[layer], weights, channels
         )
         before = lax.ppermute(tail, "sp", [(i, i + 1) for i in range(count - 1)])
         cum, state, msg = scan_call(layer, value_rows, before, consts, maps, decay_offset, count)
         msgs = exchange(msg, "sp")
-        sent = close_call(msgs, cum, state, gate_rows, chips * cores)
-        branch = exchange(sent, ("x", "core"))
         if more:
-            _, shard, hop_one = lax.optimization_barrier((sent, shard, hop_one))
-            hop_back = far_hop(shard, "sp", -1)
-            hop_two = far_hop(hop_one, "sp")
-        residual, *copies = mix_call(layer > 0, branch, weights, residual, chips if more else 0)
+            _, shard, hop_one = lax.optimization_barrier((msg, shard, hop_one))
+            hop_back = far_hop(shard, "sp")
+            hop_two = far_hop(hop_one, "sp", -1)
+        sent = close_call(msgs, cum, state, gate_rows, chips)
+        mine = exchange(sent, "x")
         if more:
-            _, *held = lax.optimization_barrier((copies[0], shard, hop_one, hop_two, hop_back))
-            later_weights = near_hops(jnp.stack(held), "sp")
+            held = (shard, hop_back, hop_two, hop_one)
+            _, *held = lax.optimization_barrier((sent, *held))
+            mix_weights = near_hops(jnp.stack([h[:channels] for h in held]), "sp")
+        else:
+            mix_weights = weights
+        theirs = swap(mine)
+        residual, *copies = mix_call(mine, theirs, mix_weights, residual, chips if more else 0)
+        if more:
+            _, *held = lax.optimization_barrier((copies[0], *held))
+            later_weights = near_hops(jnp.stack([h[channels:] for h in held]), "sp")
     return residual
 
 

time: 223 us -> 219 us (0.982)
  starting transfers between devices: 112 us -> 123 us
  blocking collectives: 64.2 us -> 54.1 us
  waiting for transfers between devices: 32.6 us -> 28 us
    ppermute x6 -> x8, starting transfers between devices: 24.2 us -> 35.2 us  [shift(): lax.ppermute(array, axis, [(i, (i + steps) % count) for i in range(count)])]
    all_to_all x3, blocking collectives: 64.2 us -> 54.1 us  [exchange(): return lax.all_to_all(copies, axis, split_axis=0, concat_axis=0, tiled=True)]
    ppermute x6 -> x9, starting transfers between devices: 23.3 us -> 31 us  [hop(): return lax.ppermute(held, (axis, 'core'), pairs)]
    all_to_all x3, starting transfers between devices: 58.4 us -> 51.1 us  [exchange(): return lax.all_to_all(copies, axis, split_axis=0, concat_axis=0, tiled=True)]
    ppermute x6 -> x8, waiting for transfers between devices: 13.4 us -> 8.66 us  [shift(): lax.ppermute(array, axis, [(i, (i + steps) % count) for i in range(count)])]
    ppermute x6 -> x9, waiting for transfers between devices: 9.39 us -> 9.27 us  [hop(): return lax.ppermute(held, (axis, 'core'), pairs)]
    pallas_call x10 -> x11, Pallas kernels: 6.38 us -> 6.28 us  [kernel_call(): pl.pallas_call(kernel, out_shape=out_shape, in_specs=vmem(len(operands)),...]
  transfers between devices with their start and end apart: 17 -> 22, of which waited for: 11 -> 13; matrix products, arithmetic and copies ran while one was open for 0% -> 0% of each run, Pallas kernels for 1% -> 1%
where the time goes in v5:
time: 219 us; the launch traced here: 216 us
  starting transfers between devices  123 us (56%)
  blocking collectives  54.1 us (25%)
  waiting for transfers between devices  28 us (13%)
  Pallas kernels  8.03 us (4%)
    all_to_all x3, blocking collectives, exchange(): return lax.all_to_all(copies, axis, split_axis=0, concat_axis=0, tiled=True)  54.1 us
    all_to_all x3, starting transfers between devices, exchange(): return lax.all_to_all(copies, axis, split_axis=0, concat_axis=0, tiled=True)  51.1 us
    ppermute x8, starting transfers between devices, shift(): lax.ppermute(array, axis, [(i, (i + steps) % count) for i in range(count)])  35.2 us
    ppermute x9, starting transfers between devices, hop(): return lax.ppermute(held, (axis, 'core'), pairs)  31 us
    ppermute x9, waiting for transfers between devices, hop(): return lax.ppermute(held, (axis, 'core'), pairs)  9.27 us
    ppermute x8, waiting for transfers between devices, shift(): lax.ppermute(array, axis, [(i, (i + steps) % count) for i in range(count)])  8.66 us
    all_to_all x3, waiting for transfers between devices, exchange(): return lax.all_to_all(copies, axis, split_axis=0, concat_axis=0, tiled=True)  7.38 us
    pallas_call x11, Pallas kernels, kernel_call(): pl.pallas_call(kernel, out_shape=out_shape, in_specs=vmem(len(operands)),...  6.28 us
  transfers between devices with their start and end apart: 22, of which 13 were waited for; matrix products, arithmetic and copies ran while one was open for 0% of the time, Pallas kernels for 1%

profile of v5, /device:TPU:80, one launch (start us, length us, event | category | flops | bytes accessed | tf_op | source)
XLA Modules:
  0.0 216.2 jit_solution(4648555461400862468)
XLA Ops:
  1.8 43.8 %all-to-all-start = ((bf16[16,128,128]{2,1,0:T(8,128)(2,1)}), bf16[16,128,128]{2,1,0:T(8,128)(2,1)S(1)}, u32[]{:S(2)}, u32[]{:S(2)}) async-start(bf16[16,128,128]{2,1,0:T(8,128)(2,1)} %get-tuple-element.31), calls=%async_computation | async-start | bytes 1048576 | tf_op jit(solution)/shard_map/all_to_all | solution.py:226
  45.6 8.0 %collective-permute-start = (bf16[256,128]{1,0:T(8,128)(2,1)S(1)}, bf16[256,128]{1,0:T(8,128)(2,1)S(1)}, u32[]{:S(2)}, u32[]{:S(2)}) collective-permute-start(bf16[256,128]{1,0:T(8,128)(2,1)S(1)} %copy-done), channel_id=1, source_target_pairs={{0,8},{2,10},{4,12},{6,14},{8,0},{10,2},{12,4},{14,6},{1,9},{3,11}... | collective-permute-start | bytes 196616 | tf_op jit(solution)/shard_map/ppermute | solution.py:231
  53.6 2.8 %collective-permute-done = bf16[256,128]{1,0:T(8,128)(2,1)S(1)} collective-permute-done((bf16[256,128]{1,0:T(8,128)(2,1)S(1)}, bf16[256,128]{1,0:T(8,128)(2,1)S(1)}, u32[]{:S(2)}, u32[]{:S(2)}) %collective-permute-start) | collective-permute-done | bytes 65568 | tf_op jit(solution)/shard_map/ppermute | solution.py:231
  56.4 6.6 %collective-permute-start.1 = (bf16[2,256,128]{2,1,0:T(8,128)(2,1)S(1)}, bf16[2,256,128]{2,1,0:T(8,128)(2,1)S(1)}, u32[]{:S(2)}, u32[]{:S(2)}) collective-permute-start(bf16[2,256,128]{2,1,0:T(8,128)(2,1)S(1)} %pad_maximum_fusion.1), channel_id=1, source_target_pairs={{0,12},{1,5},{2,14},{3,7},{4,0},{5,9},{6,2},{7,11},{8,4},{9,13},{1... | collective-permute-start | bytes 393224 | tf_op jit(solution)/shard_map/ppermute | solution.py:247
  62.9 2.9 %collective-permute-start.2 = (bf16[2,256,128]{2,1,0:T(8,128)(2,1)S(1)}, bf16[2,256,128]{2,1,0:T(8,128)(2,1)S(1)}, u32[]{:S(2)}, u32[]{:S(2)}) collective-permute-start(bf16[2,256,128]{2,1,0:T(8,128)(2,1)S(1)} %pad_maximum_fusion.1), channel_id=1, source_target_pairs={{0,14},{1,3},{2,0},{3,5},{4,2},{5,7},{6,4},{7,9},{8,6},{9,11},{10,... | collective-permute-start | bytes 393224 | tf_op jit(solution)/shard_map/ppermute | solution.py:247
  65.8 7.3 %collective-permute-start.7 = (bf16[256,128]{1,0:T(8,128)(2,1)S(1)}, bf16[256,128]{1,0:T(8,128)(2,1)S(1)}, u32[]{:S(2)}, u32[]{:S(2)}) collective-permute-start(bf16[256,128]{1,0:T(8,128)(2,1)S(1)} %get-tuple-element.46), channel_id=1, source_target_pairs={{0,192},{16,208},{32,224},{48,240},{64,0},{80,16},{96,32},{112,48}... | collective-permute-start | bytes 196616 | tf_op jit(solution)/shard_map/ppermute | solution.py:231
  74.0 3.2 %collective-permute-start.3 = (bf16[2,256,128]{2,1,0:T(8,128)(2,1)S(1)}, bf16[2,256,128]{2,1,0:T(8,128)(2,1)S(1)}, u32[]{:S(2)}, u32[]{:S(2)}) collective-permute-start(bf16[2,256,128]{2,1,0:T(8,128)(2,1)S(1)} %pad_maximum_fusion.1), channel_id=1, source_target_pairs={{0,2},{1,15},{2,4},{3,1},{4,6},{5,3},{6,8},{7,5},{8,10},{9,7},{10,... | collective-permute-start | bytes 393224 | tf_op jit(solution)/shard_map/ppermute | solution.py:247
  77.3 4.8 %collective-permute-done.3 = bf16[2,256,128]{2,1,0:T(8,128)(2,1)S(1)} collective-permute-done((bf16[2,256,128]{2,1,0:T(8,128)(2,1)S(1)}, bf16[2,256,128]{2,1,0:T(8,128)(2,1)S(1)}, u32[]{:S(2)}, u32[]{:S(2)}) %collective-permute-start.3) | collective-permute-done | bytes 131104 | tf_op jit(solution)/shard_map/ppermute | solution.py:247
  86.5 2.6 %collective-permute-start.5 = (bf16[64,128]{1,0:T(8,128)(2,1)S(1)}, bf16[64,128]{1,0:T(8,128)(2,1)S(1)}, u32[]{:S(2)}, u32[]{:S(2)}) collective-permute-start(bf16[64,128]{1,0:T(8,128)(2,1)S(1)} %get-tuple-element.33), channel_id=1, source_target_pairs={{0,16},{16,32},{32,48},{48,64},{64,80},{80,96},{96,112},{112,128},... | collective-permute-start | bytes 49160 | tf_op jit(solution)/shard_map/ppermute | solution.py:294
  91.6 5.5 %collective-permute-start.8 = (bf16[256,128]{1,0:T(8,128)(2,1)S(1)}, bf16[256,128]{1,0:T(8,128)(2,1)S(1)}, u32[]{:S(2)}, u32[]{:S(2)}) collective-permute-start(bf16[256,128]{1,0:T(8,128)(2,1)S(1)} %get-tuple-element.46), channel_id=1, source_target_pairs={{0,64},{16,80},{32,96},{48,112},{64,128},{80,144},{96,160},{112,17... | collective-permute-start | bytes 196616 | tf_op jit(solution)/shard_map/ppermute | solution.py:231
  97.1 6.7 %collective-permute-start.9 = (bf16[256,128]{1,0:T(8,128)(2,1)S(1)}, bf16[256,128]{1,0:T(8,128)(2,1)S(1)}, u32[]{:S(2)}, u32[]{:S(2)}) collective-permute-start(bf16[256,128]{1,0:T(8,128)(2,1)S(1)} %collective-permute-done.7), channel_id=1, source_target_pairs={{0,192},{16,208},{32,224},{48,240},{64,0},{80,16},{96,32},{112,48}... | collective-permute-start | bytes 196616 | tf_op jit(solution)/shard_map/ppermute | solution.py:231
  103.8 19.6 %all_to_all.30.msgs_ref = f32[16,1,128]{2,1,0:T(1,128)S(1)} all-to-all(f32[16,1,128]{2,1,0:T(1,128)S(1)} %get-tuple-element.34), channel_id=1, replica_groups=mesh['grp'=2,'sp'=16,'x'=8,'core'=2] {'sp'}, dimensions={0} | all-to-all | bytes 16384 | tf_op jit(solution)/shard_map/all_to_all | solution.py:226
  126.9 3.6 %all-to-all-start.2 = ((bf16[8,64,256]{2,1,0:T(8,128)(2,1)}), bf16[8,64,256]{2,1,0:T(8,128)(2,1)S(1)}, u32[]{:S(2)}, u32[]{:S(2)}) async-start(bf16[8,64,256]{2,1,0:T(8,128)(2,1)} %shard_map.102), calls=%async_computation.2 | async-start | bytes 524288 | tf_op jit(solution)/shard_map/all_to_all | solution.py:226
  130.5 2.6 %collective-permute-start.11 = (bf16[4,64,128]{2,1,0:T(8,128)(2,1)S(1)}, bf16[4,64,128]{2,1,0:T(8,128)(2,1)S(1)}, u32[]{:S(2)}, u32[]{:S(2)}) collective-permute-start(bf16[4,64,128]{2,1,0:T(8,128)(2,1)S(1)} %pad_maximum_fusion.2), channel_id=1, source_target_pairs={{0,240},{1,17},{16,0},{17,33},{32,16},{33,49},{48,32},{49,65},{64,... | collective-permute-start | bytes 196616 | tf_op jit(solution)/shard_map/ppermute | solution.py:247
  133.1 3.3 %collective-permute-start.12 = (bf16[4,64,128]{2,1,0:T(8,128)(2,1)S(1)}, bf16[4,64,128]{2,1,0:T(8,128)(2,1)S(1)}, u32[]{:S(2)}, u32[]{:S(2)}) collective-permute-start(bf16[4,64,128]{2,1,0:T(8,128)(2,1)S(1)} %pad_maximum_fusion.2), channel_id=1, source_target_pairs={{0,16},{1,241},{16,32},{17,1},{32,48},{33,17},{48,64},{49,33},{64,... | collective-permute-start | bytes 196616 | tf_op jit(solution)/shard_map/ppermute | solution.py:247
  136.7 4.0 %all-to-all-done.2.mine_ref = bf16[8,64,256]{2,1,0:T(8,128)(2,1)S(1)} async-done(((bf16[8,64,256]{2,1,0:T(8,128)(2,1)}), bf16[8,64,256]{2,1,0:T(8,128)(2,1)S(1)}, u32[]{:S(2)}, u32[]{:S(2)}) %all-to-all-start.2) | async-done | bytes 262176 | tf_op jit(solution)/shard_map/all_to_all | solution.py:226
  145.3 3.7 %all-to-all-start.3 = ((bf16[8,256,128]{2,1,0:T(8,128)(2,1)}), bf16[8,256,128]{2,1,0:T(8,128)(2,1)S(1)}, u32[]{:S(2)}, u32[]{:S(2)}) async-start(bf16[8,256,128]{2,1,0:T(8,128)(2,1)} %get-tuple-element.45), calls=%async_computation.3 | async-start | bytes 1048576 | tf_op jit(solution)/shard_map/all_to_all | solution.py:226
  149.1 4.1 %collective-permute-start.14 = (bf16[4,192,128]{2,1,0:T(8,128)(2,1)S(1)}, bf16[4,192,128]{2,1,0:T(8,128)(2,1)S(1)}, u32[]{:S(2)}, u32[]{:S(2)}) collective-permute-start(bf16[4,192,128]{2,1,0:T(8,128)(2,1)S(1)} %pad_maximum_fusion), channel_id=1, source_target_pairs={{0,224},{1,33},{16,240},{17,49},{32,0},{33,65},{48,16},{49,81},{64... | collective-permute-start | bytes 589832 | tf_op jit(solution)/shard_map/ppermute | solution.py:247
  155.2 4.0 %collective-permute-start.16 = (bf16[4,192,128]{2,1,0:T(8,128)(2,1)S(1)}, bf16[4,192,128]{2,1,0:T(8,128)(2,1)S(1)}, u32[]{:S(2)}, u32[]{:S(2)}) collective-permute-start(bf16[4,192,128]{2,1,0:T(8,128)(2,1)S(1)} %pad_maximum_fusion), channel_id=1, source_target_pairs={{0,16},{1,241},{16,32},{17,1},{32,48},{33,17},{48,64},{49,33},{64,... | collective-permute-start | bytes 589832 | tf_op jit(solution)/shard_map/ppermute | solution.py:247
  159.8 3.5 %collective-permute-done.15 = bf16[4,192,128]{2,1,0:T(8,128)(2,1)S(1)} collective-permute-done((bf16[4,192,128]{2,1,0:T(8,128)(2,1)S(1)}, bf16[4,192,128]{2,1,0:T(8,128)(2,1)S(1)}, u32[]{:S(2)}, u32[]{:S(2)}) %collective-permute-start.15) | collective-permute-done | bytes 196640 | tf_op jit(solution)/shard_map/ppermute | solution.py:247
  163.4 3.4 %all-to-all-done.3.mine_ref = bf16[8,256,128]{2,1,0:T(8,128)(2,1)S(1)} async-done(((bf16[8,256,128]{2,1,0:T(8,128)(2,1)}), bf16[8,256,128]{2,1,0:T(8,128)(2,1)S(1)}, u32[]{:S(2)}, u32[]{:S(2)}) %all-to-all-start.3) | async-done | bytes 524320 | tf_op jit(solution)/shard_map/all_to_all | solution.py:226
  171.2 3.5 %collective-permute-start.17 = (bf16[64,128]{1,0:T(8,128)(2,1)S(1)}, bf16[64,128]{1,0:T(8,128)(2,1)S(1)}, u32[]{:S(2)}, u32[]{:S(2)}) collective-permute-start(bf16[64,128]{1,0:T(8,128)(2,1)S(1)} %get-tuple-element.51), channel_id=1, source_target_pairs={{0,16},{16,32},{32,48},{48,64},{64,80},{80,96},{96,112},{112,128},... | collective-permute-start | bytes 49160 | tf_op jit(solution)/shard_map/ppermute | solution.py:294
  177.1 19.3 %all_to_all.31.msgs_ref = f32[16,1,128]{2,1,0:T(1,128)S(1)} all-to-all(f32[16,1,128]{2,1,0:T(1,128)S(1)} %get-tuple-element.52), channel_id=1, replica_groups=mesh['grp'=2,'sp'=16,'x'=8,'core'=2] {'sp'}, dimensions={0} | all-to-all | bytes 16384 | tf_op jit(solution)/shard_map/all_to_all | solution.py:226
  196.6 15.2 %all_to_all.32.mine_ref = bf16[8,64,256]{2,1,0:T(8,128)(2,1)S(1)} all-to-all(bf16[8,64,256]{2,1,0:T(8,128)(2,1)S(1)} %shard_map.109), channel_id=1, replica_groups=mesh['grp'=2,'sp'=16,'x'=8,'core'=2] {'x'}, dimensions={0} | all-to-all | bytes 524288 | tf_op jit(solution)/shard_map/all_to_all | solution.py:226
  (86 shorter events, 31.8 us)
Async XLA Ops:
  1.8 43.8 %copy-start = (bf16[256,128]{1,0:T(8,128)(2,1)S(1)}, bf16[256,128]{1,0:T(8,128)(2,1)}, u32[]{:S(2)}) copy-start(bf16[256,128]{1,0:T(8,128)(2,1)} %residual_ref.1) | copy-start | bytes 196612
  1.8 84.2 %all-to-all-start = ((bf16[16,128,128]{2,1,0:T(8,128)(2,1)}), bf16[16,128,128]{2,1,0:T(8,128)(2,1)S(1)}, u32[]{:S(2)}, u32[]{:S(2)}) async-start(bf16[16,128,128]{2,1,0:T(8,128)(2,1)} %get-tuple-element.31), calls=%async_computation | async-start | bytes 1048576 | tf_op jit(solution)/shard_map/all_to_all | solution.py:226
  45.6 10.7 %collective-permute-start = (bf16[256,128]{1,0:T(8,128)(2,1)S(1)}, bf16[256,128]{1,0:T(8,128)(2,1)S(1)}, u32[]{:S(2)}, u32[]{:S(2)}) collective-permute-start(bf16[256,128]{1,0:T(8,128)(2,1)S(1)} %copy-done), channel_id=1, source_target_pairs={{0,8},{2,10},{4,12},{6,14},{8,0},{10,2},{12,4},{14,6},{1,9},{3,11}... | collective-permute-start | bytes 196616 | tf_op jit(solution)/shard_map/ppermute | solution.py:231
  56.4 16.8 %copy-start.2 = (bf16[2,1,64,64]{3,2,1,0:T(8,128)(2,1)S(1)}, bf16[2,1,64,64]{3,2,1,0:T(8,128)(2,1)}, u32[]{:S(2)}) copy-start(bf16[2,1,64,64]{3,2,1,0:T(8,128)(2,1)} %param.15) | copy-start | bytes 49156
  56.4 20.8 %collective-permute-start.1 = (bf16[2,256,128]{2,1,0:T(8,128)(2,1)S(1)}, bf16[2,256,128]{2,1,0:T(8,128)(2,1)S(1)}, u32[]{:S(2)}, u32[]{:S(2)}) collective-permute-start(bf16[2,256,128]{2,1,0:T(8,128)(2,1)S(1)} %pad_maximum_fusion.1), channel_id=1, source_target_pairs={{0,12},{1,5},{2,14},{3,7},{4,0},{5,9},{6,2},{7,11},{8,4},{9,13},{1... | collective-permute-start | bytes 393224 | tf_op jit(solution)/shard_map/ppermute | solution.py:247
  62.9 14.3 %collective-permute-start.2 = (bf16[2,256,128]{2,1,0:T(8,128)(2,1)S(1)}, bf16[2,256,128]{2,1,0:T(8,128)(2,1)S(1)}, u32[]{:S(2)}, u32[]{:S(2)}) collective-permute-start(bf16[2,256,128]{2,1,0:T(8,128)(2,1)S(1)} %pad_maximum_fusion.1), channel_id=1, source_target_pairs={{0,14},{1,3},{2,0},{3,5},{4,2},{5,7},{6,4},{7,9},{8,6},{9,11},{10,... | collective-permute-start | bytes 393224 | tf_op jit(solution)/shard_map/ppermute | solution.py:247
  65.8 25.8 %collective-permute-start.7 = (bf16[256,128]{1,0:T(8,128)(2,1)S(1)}, bf16[256,128]{1,0:T(8,128)(2,1)S(1)}, u32[]{:S(2)}, u32[]{:S(2)}) collective-permute-start(bf16[256,128]{1,0:T(8,128)(2,1)S(1)} %get-tuple-element.46), channel_id=1, source_target_pairs={{0,192},{16,208},{32,224},{48,240},{64,0},{80,16},{96,32},{112,48}... | collective-permute-start | bytes 196616 | tf_op jit(solution)/shard_map/ppermute | solution.py:231
  74.0 8.1 %collective-permute-start.3 = (bf16[2,256,128]{2,1,0:T(8,128)(2,1)S(1)}, bf16[2,256,128]{2,1,0:T(8,128)(2,1)S(1)}, u32[]{:S(2)}, u32[]{:S(2)}) collective-permute-start(bf16[2,256,128]{2,1,0:T(8,128)(2,1)S(1)} %pad_maximum_fusion.1), channel_id=1, source_target_pairs={{0,2},{1,15},{2,4},{3,1},{4,6},{5,3},{6,8},{7,5},{8,10},{9,7},{10,... | collective-permute-start | bytes 393224 | tf_op jit(solution)/shard_map/ppermute | solution.py:247
  82.1 3.8 %collective-permute-start.4 = (bf16[8,256,128]{2,1,0:T(8,128)(2,1)S(1)}, bf16[8,256,128]{2,1,0:T(8,128)(2,1)S(1)}, u32[]{:S(2)}, u32[]{:S(2)}) collective-permute-start(bf16[8,256,128]{2,1,0:T(8,128)(2,1)S(1)} %constant_dynamic-update-slice_fusion.mine_ref), channel_id=1, source_target_pairs={{0,1},{1,0},{2,3},{3,2},{4,5},{5,4},{6,7},{7,6},{8,9},{9,8},{10,11... | collective-permute-start | bytes 1572872 | tf_op jit(solution)/shard_map/ppermute | solution.py:231
  86.5 4.1 %collective-permute-start.5 = (bf16[64,128]{1,0:T(8,128)(2,1)S(1)}, bf16[64,128]{1,0:T(8,128)(2,1)S(1)}, u32[]{:S(2)}, u32[]{:S(2)}) collective-permute-start(bf16[64,128]{1,0:T(8,128)(2,1)S(1)} %get-tuple-element.33), channel_id=1, source_target_pairs={{0,16},{16,32},{32,48},{48,64},{64,80},{80,96},{96,112},{112,128},... | collective-permute-start | bytes 49160 | tf_op jit(solution)/shard_map/ppermute | solution.py:294
  91.6 32.7 %collective-permute-start.8 = (bf16[256,128]{1,0:T(8,128)(2,1)S(1)}, bf16[256,128]{1,0:T(8,128)(2,1)S(1)}, u32[]{:S(2)}, u32[]{:S(2)}) collective-permute-start(bf16[256,128]{1,0:T(8,128)(2,1)S(1)} %get-tuple-element.46), channel_id=1, source_target_pairs={{0,64},{16,80},{32,96},{48,112},{64,128},{80,144},{96,160},{112,17... | collective-permute-start | bytes 196616 | tf_op jit(solution)/shard_map/ppermute | solution.py:231
  97.1 27.2 %collective-permute-start.9 = (bf16[256,128]{1,0:T(8,128)(2,1)S(1)}, bf16[256,128]{1,0:T(8,128)(2,1)S(1)}, u32[]{:S(2)}, u32[]{:S(2)}) collective-permute-start(bf16[256,128]{1,0:T(8,128)(2,1)S(1)} %collective-permute-done.7), channel_id=1, source_target_pairs={{0,192},{16,208},{32,224},{48,240},{64,0},{80,16},{96,32},{112,48}... | collective-permute-start | bytes 196616 | tf_op jit(solution)/shard_map/ppermute | solution.py:231
  124.4 12.0 %collective-permute-start.10 = (bf16[4,64,128]{2,1,0:T(8,128)(2,1)S(1)}, bf16[4,64,128]{2,1,0:T(8,128)(2,1)S(1)}, u32[]{:S(2)}, u32[]{:S(2)}) collective-permute-start(bf16[4,64,128]{2,1,0:T(8,128)(2,1)S(1)} %pad_maximum_fusion.2), channel_id=1, source_target_pairs={{0,224},{1,33},{16,240},{17,49},{32,0},{33,65},{48,16},{49,81},{64... | collective-permute-start | bytes 196616 | tf_op jit(solution)/shard_map/ppermute | solution.py:247
  126.9 13.8 %all-to-all-start.2 = ((bf16[8,64,256]{2,1,0:T(8,128)(2,1)}), bf16[8,64,256]{2,1,0:T(8,128)(2,1)S(1)}, u32[]{:S(2)}, u32[]{:S(2)}) async-start(bf16[8,64,256]{2,1,0:T(8,128)(2,1)} %shard_map.102), calls=%async_computation.2 | async-start | bytes 524288 | tf_op jit(solution)/shard_map/all_to_all | solution.py:226
  130.5 6.2 %collective-permute-start.11 = (bf16[4,64,128]{2,1,0:T(8,128)(2,1)S(1)}, bf16[4,64,128]{2,1,0:T(8,128)(2,1)S(1)}, u32[]{:S(2)}, u32[]{:S(2)}) collective-permute-start(bf16[4,64,128]{2,1,0:T(8,128)(2,1)S(1)} %pad_maximum_fusion.2), channel_id=1, source_target_pairs={{0,240},{1,17},{16,0},{17,33},{32,16},{33,49},{48,32},{49,65},{64,... | collective-permute-start | bytes 196616 | tf_op jit(solution)/shard_map/ppermute | solution.py:247
  133.1 9.6 %collective-permute-start.12 = (bf16[4,64,128]{2,1,0:T(8,128)(2,1)S(1)}, bf16[4,64,128]{2,1,0:T(8,128)(2,1)S(1)}, u32[]{:S(2)}, u32[]{:S(2)}) collective-permute-start(bf16[4,64,128]{2,1,0:T(8,128)(2,1)S(1)} %pad_maximum_fusion.2), channel_id=1, source_target_pairs={{0,16},{1,241},{16,32},{17,1},{32,48},{33,17},{48,64},{49,33},{64,... | collective-permute-start | bytes 196616 | tf_op jit(solution)/shard_map/ppermute | solution.py:247
  140.7 3.4 %collective-permute-start.6 = (bf16[8,64,256]{2,1,0:T(8,128)(2,1)S(1)}, bf16[8,64,256]{2,1,0:T(8,128)(2,1)S(1)}, u32[]{:S(2)}, u32[]{:S(2)}) collective-permute-start(bf16[8,64,256]{2,1,0:T(8,128)(2,1)S(1)} %all-to-all-done.2.mine_ref), channel_id=1, source_target_pairs={{0,1},{1,0},{2,3},{3,2},{4,5},{5,4},{6,7},{7,6},{8,9},{9,8},{10,11... | collective-permute-start | bytes 786440 | tf_op jit(solution)/shard_map/ppermute | solution.py:231
  145.3 21.5 %all-to-all-start.3 = ((bf16[8,256,128]{2,1,0:T(8,128)(2,1)}), bf16[8,256,128]{2,1,0:T(8,128)(2,1)S(1)}, u32[]{:S(2)}, u32[]{:S(2)}) async-start(bf16[8,256,128]{2,1,0:T(8,128)(2,1)} %get-tuple-element.45), calls=%async_computation.3 | async-start | bytes 1048576 | tf_op jit(solution)/shard_map/all_to_all | solution.py:226
  149.1 10.7 %collective-permute-start.14 = (bf16[4,192,128]{2,1,0:T(8,128)(2,1)S(1)}, bf16[4,192,128]{2,1,0:T(8,128)(2,1)S(1)}, u32[]{:S(2)}, u32[]{:S(2)}) collective-permute-start(bf16[4,192,128]{2,1,0:T(8,128)(2,1)S(1)} %pad_maximum_fusion), channel_id=1, source_target_pairs={{0,224},{1,33},{16,240},{17,49},{32,0},{33,65},{48,16},{49,81},{64... | collective-permute-start | bytes 589832 | tf_op jit(solution)/shard_map/ppermute | solution.py:247
  153.2 10.1 %collective-permute-start.15 = (bf16[4,192,128]{2,1,0:T(8,128)(2,1)S(1)}, bf16[4,192,128]{2,1,0:T(8,128)(2,1)S(1)}, u32[]{:S(2)}, u32[]{:S(2)}) collective-permute-start(bf16[4,192,128]{2,1,0:T(8,128)(2,1)S(1)} %pad_maximum_fusion), channel_id=1, source_target_pairs={{0,240},{1,17},{16,0},{17,33},{32,16},{33,49},{48,32},{49,65},{64,... | collective-permute-start | bytes 589832 | tf_op jit(solution)/shard_map/ppermute | solution.py:247
  155.2 13.6 %collective-permute-start.16 = (bf16[4,192,128]{2,1,0:T(8,128)(2,1)S(1)}, bf16[4,192,128]{2,1,0:T(8,128)(2,1)S(1)}, u32[]{:S(2)}, u32[]{:S(2)}) collective-permute-start(bf16[4,192,128]{2,1,0:T(8,128)(2,1)S(1)} %pad_maximum_fusion), channel_id=1, source_target_pairs={{0,16},{1,241},{16,32},{17,1},{32,48},{33,17},{48,64},{49,33},{64,... | collective-permute-start | bytes 589832 | tf_op jit(solution)/shard_map/ppermute | solution.py:247
  166.8 3.8 %collective-permute-start.13 = (bf16[8,256,128]{2,1,0:T(8,128)(2,1)S(1)}, bf16[8,256,128]{2,1,0:T(8,128)(2,1)S(1)}, u32[]{:S(2)}, u32[]{:S(2)}) collective-permute-start(bf16[8,256,128]{2,1,0:T(8,128)(2,1)S(1)} %all-to-all-done.3.mine_ref), channel_id=1, source_target_pairs={{0,1},{1,0},{2,3},{3,2},{4,5},{5,4},{6,7},{7,6},{8,9},{9,8},{10,11... | collective-permute-start | bytes 1572872 | tf_op jit(solution)/shard_map/ppermute | solution.py:231
  171.2 4.9 %collective-permute-start.17 = (bf16[64,128]{1,0:T(8,128)(2,1)S(1)}, bf16[64,128]{1,0:T(8,128)(2,1)S(1)}, u32[]{:S(2)}, u32[]{:S(2)}) collective-permute-start(bf16[64,128]{1,0:T(8,128)(2,1)S(1)} %get-tuple-element.51), channel_id=1, source_target_pairs={{0,16},{16,32},{32,48},{48,64},{64,80},{80,96},{96,112},{112,128},... | collective-permute-start | bytes 49160 | tf_op jit(solution)/shard_map/ppermute | solution.py:294
  211.8 3.4 %collective-permute-start.18 = (bf16[8,64,256]{2,1,0:T(8,128)(2,1)S(1)}, bf16[8,64,256]{2,1,0:T(8,128)(2,1)S(1)}, u32[]{:S(2)}, u32[]{:S(2)}) collective-permute-start(bf16[8,64,256]{2,1,0:T(8,128)(2,1)S(1)} %all_to_all.32.mine_ref), channel_id=1, source_target_pairs={{0,1},{1,0},{2,3},{3,2},{4,5},{5,4},{6,7},{7,6},{8,9},{9,8},{10,11... | collective-permute-start | bytes 786440 | tf_op jit(solution)/shard_map/ppermute | solution.py:231
  (5 other events, 23.0 us)

commit v6 on v5

--- a/solution.py
+++ b/solution.py
@@ -22,21 +22,45 @@
     return jnp.where(u > -0.5, -u * series, 1.0 - jnp.exp(u))
 
 
+def softplus(x):
+    y = jnp.exp(-jnp.abs(x))
+    z = y / (2.0 + y)
+    series = jnp.zeros_like(z)
+    for n in range(17, 0, -2):
+        series = series * (z * z) + 1.0 / n
+    return jnp.maximum(x, 0.0) + 2.0 * z * series
+
+
 def scan_kernel(
-    layer, value_ref, before_ref, consts_ref, maps_ref, offset_ref, cum_ref, state_ref, msg_ref
+    layer,
+    value_ref,
+    before_ref,
+    taps_ref,
+    param_ref,
+    recur_ref,
+    input_ref,
+    offset_ref,
+    cum_ref,
+    state_ref,
+    msg_ref,
 ):
     channels, tok = value_ref.shape
-    taps = 4
+    taps = taps_ref.shape[1]
+    rate = -RATE_SCALE * softplus(-param_ref[layer : layer + 1, :])
+    rest = jnp.zeros((LANES - taps - 1, channels), jnp.float32)
+    consts = jnp.concatenate([taps_ref[layer], rate, rest], axis=0)
+    consts = jnp.concatenate([consts, jnp.zeros((LANES, LANES - channels), jnp.float32)], axis=1).T
+    consts = consts[:channels]
+    maps = jnp.concatenate([recur_ref[layer, 0], input_ref[layer, 0]], axis=1)
     value = value_ref[...].astype(jnp.float32)
     full = jnp.concatenate([before_ref[...].astype(jnp.float32), value], axis=1)
-    consts = consts_ref[layer]
     smoothed = consts[:, taps - 1 : taps] * value
     for back in range(1, taps):
         shifted = pltpu.roll(full, back, axis=1)[:, LANES:]
         smoothed = smoothed + consts[:, taps - 1 - back : taps - back] * shifted
     half = smoothed.astype(jnp.bfloat16)
     gates = lax.dot_general(
-        maps_ref[layer], half, (((1,), (0,)), ((), ())), preferred_element_type=jnp.float32
+        maps, half, (((0,), (0,)), ((), ())), preferred_element_type=jnp.float32
     )
     gates = 1.0 / (1.0 + jnp.exp(-gates))
     recur, inputs = gates[:channels], gates[channels:]
@@ -198,7 +222,7 @@
     return kernel_call(mix_kernel, out, mine, theirs, weights, residual)
 
 
-def scan_call(layer, value, before, consts, maps, offset, count):
+def scan_call(layer, value, before, taps, param, recur_map, input_map, offset, count):
     channels, tok = value.shape
     out = [
         pltpu.VMEM((channels, tok), jnp.float32),
@@ -206,7 +230,8 @@
         pltpu.VMEM((count, 1, 2 * channels), jnp.float32),
     ]
     kernel = functools.partial(scan_kernel, layer)
-    return kernel_call(kernel, out, value, before, consts, maps, offset)
+    operands = (value, before, taps, param, recur_map, input_map, offset)
+    return kernel_call(kernel, out, *operands)
 
 
 def close_call(msgs, cum, state, gate, copies):
@@ -270,12 +295,7 @@
     first, shard = pack_call(value_proj, gate_proj, mix_proj, count)
     weights = exchange(first, "sp")
     held = jnp.stack([tokens, far_hop(tokens, "x")])
-    hop_one = far_hop(shard, "sp", -1)
     mine = near_hops(held, "x")
-    rates = -RATE_SCALE * jax.nn.softplus(-decay_param)
-    consts = jnp.concatenate([conv_taps.transpose(0, 2, 1), rates[:, :, None]], axis=2)
-    consts = jnp.pad(consts, ((0, 0), (0, 0), (0, LANES - consts.shape[2])))
-    maps = jnp.concatenate([recur_map[:, 0], input_map[:, 0]], axis=2).transpose(0, 2, 1)
     gains = [gain.reshape(chips * cores, 1, own_cols) for gain in norm_gain]
     gains[1] = copy_call(gains[1])
     gains[1] = copy_call(gains[1])
@@ -292,7 +312,20 @@
             layer == 0, layer > 0, mine, theirs, gains[layer], weights, channels
         )
         before = lax.ppermute(tail, "sp", [(i, i + 1) for i in range(count - 1)])
-        cum, state, msg = scan_call(layer, value_rows, before, consts, maps, decay_offset, count)
+        if more:
+            _, shard = lax.optimization_barrier((tail, shard))
+            hop_one = far_hop(shard, "sp", -1)
+        cum, state, msg = scan_call(
+            layer,
+            value_rows,
+            before,
+            conv_taps,
+            decay_param,
+            recur_map,
+            input_map,
+            decay_offset,
+            count,
+        )
         msgs = exchange(msg, "sp")
         if more:
             _, shard, hop_one = lax.optimization_barrier((msg, shard, hop_one))

time: 219 us -> 221 us (level)
  blocking collectives: 54.1 us -> 57.5 us
    all_to_all x3, blocking collectives: 54.1 us -> 57.5 us  [exchange(): return lax.all_to_all(copies, axis, split_axis=0, concat_axis=0, tiled=True)]
    ppermute x8, waiting for transfers between devices: 8.66 us -> 10.9 us  [shift(): lax.ppermute(array, axis, [(i, (i + steps) % count) for i in range(count)])]
  transfers between devices with their start and end apart: 22 -> 22, of which waited for: 13 -> 15; matrix products, arithmetic and copies ran while one was open for 0% -> 0% of each run, Pallas kernels for 1% -> 1%
where the time goes in v6:
time: 221 us; the launch traced here: 219 us
  starting transfers between devices  122 us (55%)
  blocking collectives  57.5 us (26%)
  waiting for transfers between devices  30.1 us (14%)
  Pallas kernels  8.2 us (4%)
    all_to_all x3, blocking collectives, exchange(): return lax.all_to_all(copies, axis, split_axis=0, concat_axis=0, tiled=True)  57.5 us
    all_to_all x3, starting transfers between devices, exchange(): return lax.all_to_all(copies, axis, split_axis=0, concat_axis=0, tiled=True)  51.1 us
    ppermute x8, starting transfers between devices, shift(): lax.ppermute(array, axis, [(i, (i + steps) % count) for i in range(count)])  33.7 us
    ppermute x9, starting transfers between devices, hop(): return lax.ppermute(held, (axis, 'core'), pairs)  31.3 us
    ppermute x8, waiting for transfers between devices, shift(): lax.ppermute(array, axis, [(i, (i + steps) % count) for i in range(count)])  10.9 us
    ppermute x9, waiting for transfers between devices, hop(): return lax.ppermute(held, (axis, 'core'), pairs)  9.01 us
    all_to_all x3, waiting for transfers between devices, exchange(): return lax.all_to_all(copies, axis, split_axis=0, concat_axis=0, tiled=True)  7.39 us
    pallas_call x11, Pallas kernels, kernel_call(): pl.pallas_call(kernel, out_shape=out_shape, in_specs=vmem(len(operands)),...  6.45 us
  transfers between devices with their start and end apart: 22, of which 15 were waited for; matrix products, arithmetic and copies ran while one was open for 0% of the time, Pallas kernels for 1%

profile of v6, /device:TPU:80, one launch (start us, length us, event | category | flops | bytes accessed | tf_op | source)
XLA Modules:
  0.0 218.8 jit_solution(14484301290909852614)
XLA Ops:
  1.8 43.8 %all-to-all-start = ((bf16[16,128,128]{2,1,0:T(8,128)(2,1)}), bf16[16,128,128]{2,1,0:T(8,128)(2,1)S(1)}, u32[]{:S(2)}, u32[]{:S(2)}) async-start(bf16[16,128,128]{2,1,0:T(8,128)(2,1)} %get-tuple-element.32), calls=%async_computation | async-start | bytes 1048576 | tf_op jit(solution)/shard_map/all_to_all | solution.py:251
  45.6 8.0 %collective-permute-start = (bf16[256,128]{1,0:T(8,128)(2,1)S(1)}, bf16[256,128]{1,0:T(8,128)(2,1)S(1)}, u32[]{:S(2)}, u32[]{:S(2)}) collective-permute-start(bf16[256,128]{1,0:T(8,128)(2,1)S(1)} %copy-done), channel_id=1, source_target_pairs={{0,8},{2,10},{4,12},{6,14},{8,0},{10,2},{12,4},{14,6},{1,9},{3,11}... | collective-permute-start | bytes 196616 | tf_op jit(solution)/shard_map/ppermute | solution.py:256
  53.6 2.8 %collective-permute-done = bf16[256,128]{1,0:T(8,128)(2,1)S(1)} collective-permute-done((bf16[256,128]{1,0:T(8,128)(2,1)S(1)}, bf16[256,128]{1,0:T(8,128)(2,1)S(1)}, u32[]{:S(2)}, u32[]{:S(2)}) %collective-permute-start) | collective-permute-done | bytes 65568 | tf_op jit(solution)/shard_map/ppermute | solution.py:256
  56.4 6.6 %collective-permute-start.1 = (bf16[2,256,128]{2,1,0:T(8,128)(2,1)S(1)}, bf16[2,256,128]{2,1,0:T(8,128)(2,1)S(1)}, u32[]{:S(2)}, u32[]{:S(2)}) collective-permute-start(bf16[2,256,128]{2,1,0:T(8,128)(2,1)S(1)} %pad_maximum_fusion.1), channel_id=1, source_target_pairs={{0,12},{1,5},{2,14},{3,7},{4,0},{5,9},{6,2},{7,11},{8,4},{9,13},{1... | collective-permute-start | bytes 393224 | tf_op jit(solution)/shard_map/ppermute | solution.py:272
  62.9 2.9 %collective-permute-start.2 = (bf16[2,256,128]{2,1,0:T(8,128)(2,1)S(1)}, bf16[2,256,128]{2,1,0:T(8,128)(2,1)S(1)}, u32[]{:S(2)}, u32[]{:S(2)}) collective-permute-start(bf16[2,256,128]{2,1,0:T(8,128)(2,1)S(1)} %pad_maximum_fusion.1), channel_id=1, source_target_pairs={{0,14},{1,3},{2,0},{3,5},{4,2},{5,7},{6,4},{7,9},{8,6},{9,11},{10,... | collective-permute-start | bytes 393224 | tf_op jit(solution)/shard_map/ppermute | solution.py:272
  65.8 3.0 %collective-permute-start.3 = (bf16[2,256,128]{2,1,0:T(8,128)(2,1)S(1)}, bf16[2,256,128]{2,1,0:T(8,128)(2,1)S(1)}, u32[]{:S(2)}, u32[]{:S(2)}) collective-permute-start(bf16[2,256,128]{2,1,0:T(8,128)(2,1)S(1)} %pad_maximum_fusion.1), channel_id=1, source_target_pairs={{0,2},{1,15},{2,4},{3,1},{4,6},{5,3},{6,8},{7,5},{8,10},{9,7},{10,... | collective-permute-start | bytes 393224 | tf_op jit(solution)/shard_map/ppermute | solution.py:272
  70.6 3.3 %collective-permute-done.3 = bf16[2,256,128]{2,1,0:T(8,128)(2,1)S(1)} collective-permute-done((bf16[2,256,128]{2,1,0:T(8,128)(2,1)S(1)}, bf16[2,256,128]{2,1,0:T(8,128)(2,1)S(1)}, u32[]{:S(2)}, u32[]{:S(2)}) %collective-permute-start.3) | collective-permute-done | bytes 131104 | tf_op jit(solution)/shard_map/ppermute | solution.py:272
  78.3 7.3 %collective-permute-start.7 = (bf16[256,128]{1,0:T(8,128)(2,1)S(1)}, bf16[256,128]{1,0:T(8,128)(2,1)S(1)}, u32[]{:S(2)}, u32[]{:S(2)}) collective-permute-start(bf16[256,128]{1,0:T(8,128)(2,1)S(1)} %get-tuple-element.48), channel_id=1, source_target_pairs={{0,192},{16,208},{32,224},{48,240},{64,0},{80,16},{96,32},{112,48}... | collective-permute-start | bytes 196616 | tf_op jit(solution)/shard_map/ppermute | solution.py:256
  85.6 2.5 %collective-permute-start.5 = (bf16[64,128]{1,0:T(8,128)(2,1)S(1)}, bf16[64,128]{1,0:T(8,128)(2,1)S(1)}, u32[]{:S(2)}, u32[]{:S(2)}) collective-permute-start(bf16[64,128]{1,0:T(8,128)(2,1)S(1)} %get-tuple-element.34), channel_id=1, source_target_pairs={{0,16},{16,32},{32,48},{48,64},{64,80},{80,96},{96,112},{112,128},... | collective-permute-start | bytes 49160 | tf_op jit(solution)/shard_map/ppermute | solution.py:314
  92.2 7.6 %collective-permute-start.8 = (bf16[256,128]{1,0:T(8,128)(2,1)S(1)}, bf16[256,128]{1,0:T(8,128)(2,1)S(1)}, u32[]{:S(2)}, u32[]{:S(2)}) collective-permute-start(bf16[256,128]{1,0:T(8,128)(2,1)S(1)} %get-tuple-element.48), channel_id=1, source_target_pairs={{0,64},{16,80},{32,96},{48,112},{64,128},{80,144},{96,160},{112,17... | collective-permute-start | bytes 196616 | tf_op jit(solution)/shard_map/ppermute | solution.py:256
  99.8 3.1 %collective-permute-start.9 = (bf16[256,128]{1,0:T(8,128)(2,1)S(1)}, bf16[256,128]{1,0:T(8,128)(2,1)S(1)}, u32[]{:S(2)}, u32[]{:S(2)}) collective-permute-start(bf16[256,128]{1,0:T(8,128)(2,1)S(1)} %collective-permute-done.7), channel_id=1, source_target_pairs={{0,192},{16,208},{32,224},{48,240},{64,0},{80,16},{96,32},{112,48}... | collective-permute-start | bytes 196616 | tf_op jit(solution)/shard_map/ppermute | solution.py:256
  102.9 23.0 %all_to_all.30.msgs_ref = f32[16,1,128]{2,1,0:T(1,128)S(1)} all-to-all(f32[16,1,128]{2,1,0:T(1,128)S(1)} %get-tuple-element.35), channel_id=1, replica_groups=mesh['grp'=2,'sp'=16,'x'=8,'core'=2] {'sp'}, dimensions={0} | all-to-all | bytes 16384 | tf_op jit(solution)/shard_map/all_to_all | solution.py:251
  129.3 3.6 %all-to-all-start.2 = ((bf16[8,64,256]{2,1,0:T(8,128)(2,1)}), bf16[8,64,256]{2,1,0:T(8,128)(2,1)S(1)}, u32[]{:S(2)}, u32[]{:S(2)}) async-start(bf16[8,64,256]{2,1,0:T(8,128)(2,1)} %shard_map.102), calls=%async_computation.2 | async-start | bytes 524288 | tf_op jit(solution)/shard_map/all_to_all | solution.py:251
  133.0 2.6 %collective-permute-start.11 = (bf16[4,64,128]{2,1,0:T(8,128)(2,1)S(1)}, bf16[4,64,128]{2,1,0:T(8,128)(2,1)S(1)}, u32[]{:S(2)}, u32[]{:S(2)}) collective-permute-start(bf16[4,64,128]{2,1,0:T(8,128)(2,1)S(1)} %pad_maximum_fusion.2), channel_id=1, source_target_pairs={{0,240},{1,17},{16,0},{17,33},{32,16},{33,49},{48,32},{49,65},{64,... | collective-permute-start | bytes 196616 | tf_op jit(solution)/shard_map/ppermute | solution.py:272
  135.5 3.3 %collective-permute-start.12 = (bf16[4,64,128]{2,1,0:T(8,128)(2,1)S(1)}, bf16[4,64,128]{2,1,0:T(8,128)(2,1)S(1)}, u32[]{:S(2)}, u32[]{:S(2)}) collective-permute-start(bf16[4,64,128]{2,1,0:T(8,128)(2,1)S(1)} %pad_maximum_fusion.2), channel_id=1, source_target_pairs={{0,16},{1,241},{16,32},{17,1},{32,48},{33,17},{48,64},{49,33},{64,... | collective-permute-start | bytes 196616 | tf_op jit(solution)/shard_map/ppermute | solution.py:272
  139.2 4.0 %all-to-all-done.2.mine_ref = bf16[8,64,256]{2,1,0:T(8,128)(2,1)S(1)} async-done(((bf16[8,64,256]{2,1,0:T(8,128)(2,1)}), bf16[8,64,256]{2,1,0:T(8,128)(2,1)S(1)}, u32[]{:S(2)}, u32[]{:S(2)}) %all-to-all-start.2) | async-done | bytes 262176 | tf_op jit(solution)/shard_map/all_to_all | solution.py:251
  147.8 3.7 %all-to-all-start.3 = ((bf16[8,256,128]{2,1,0:T(8,128)(2,1)}), bf16[8,256,128]{2,1,0:T(8,128)(2,1)S(1)}, u32[]{:S(2)}, u32[]{:S(2)}) async-start(bf16[8,256,128]{2,1,0:T(8,128)(2,1)} %get-tuple-element.47), calls=%async_computation.3 | async-start | bytes 1048576 | tf_op jit(solution)/shard_map/all_to_all | solution.py:251
  151.6 4.5 %collective-permute-start.14 = (bf16[4,192,128]{2,1,0:T(8,128)(2,1)S(1)}, bf16[4,192,128]{2,1,0:T(8,128)(2,1)S(1)}, u32[]{:S(2)}, u32[]{:S(2)}) collective-permute-start(bf16[4,192,128]{2,1,0:T(8,128)(2,1)S(1)} %pad_maximum_fusion), channel_id=1, source_target_pairs={{0,224},{1,33},{16,240},{17,49},{32,0},{33,65},{48,16},{49,81},{64... | collective-permute-start | bytes 589832 | tf_op jit(solution)/shard_map/ppermute | solution.py:272
  158.1 4.0 %collective-permute-start.16 = (bf16[4,192,128]{2,1,0:T(8,128)(2,1)S(1)}, bf16[4,192,128]{2,1,0:T(8,128)(2,1)S(1)}, u32[]{:S(2)}, u32[]{:S(2)}) collective-permute-start(bf16[4,192,128]{2,1,0:T(8,128)(2,1)S(1)} %pad_maximum_fusion), channel_id=1, source_target_pairs={{0,16},{1,241},{16,32},{17,1},{32,48},{33,17},{48,64},{49,33},{64,... | collective-permute-start | bytes 589832 | tf_op jit(solution)/shard_map/ppermute | solution.py:272
  162.3 3.6 %collective-permute-done.15 = bf16[4,192,128]{2,1,0:T(8,128)(2,1)S(1)} collective-permute-done((bf16[4,192,128]{2,1,0:T(8,128)(2,1)S(1)}, bf16[4,192,128]{2,1,0:T(8,128)(2,1)S(1)}, u32[]{:S(2)}, u32[]{:S(2)}) %collective-permute-start.15) | collective-permute-done | bytes 196640 | tf_op jit(solution)/shard_map/ppermute | solution.py:272
  165.9 3.4 %all-to-all-done.3.mine_ref = bf16[8,256,128]{2,1,0:T(8,128)(2,1)S(1)} async-done(((bf16[8,256,128]{2,1,0:T(8,128)(2,1)}), bf16[8,256,128]{2,1,0:T(8,128)(2,1)S(1)}, u32[]{:S(2)}, u32[]{:S(2)}) %all-to-all-start.3) | async-done | bytes 524320 | tf_op jit(solution)/shard_map/all_to_all | solution.py:251
  173.7 3.5 %collective-permute-start.17 = (bf16[64,128]{1,0:T(8,128)(2,1)S(1)}, bf16[64,128]{1,0:T(8,128)(2,1)S(1)}, u32[]{:S(2)}, u32[]{:S(2)}) collective-permute-start(bf16[64,128]{1,0:T(8,128)(2,1)S(1)} %get-tuple-element.53), channel_id=1, source_target_pairs={{0,16},{16,32},{32,48},{48,64},{64,80},{80,96},{96,112},{112,128},... | collective-permute-start | bytes 49160 | tf_op jit(solution)/shard_map/ppermute | solution.py:314
  179.7 19.3 %all_to_all.31.msgs_ref = f32[16,1,128]{2,1,0:T(1,128)S(1)} all-to-all(f32[16,1,128]{2,1,0:T(1,128)S(1)} %get-tuple-element.54), channel_id=1, replica_groups=mesh['grp'=2,'sp'=16,'x'=8,'core'=2] {'sp'}, dimensions={0} | all-to-all | bytes 16384 | tf_op jit(solution)/shard_map/all_to_all | solution.py:251
  199.1 15.2 %all_to_all.32.mine_ref = bf16[8,64,256]{2,1,0:T(8,128)(2,1)S(1)} all-to-all(bf16[8,64,256]{2,1,0:T(8,128)(2,1)S(1)} %shard_map.109), channel_id=1, replica_groups=mesh['grp'=2,'sp'=16,'x'=8,'core'=2] {'x'}, dimensions={0} | all-to-all | bytes 524288 | tf_op jit(solution)/shard_map/all_to_all | solution.py:251
  (78 shorter events, 33.9 us)
Async XLA Ops:
  1.8 43.8 %copy-start = (bf16[256,128]{1,0:T(8,128)(2,1)S(1)}, bf16[256,128]{1,0:T(8,128)(2,1)}, u32[]{:S(2)}) copy-start(bf16[256,128]{1,0:T(8,128)(2,1)} %residual_ref.1) | copy-start | bytes 196612
  1.8 76.0 %all-to-all-start = ((bf16[16,128,128]{2,1,0:T(8,128)(2,1)}), bf16[16,128,128]{2,1,0:T(8,128)(2,1)S(1)}, u32[]{:S(2)}, u32[]{:S(2)}) async-start(bf16[16,128,128]{2,1,0:T(8,128)(2,1)} %get-tuple-element.32), calls=%async_computation | async-start | bytes 1048576 | tf_op jit(solution)/shard_map/all_to_all | solution.py:251
  45.6 10.7 %collective-permute-start = (bf16[256,128]{1,0:T(8,128)(2,1)S(1)}, bf16[256,128]{1,0:T(8,128)(2,1)S(1)}, u32[]{:S(2)}, u32[]{:S(2)}) collective-permute-start(bf16[256,128]{1,0:T(8,128)(2,1)S(1)} %copy-done), channel_id=1, source_target_pairs={{0,8},{2,10},{4,12},{6,14},{8,0},{10,2},{12,4},{14,6},{1,9},{3,11}... | collective-permute-start | bytes 196616 | tf_op jit(solution)/shard_map/ppermute | solution.py:256
  56.4 12.5 %collective-permute-start.1 = (bf16[2,256,128]{2,1,0:T(8,128)(2,1)S(1)}, bf16[2,256,128]{2,1,0:T(8,128)(2,1)S(1)}, u32[]{:S(2)}, u32[]{:S(2)}) collective-permute-start(bf16[2,256,128]{2,1,0:T(8,128)(2,1)S(1)} %pad_maximum_fusion.1), channel_id=1, source_target_pairs={{0,12},{1,5},{2,14},{3,7},{4,0},{5,9},{6,2},{7,11},{8,4},{9,13},{1... | collective-permute-start | bytes 393224 | tf_op jit(solution)/shard_map/ppermute | solution.py:272
  62.9 7.6 %collective-permute-start.2 = (bf16[2,256,128]{2,1,0:T(8,128)(2,1)S(1)}, bf16[2,256,128]{2,1,0:T(8,128)(2,1)S(1)}, u32[]{:S(2)}, u32[]{:S(2)}) collective-permute-start(bf16[2,256,128]{2,1,0:T(8,128)(2,1)S(1)} %pad_maximum_fusion.1), channel_id=1, source_target_pairs={{0,14},{1,3},{2,0},{3,5},{4,2},{5,7},{6,4},{7,9},{8,6},{9,11},{10,... | collective-permute-start | bytes 393224 | tf_op jit(solution)/shard_map/ppermute | solution.py:272
  65.8 8.1 %collective-permute-start.3 = (bf16[2,256,128]{2,1,0:T(8,128)(2,1)S(1)}, bf16[2,256,128]{2,1,0:T(8,128)(2,1)S(1)}, u32[]{:S(2)}, u32[]{:S(2)}) collective-permute-start(bf16[2,256,128]{2,1,0:T(8,128)(2,1)S(1)} %pad_maximum_fusion.1), channel_id=1, source_target_pairs={{0,2},{1,15},{2,4},{3,1},{4,6},{5,3},{6,8},{7,5},{8,10},{9,7},{10,... | collective-permute-start | bytes 393224 | tf_op jit(solution)/shard_map/ppermute | solution.py:272
  73.9 3.8 %collective-permute-start.4 = (bf16[8,256,128]{2,1,0:T(8,128)(2,1)S(1)}, bf16[8,256,128]{2,1,0:T(8,128)(2,1)S(1)}, u32[]{:S(2)}, u32[]{:S(2)}) collective-permute-start(bf16[8,256,128]{2,1,0:T(8,128)(2,1)S(1)} %constant_dynamic-update-slice_fusion.mine_ref), channel_id=1, source_target_pairs={{0,1},{1,0},{2,3},{3,2},{4,5},{5,4},{6,7},{7,6},{8,9},{9,8},{10,11... | collective-permute-start | bytes 1572872 | tf_op jit(solution)/shard_map/ppermute | solution.py:256
  77.8 11.8 %copy-start.3 = (bf16[2,1,64,64]{3,2,1,0:T(8,128)(2,1)S(1)}, bf16[2,1,64,64]{3,2,1,0:T(8,128)(2,1)}, u32[]{:S(2)}) copy-start(bf16[2,1,64,64]{3,2,1,0:T(8,128)(2,1)} %input_ref.3) | copy-start | bytes 49156
  78.3 13.9 %collective-permute-start.7 = (bf16[256,128]{1,0:T(8,128)(2,1)S(1)}, bf16[256,128]{1,0:T(8,128)(2,1)S(1)}, u32[]{:S(2)}, u32[]{:S(2)}) collective-permute-start(bf16[256,128]{1,0:T(8,128)(2,1)S(1)} %get-tuple-element.48), channel_id=1, source_target_pairs={{0,192},{16,208},{32,224},{48,240},{64,0},{80,16},{96,32},{112,48}... | collective-permute-start | bytes 196616 | tf_op jit(solution)/shard_map/ppermute | solution.py:256
  85.6 3.9 %collective-permute-start.5 = (bf16[64,128]{1,0:T(8,128)(2,1)S(1)}, bf16[64,128]{1,0:T(8,128)(2,1)S(1)}, u32[]{:S(2)}, u32[]{:S(2)}) collective-permute-start(bf16[64,128]{1,0:T(8,128)(2,1)S(1)} %get-tuple-element.34), channel_id=1, source_target_pairs={{0,16},{16,32},{32,48},{48,64},{64,80},{80,96},{96,112},{112,128},... | collective-permute-start | bytes 49160 | tf_op jit(solution)/shard_map/ppermute | solution.py:314
  92.2 34.6 %collective-permute-start.8 = (bf16[256,128]{1,0:T(8,128)(2,1)S(1)}, bf16[256,128]{1,0:T(8,128)(2,1)S(1)}, u32[]{:S(2)}, u32[]{:S(2)}) collective-permute-start(bf16[256,128]{1,0:T(8,128)(2,1)S(1)} %get-tuple-element.48), channel_id=1, source_target_pairs={{0,64},{16,80},{32,96},{48,112},{64,128},{80,144},{96,160},{112,17... | collective-permute-start | bytes 196616 | tf_op jit(solution)/shard_map/ppermute | solution.py:256
  99.8 27.0 %collective-permute-start.9 = (bf16[256,128]{1,0:T(8,128)(2,1)S(1)}, bf16[256,128]{1,0:T(8,128)(2,1)S(1)}, u32[]{:S(2)}, u32[]{:S(2)}) collective-permute-start(bf16[256,128]{1,0:T(8,128)(2,1)S(1)} %collective-permute-done.7), channel_id=1, source_target_pairs={{0,192},{16,208},{32,224},{48,240},{64,0},{80,16},{96,32},{112,48}... | collective-permute-start | bytes 196616 | tf_op jit(solution)/shard_map/ppermute | solution.py:256
  126.8 12.0 %collective-permute-start.10 = (bf16[4,64,128]{2,1,0:T(8,128)(2,1)S(1)}, bf16[4,64,128]{2,1,0:T(8,128)(2,1)S(1)}, u32[]{:S(2)}, u32[]{:S(2)}) collective-permute-start(bf16[4,64,128]{2,1,0:T(8,128)(2,1)S(1)} %pad_maximum_fusion.2), channel_id=1, source_target_pairs={{0,224},{1,33},{16,240},{17,49},{32,0},{33,65},{48,16},{49,81},{64... | collective-permute-start | bytes 196616 | tf_op jit(solution)/shard_map/ppermute | solution.py:272
  129.3 13.9 %all-to-all-start.2 = ((bf16[8,64,256]{2,1,0:T(8,128)(2,1)}), bf16[8,64,256]{2,1,0:T(8,128)(2,1)S(1)}, u32[]{:S(2)}, u32[]{:S(2)}) async-start(bf16[8,64,256]{2,1,0:T(8,128)(2,1)} %shard_map.102), calls=%async_computation.2 | async-start | bytes 524288 | tf_op jit(solution)/shard_map/all_to_all | solution.py:251
  133.0 6.2 %collective-permute-start.11 = (bf16[4,64,128]{2,1,0:T(8,128)(2,1)S(1)}, bf16[4,64,128]{2,1,0:T(8,128)(2,1)S(1)}, u32[]{:S(2)}, u32[]{:S(2)}) collective-permute-start(bf16[4,64,128]{2,1,0:T(8,128)(2,1)S(1)} %pad_maximum_fusion.2), channel_id=1, source_target_pairs={{0,240},{1,17},{16,0},{17,33},{32,16},{33,49},{48,32},{49,65},{64,... | collective-permute-start | bytes 196616 | tf_op jit(solution)/shard_map/ppermute | solution.py:272
  135.5 9.6 %collective-permute-start.12 = (bf16[4,64,128]{2,1,0:T(8,128)(2,1)S(1)}, bf16[4,64,128]{2,1,0:T(8,128)(2,1)S(1)}, u32[]{:S(2)}, u32[]{:S(2)}) collective-permute-start(bf16[4,64,128]{2,1,0:T(8,128)(2,1)S(1)} %pad_maximum_fusion.2), channel_id=1, source_target_pairs={{0,16},{1,241},{16,32},{17,1},{32,48},{33,17},{48,64},{49,33},{64,... | collective-permute-start | bytes 196616 | tf_op jit(solution)/shard_map/ppermute | solution.py:272
  143.2 3.4 %collective-permute-start.6 = (bf16[8,64,256]{2,1,0:T(8,128)(2,1)S(1)}, bf16[8,64,256]{2,1,0:T(8,128)(2,1)S(1)}, u32[]{:S(2)}, u32[]{:S(2)}) collective-permute-start(bf16[8,64,256]{2,1,0:T(8,128)(2,1)S(1)} %all-to-all-done.2.mine_ref), channel_id=1, source_target_pairs={{0,1},{1,0},{2,3},{3,2},{4,5},{5,4},{6,7},{7,6},{8,9},{9,8},{10,11... | collective-permute-start | bytes 786440 | tf_op jit(solution)/shard_map/ppermute | solution.py:256
  147.8 21.5 %all-to-all-start.3 = ((bf16[8,256,128]{2,1,0:T(8,128)(2,1)}), bf16[8,256,128]{2,1,0:T(8,128)(2,1)S(1)}, u32[]{:S(2)}, u32[]{:S(2)}) async-start(bf16[8,256,128]{2,1,0:T(8,128)(2,1)} %get-tuple-element.47), calls=%async_computation.3 | async-start | bytes 1048576 | tf_op jit(solution)/shard_map/all_to_all | solution.py:251
  151.6 10.7 %collective-permute-start.14 = (bf16[4,192,128]{2,1,0:T(8,128)(2,1)S(1)}, bf16[4,192,128]{2,1,0:T(8,128)(2,1)S(1)}, u32[]{:S(2)}, u32[]{:S(2)}) collective-permute-start(bf16[4,192,128]{2,1,0:T(8,128)(2,1)S(1)} %pad_maximum_fusion), channel_id=1, source_target_pairs={{0,224},{1,33},{16,240},{17,49},{32,0},{33,65},{48,16},{49,81},{64... | collective-permute-start | bytes 589832 | tf_op jit(solution)/shard_map/ppermute | solution.py:272
  156.1 9.8 %collective-permute-start.15 = (bf16[4,192,128]{2,1,0:T(8,128)(2,1)S(1)}, bf16[4,192,128]{2,1,0:T(8,128)(2,1)S(1)}, u32[]{:S(2)}, u32[]{:S(2)}) collective-permute-start(bf16[4,192,128]{2,1,0:T(8,128)(2,1)S(1)} %pad_maximum_fusion), channel_id=1, source_target_pairs={{0,240},{1,17},{16,0},{17,33},{32,16},{33,49},{48,32},{49,65},{64,... | collective-permute-start | bytes 589832 | tf_op jit(solution)/shard_map/ppermute | solution.py:272
  158.1 13.2 %collective-permute-start.16 = (bf16[4,192,128]{2,1,0:T(8,128)(2,1)S(1)}, bf16[4,192,128]{2,1,0:T(8,128)(2,1)S(1)}, u32[]{:S(2)}, u32[]{:S(2)}) collective-permute-start(bf16[4,192,128]{2,1,0:T(8,128)(2,1)S(1)} %pad_maximum_fusion), channel_id=1, source_target_pairs={{0,16},{1,241},{16,32},{17,1},{32,48},{33,17},{48,64},{49,33},{64,... | collective-permute-start | bytes 589832 | tf_op jit(solution)/shard_map/ppermute | solution.py:272
  169.3 3.8 %collective-permute-start.13 = (bf16[8,256,128]{2,1,0:T(8,128)(2,1)S(1)}, bf16[8,256,128]{2,1,0:T(8,128)(2,1)S(1)}, u32[]{:S(2)}, u32[]{:S(2)}) collective-permute-start(bf16[8,256,128]{2,1,0:T(8,128)(2,1)S(1)} %all-to-all-done.3.mine_ref), channel_id=1, source_target_pairs={{0,1},{1,0},{2,3},{3,2},{4,5},{5,4},{6,7},{7,6},{8,9},{9,8},{10,11... | collective-permute-start | bytes 1572872 | tf_op jit(solution)/shard_map/ppermute | solution.py:256
  173.7 4.9 %collective-permute-start.17 = (bf16[64,128]{1,0:T(8,128)(2,1)S(1)}, bf16[64,128]{1,0:T(8,128)(2,1)S(1)}, u32[]{:S(2)}, u32[]{:S(2)}) collective-permute-start(bf16[64,128]{1,0:T(8,128)(2,1)S(1)} %get-tuple-element.53), channel_id=1, source_target_pairs={{0,16},{16,32},{32,48},{48,64},{64,80},{80,96},{96,112},{112,128},... | collective-permute-start | bytes 49160 | tf_op jit(solution)/shard_map/ppermute | solution.py:314
  214.4 3.4 %collective-permute-start.18 = (bf16[8,64,256]{2,1,0:T(8,128)(2,1)S(1)}, bf16[8,64,256]{2,1,0:T(8,128)(2,1)S(1)}, u32[]{:S(2)}, u32[]{:S(2)}) collective-permute-start(bf16[8,64,256]{2,1,0:T(8,128)(2,1)S(1)} %all_to_all.32.mine_ref), channel_id=1, source_target_pairs={{0,1},{1,0},{2,3},{3,2},{4,5},{5,4},{6,7},{7,6},{8,9},{9,8},{10,11... | collective-permute-start | bytes 786440 | tf_op jit(solution)/shard_map/ppermute | solution.py:256
  (5 other events, 51.4 us)

commit v7 on v6

--- a/solution.py
+++ b/solution.py
@@ -292,10 +292,12 @@
     def swap(array):
         return shift(array, "core", 1)
 
+    far_tokens = far_hop(tokens, "x")
     first, shard = pack_call(value_proj, gate_proj, mix_proj, count)
     weights = exchange(first, "sp")
-    held = jnp.stack([tokens, far_hop(tokens, "x")])
-    mine = near_hops(held, "x")
+    mine = near_hops(jnp.stack([tokens, far_tokens]), "x")
+    _, shard = lax.optimization_barrier((mine, shard))
+    hop_one = far_hop(shard, "sp", -1)
     gains = [gain.reshape(chips * cores, 1, own_cols) for gain in norm_gain]
     gains[1] = copy_call(gains[1])
     gains[1] = copy_call(gains[1])
@@ -312,9 +314,6 @@
             layer == 0, layer > 0, mine, theirs, gains[layer], weights, channels
         )
         before = lax.ppermute(tail, "sp", [(i, i + 1) for i in range(count - 1)])
-        if more:
-            _, shard = lax.optimization_barrier((tail, shard))
-            hop_one = far_hop(shard, "sp", -1)
         cum, state, msg = scan_call(
             layer,
             value_rows,

time: 221 us -> 219 us (level)
  waiting for transfers between devices: 30.1 us -> 27.5 us
  transfers between devices with their start and end apart: 22 -> 22, of which waited for: 15 -> 13; matrix products, arithmetic and copies ran while one was open for 0% -> 0% of each run, Pallas kernels for 1% -> 1%
where the time goes in v7:
time: 219 us; the launch traced here: 217 us
  starting transfers between devices  123 us (56%)
  blocking collectives  57.2 us (26%)
  waiting for transfers between devices  27.5 us (13%)
  Pallas kernels  8.2 us (4%)
    all_to_all x3, blocking collectives, exchange(): return lax.all_to_all(copies, axis, split_axis=0, concat_axis=0, tiled=True)  57.2 us
    all_to_all x3, starting transfers between devices, exchange(): return lax.all_to_all(copies, axis, split_axis=0, concat_axis=0, tiled=True)  51.1 us
    ppermute x8, starting transfers between devices, shift(): lax.ppermute(array, axis, [(i, (i + steps) % count) for i in range(count)])  33.9 us
    ppermute x9, starting transfers between devices, hop(): return lax.ppermute(held, (axis, 'core'), pairs)  31.8 us
    ppermute x8, waiting for transfers between devices, shift(): lax.ppermute(array, axis, [(i, (i + steps) % count) for i in range(count)])  8.83 us
    ppermute x9, waiting for transfers between devices, hop(): return lax.ppermute(held, (axis, 'core'), pairs)  8.42 us
    all_to_all x3, waiting for transfers between devices, exchange(): return lax.all_to_all(copies, axis, split_axis=0, concat_axis=0, tiled=True)  7.39 us
    pallas_call x11, Pallas kernels, kernel_call(): pl.pallas_call(kernel, out_shape=out_shape, in_specs=vmem(len(operands)),...  6.45 us
  transfers between devices with their start and end apart: 22, of which 13 were waited for; matrix products, arithmetic and copies ran while one was open for 0% of the time, Pallas kernels for 1%

profile of v7, /device:TPU:80, one launch (start us, length us, event | category | flops | bytes accessed | tf_op | source)
XLA Modules:
  0.0 216.8 jit_solution(481340040762710058)
XLA Ops:
  1.8 43.8 %all-to-all-start = ((bf16[16,128,128]{2,1,0:T(8,128)(2,1)}), bf16[16,128,128]{2,1,0:T(8,128)(2,1)S(1)}, u32[]{:S(2)}, u32[]{:S(2)}) async-start(bf16[16,128,128]{2,1,0:T(8,128)(2,1)} %get-tuple-element.32), calls=%async_computation | async-start | bytes 1048576 | tf_op jit(solution)/shard_map/all_to_all | solution.py:251
  45.6 8.0 %collective-permute-start = (bf16[256,128]{1,0:T(8,128)(2,1)S(1)}, bf16[256,128]{1,0:T(8,128)(2,1)S(1)}, u32[]{:S(2)}, u32[]{:S(2)}) collective-permute-start(bf16[256,128]{1,0:T(8,128)(2,1)S(1)} %copy-done), channel_id=1, source_target_pairs={{0,8},{2,10},{4,12},{6,14},{8,0},{10,2},{12,4},{14,6},{1,9},{3,11}... | collective-permute-start | bytes 196616 | tf_op jit(solution)/shard_map/ppermute | solution.py:256
  53.6 2.8 %collective-permute-done = bf16[256,128]{1,0:T(8,128)(2,1)S(1)} collective-permute-done((bf16[256,128]{1,0:T(8,128)(2,1)S(1)}, bf16[256,128]{1,0:T(8,128)(2,1)S(1)}, u32[]{:S(2)}, u32[]{:S(2)}) %collective-permute-start) | collective-permute-done | bytes 65568 | tf_op jit(solution)/shard_map/ppermute | solution.py:256
  56.4 6.6 %collective-permute-start.1 = (bf16[2,256,128]{2,1,0:T(8,128)(2,1)S(1)}, bf16[2,256,128]{2,1,0:T(8,128)(2,1)S(1)}, u32[]{:S(2)}, u32[]{:S(2)}) collective-permute-start(bf16[2,256,128]{2,1,0:T(8,128)(2,1)S(1)} %pad_maximum_fusion.1), channel_id=1, source_target_pairs={{0,12},{1,5},{2,14},{3,7},{4,0},{5,9},{6,2},{7,11},{8,4},{9,13},{1... | collective-permute-start | bytes 393224 | tf_op jit(solution)/shard_map/ppermute | solution.py:272
  62.9 2.9 %collective-permute-start.2 = (bf16[2,256,128]{2,1,0:T(8,128)(2,1)S(1)}, bf16[2,256,128]{2,1,0:T(8,128)(2,1)S(1)}, u32[]{:S(2)}, u32[]{:S(2)}) collective-permute-start(bf16[2,256,128]{2,1,0:T(8,128)(2,1)S(1)} %pad_maximum_fusion.1), channel_id=1, source_target_pairs={{0,14},{1,3},{2,0},{3,5},{4,2},{5,7},{6,4},{7,9},{8,6},{9,11},{10,... | collective-permute-start | bytes 393224 | tf_op jit(solution)/shard_map/ppermute | solution.py:272
  65.8 3.0 %collective-permute-start.3 = (bf16[2,256,128]{2,1,0:T(8,128)(2,1)S(1)}, bf16[2,256,128]{2,1,0:T(8,128)(2,1)S(1)}, u32[]{:S(2)}, u32[]{:S(2)}) collective-permute-start(bf16[2,256,128]{2,1,0:T(8,128)(2,1)S(1)} %pad_maximum_fusion.1), channel_id=1, source_target_pairs={{0,2},{1,15},{2,4},{3,1},{4,6},{5,3},{6,8},{7,5},{8,10},{9,7},{10,... | collective-permute-start | bytes 393224 | tf_op jit(solution)/shard_map/ppermute | solution.py:272
  70.6 3.3 %collective-permute-done.3 = bf16[2,256,128]{2,1,0:T(8,128)(2,1)S(1)} collective-permute-done((bf16[2,256,128]{2,1,0:T(8,128)(2,1)S(1)}, bf16[2,256,128]{2,1,0:T(8,128)(2,1)S(1)}, u32[]{:S(2)}, u32[]{:S(2)}) %collective-permute-start.3) | collective-permute-done | bytes 131104 | tf_op jit(solution)/shard_map/ppermute | solution.py:272
  75.9 7.3 %collective-permute-start.7 = (bf16[256,128]{1,0:T(8,128)(2,1)S(1)}, bf16[256,128]{1,0:T(8,128)(2,1)S(1)}, u32[]{:S(2)}, u32[]{:S(2)}) collective-permute-start(bf16[256,128]{1,0:T(8,128)(2,1)S(1)} %get-tuple-element.48), channel_id=1, source_target_pairs={{0,192},{16,208},{32,224},{48,240},{64,0},{80,16},{96,32},{112,48}... | collective-permute-start | bytes 196616 | tf_op jit(solution)/shard_map/ppermute | solution.py:256
  83.8 2.5 %collective-permute-start.5 = (bf16[64,128]{1,0:T(8,128)(2,1)S(1)}, bf16[64,128]{1,0:T(8,128)(2,1)S(1)}, u32[]{:S(2)}, u32[]{:S(2)}) collective-permute-start(bf16[64,128]{1,0:T(8,128)(2,1)S(1)} %get-tuple-element.34), channel_id=1, source_target_pairs={{0,16},{16,32},{32,48},{48,64},{64,80},{80,96},{96,112},{112,128},... | collective-permute-start | bytes 49160 | tf_op jit(solution)/shard_map/ppermute | solution.py:316
  90.2 7.5 %collective-permute-start.8 = (bf16[256,128]{1,0:T(8,128)(2,1)S(1)}, bf16[256,128]{1,0:T(8,128)(2,1)S(1)}, u32[]{:S(2)}, u32[]{:S(2)}) collective-permute-start(bf16[256,128]{1,0:T(8,128)(2,1)S(1)} %get-tuple-element.48), channel_id=1, source_target_pairs={{0,64},{16,80},{32,96},{48,112},{64,128},{80,144},{96,160},{112,17... | collective-permute-start | bytes 196616 | tf_op jit(solution)/shard_map/ppermute | solution.py:256
  97.7 3.4 %collective-permute-start.9 = (bf16[256,128]{1,0:T(8,128)(2,1)S(1)}, bf16[256,128]{1,0:T(8,128)(2,1)S(1)}, u32[]{:S(2)}, u32[]{:S(2)}) collective-permute-start(bf16[256,128]{1,0:T(8,128)(2,1)S(1)} %collective-permute-done.7), channel_id=1, source_target_pairs={{0,192},{16,208},{32,224},{48,240},{64,0},{80,16},{96,32},{112,48}... | collective-permute-start | bytes 196616 | tf_op jit(solution)/shard_map/ppermute | solution.py:256
  101.1 22.8 %all_to_all.30.msgs_ref = f32[16,1,128]{2,1,0:T(1,128)S(1)} all-to-all(f32[16,1,128]{2,1,0:T(1,128)S(1)} %get-tuple-element.35), channel_id=1, replica_groups=mesh['grp'=2,'sp'=16,'x'=8,'core'=2] {'sp'}, dimensions={0} | all-to-all | bytes 16384 | tf_op jit(solution)/shard_map/all_to_all | solution.py:251
  127.3 3.6 %all-to-all-start.2 = ((bf16[8,64,256]{2,1,0:T(8,128)(2,1)}), bf16[8,64,256]{2,1,0:T(8,128)(2,1)S(1)}, u32[]{:S(2)}, u32[]{:S(2)}) async-start(bf16[8,64,256]{2,1,0:T(8,128)(2,1)} %shard_map.102), calls=%async_computation.2 | async-start | bytes 524288 | tf_op jit(solution)/shard_map/all_to_all | solution.py:251
  131.0 2.6 %collective-permute-start.11 = (bf16[4,64,128]{2,1,0:T(8,128)(2,1)S(1)}, bf16[4,64,128]{2,1,0:T(8,128)(2,1)S(1)}, u32[]{:S(2)}, u32[]{:S(2)}) collective-permute-start(bf16[4,64,128]{2,1,0:T(8,128)(2,1)S(1)} %pad_maximum_fusion.2), channel_id=1, source_target_pairs={{0,240},{1,17},{16,0},{17,33},{32,16},{33,49},{48,32},{49,65},{64,... | collective-permute-start | bytes 196616 | tf_op jit(solution)/shard_map/ppermute | solution.py:272
  133.5 3.3 %collective-permute-start.12 = (bf16[4,64,128]{2,1,0:T(8,128)(2,1)S(1)}, bf16[4,64,128]{2,1,0:T(8,128)(2,1)S(1)}, u32[]{:S(2)}, u32[]{:S(2)}) collective-permute-start(bf16[4,64,128]{2,1,0:T(8,128)(2,1)S(1)} %pad_maximum_fusion.2), channel_id=1, source_target_pairs={{0,16},{1,241},{16,32},{17,1},{32,48},{33,17},{48,64},{49,33},{64,... | collective-permute-start | bytes 196616 | tf_op jit(solution)/shard_map/ppermute | solution.py:272
  137.2 4.0 %all-to-all-done.2.mine_ref = bf16[8,64,256]{2,1,0:T(8,128)(2,1)S(1)} async-done(((bf16[8,64,256]{2,1,0:T(8,128)(2,1)}), bf16[8,64,256]{2,1,0:T(8,128)(2,1)S(1)}, u32[]{:S(2)}, u32[]{:S(2)}) %all-to-all-start.2) | async-done | bytes 262176 | tf_op jit(solution)/shard_map/all_to_all | solution.py:251
  145.8 3.7 %all-to-all-start.3 = ((bf16[8,256,128]{2,1,0:T(8,128)(2,1)}), bf16[8,256,128]{2,1,0:T(8,128)(2,1)S(1)}, u32[]{:S(2)}, u32[]{:S(2)}) async-start(bf16[8,256,128]{2,1,0:T(8,128)(2,1)} %get-tuple-element.47), calls=%async_computation.3 | async-start | bytes 1048576 | tf_op jit(solution)/shard_map/all_to_all | solution.py:251
  149.6 5.1 %collective-permute-start.14 = (bf16[4,192,128]{2,1,0:T(8,128)(2,1)S(1)}, bf16[4,192,128]{2,1,0:T(8,128)(2,1)S(1)}, u32[]{:S(2)}, u32[]{:S(2)}) collective-permute-start(bf16[4,192,128]{2,1,0:T(8,128)(2,1)S(1)} %pad_maximum_fusion), channel_id=1, source_target_pairs={{0,224},{1,33},{16,240},{17,49},{32,0},{33,65},{48,16},{49,81},{64... | collective-permute-start | bytes 589832 | tf_op jit(solution)/shard_map/ppermute | solution.py:272
  156.7 4.0 %collective-permute-start.16 = (bf16[4,192,128]{2,1,0:T(8,128)(2,1)S(1)}, bf16[4,192,128]{2,1,0:T(8,128)(2,1)S(1)}, u32[]{:S(2)}, u32[]{:S(2)}) collective-permute-start(bf16[4,192,128]{2,1,0:T(8,128)(2,1)S(1)} %pad_maximum_fusion), channel_id=1, source_target_pairs={{0,16},{1,241},{16,32},{17,1},{32,48},{33,17},{48,64},{49,33},{64,... | collective-permute-start | bytes 589832 | tf_op jit(solution)/shard_map/ppermute | solution.py:272
  160.7 3.2 %collective-permute-done.15 = bf16[4,192,128]{2,1,0:T(8,128)(2,1)S(1)} collective-permute-done((bf16[4,192,128]{2,1,0:T(8,128)(2,1)S(1)}, bf16[4,192,128]{2,1,0:T(8,128)(2,1)S(1)}, u32[]{:S(2)}, u32[]{:S(2)}) %collective-permute-start.15) | collective-permute-done | bytes 196640 | tf_op jit(solution)/shard_map/ppermute | solution.py:272
  164.0 3.4 %all-to-all-done.3.mine_ref = bf16[8,256,128]{2,1,0:T(8,128)(2,1)S(1)} async-done(((bf16[8,256,128]{2,1,0:T(8,128)(2,1)}), bf16[8,256,128]{2,1,0:T(8,128)(2,1)S(1)}, u32[]{:S(2)}, u32[]{:S(2)}) %all-to-all-start.3) | async-done | bytes 524320 | tf_op jit(solution)/shard_map/all_to_all | solution.py:251
  171.7 3.4 %collective-permute-start.17 = (bf16[64,128]{1,0:T(8,128)(2,1)S(1)}, bf16[64,128]{1,0:T(8,128)(2,1)S(1)}, u32[]{:S(2)}, u32[]{:S(2)}) collective-permute-start(bf16[64,128]{1,0:T(8,128)(2,1)S(1)} %get-tuple-element.53), channel_id=1, source_target_pairs={{0,16},{16,32},{32,48},{48,64},{64,80},{80,96},{96,112},{112,128},... | collective-permute-start | bytes 49160 | tf_op jit(solution)/shard_map/ppermute | solution.py:316
  177.7 19.3 %all_to_all.31.msgs_ref = f32[16,1,128]{2,1,0:T(1,128)S(1)} all-to-all(f32[16,1,128]{2,1,0:T(1,128)S(1)} %get-tuple-element.54), channel_id=1, replica_groups=mesh['grp'=2,'sp'=16,'x'=8,'core'=2] {'sp'}, dimensions={0} | all-to-all | bytes 16384 | tf_op jit(solution)/shard_map/all_to_all | solution.py:251
  197.1 15.2 %all_to_all.32.mine_ref = bf16[8,64,256]{2,1,0:T(8,128)(2,1)S(1)} all-to-all(bf16[8,64,256]{2,1,0:T(8,128)(2,1)S(1)} %shard_map.109), channel_id=1, replica_groups=mesh['grp'=2,'sp'=16,'x'=8,'core'=2] {'x'}, dimensions={0} | all-to-all | bytes 524288 | tf_op jit(solution)/shard_map/all_to_all | solution.py:251
  (78 shorter events, 31.7 us)
Async XLA Ops:
  1.8 43.8 %copy-start = (bf16[256,128]{1,0:T(8,128)(2,1)S(1)}, bf16[256,128]{1,0:T(8,128)(2,1)}, u32[]{:S(2)}) copy-start(bf16[256,128]{1,0:T(8,128)(2,1)} %residual_ref.1) | copy-start | bytes 196612
  1.8 81.5 %all-to-all-start = ((bf16[16,128,128]{2,1,0:T(8,128)(2,1)}), bf16[16,128,128]{2,1,0:T(8,128)(2,1)S(1)}, u32[]{:S(2)}, u32[]{:S(2)}) async-start(bf16[16,128,128]{2,1,0:T(8,128)(2,1)} %get-tuple-element.32), calls=%async_computation | async-start | bytes 1048576 | tf_op jit(solution)/shard_map/all_to_all | solution.py:251
  45.6 10.7 %collective-permute-start = (bf16[256,128]{1,0:T(8,128)(2,1)S(1)}, bf16[256,128]{1,0:T(8,128)(2,1)S(1)}, u32[]{:S(2)}, u32[]{:S(2)}) collective-permute-start(bf16[256,128]{1,0:T(8,128)(2,1)S(1)} %copy-done), channel_id=1, source_target_pairs={{0,8},{2,10},{4,12},{6,14},{8,0},{10,2},{12,4},{14,6},{1,9},{3,11}... | collective-permute-start | bytes 196616 | tf_op jit(solution)/shard_map/ppermute | solution.py:256
  56.4 12.5 %collective-permute-start.1 = (bf16[2,256,128]{2,1,0:T(8,128)(2,1)S(1)}, bf16[2,256,128]{2,1,0:T(8,128)(2,1)S(1)}, u32[]{:S(2)}, u32[]{:S(2)}) collective-permute-start(bf16[2,256,128]{2,1,0:T(8,128)(2,1)S(1)} %pad_maximum_fusion.1), channel_id=1, source_target_pairs={{0,12},{1,5},{2,14},{3,7},{4,0},{5,9},{6,2},{7,11},{8,4},{9,13},{1... | collective-permute-start | bytes 393224 | tf_op jit(solution)/shard_map/ppermute | solution.py:272
  62.9 7.6 %collective-permute-start.2 = (bf16[2,256,128]{2,1,0:T(8,128)(2,1)S(1)}, bf16[2,256,128]{2,1,0:T(8,128)(2,1)S(1)}, u32[]{:S(2)}, u32[]{:S(2)}) collective-permute-start(bf16[2,256,128]{2,1,0:T(8,128)(2,1)S(1)} %pad_maximum_fusion.1), channel_id=1, source_target_pairs={{0,14},{1,3},{2,0},{3,5},{4,2},{5,7},{6,4},{7,9},{8,6},{9,11},{10,... | collective-permute-start | bytes 393224 | tf_op jit(solution)/shard_map/ppermute | solution.py:272
  65.8 8.1 %collective-permute-start.3 = (bf16[2,256,128]{2,1,0:T(8,128)(2,1)S(1)}, bf16[2,256,128]{2,1,0:T(8,128)(2,1)S(1)}, u32[]{:S(2)}, u32[]{:S(2)}) collective-permute-start(bf16[2,256,128]{2,1,0:T(8,128)(2,1)S(1)} %pad_maximum_fusion.1), channel_id=1, source_target_pairs={{0,2},{1,15},{2,4},{3,1},{4,6},{5,3},{6,8},{7,5},{8,10},{9,7},{10,... | collective-permute-start | bytes 393224 | tf_op jit(solution)/shard_map/ppermute | solution.py:272
  70.6 12.6 %copy-start.6 = (f32[2,2048]{1,0:T(2,128)S(1)}, f32[2,2048]{1,0:T(2,128)}, u32[]{:S(2)}) copy-start(f32[2,2048]{1,0:T(2,128)} %param.11) | copy-start | bytes 49156
  73.9 9.3 %collective-permute-start.4 = (bf16[8,256,128]{2,1,0:T(8,128)(2,1)S(1)}, bf16[8,256,128]{2,1,0:T(8,128)(2,1)S(1)}, u32[]{:S(2)}, u32[]{:S(2)}) collective-permute-start(bf16[8,256,128]{2,1,0:T(8,128)(2,1)S(1)} %constant_dynamic-update-slice_fusion.mine_ref), channel_id=1, source_target_pairs={{0,1},{1,0},{2,3},{3,2},{4,5},{5,4},{6,7},{7,6},{8,9},{9,8},{10,11... | collective-permute-start | bytes 1572872 | tf_op jit(solution)/shard_map/ppermute | solution.py:256
  75.9 14.3 %collective-permute-start.7 = (bf16[256,128]{1,0:T(8,128)(2,1)S(1)}, bf16[256,128]{1,0:T(8,128)(2,1)S(1)}, u32[]{:S(2)}, u32[]{:S(2)}) collective-permute-start(bf16[256,128]{1,0:T(8,128)(2,1)S(1)} %get-tuple-element.48), channel_id=1, source_target_pairs={{0,192},{16,208},{32,224},{48,240},{64,0},{80,16},{96,32},{112,48}... | collective-permute-start | bytes 196616 | tf_op jit(solution)/shard_map/ppermute | solution.py:256
  83.8 3.9 %collective-permute-start.5 = (bf16[64,128]{1,0:T(8,128)(2,1)S(1)}, bf16[64,128]{1,0:T(8,128)(2,1)S(1)}, u32[]{:S(2)}, u32[]{:S(2)}) collective-permute-start(bf16[64,128]{1,0:T(8,128)(2,1)S(1)} %get-tuple-element.34), channel_id=1, source_target_pairs={{0,16},{16,32},{32,48},{48,64},{64,80},{80,96},{96,112},{112,128},... | collective-permute-start | bytes 49160 | tf_op jit(solution)/shard_map/ppermute | solution.py:316
  90.2 34.6 %collective-permute-start.8 = (bf16[256,128]{1,0:T(8,128)(2,1)S(1)}, bf16[256,128]{1,0:T(8,128)(2,1)S(1)}, u32[]{:S(2)}, u32[]{:S(2)}) collective-permute-start(bf16[256,128]{1,0:T(8,128)(2,1)S(1)} %get-tuple-element.48), channel_id=1, source_target_pairs={{0,64},{16,80},{32,96},{48,112},{64,128},{80,144},{96,160},{112,17... | collective-permute-start | bytes 196616 | tf_op jit(solution)/shard_map/ppermute | solution.py:256
  97.7 27.1 %collective-permute-start.9 = (bf16[256,128]{1,0:T(8,128)(2,1)S(1)}, bf16[256,128]{1,0:T(8,128)(2,1)S(1)}, u32[]{:S(2)}, u32[]{:S(2)}) collective-permute-start(bf16[256,128]{1,0:T(8,128)(2,1)S(1)} %collective-permute-done.7), channel_id=1, source_target_pairs={{0,192},{16,208},{32,224},{48,240},{64,0},{80,16},{96,32},{112,48}... | collective-permute-start | bytes 196616 | tf_op jit(solution)/shard_map/ppermute | solution.py:256
  124.8 12.0 %collective-permute-start.10 = (bf16[4,64,128]{2,1,0:T(8,128)(2,1)S(1)}, bf16[4,64,128]{2,1,0:T(8,128)(2,1)S(1)}, u32[]{:S(2)}, u32[]{:S(2)}) collective-permute-start(bf16[4,64,128]{2,1,0:T(8,128)(2,1)S(1)} %pad_maximum_fusion.2), channel_id=1, source_target_pairs={{0,224},{1,33},{16,240},{17,49},{32,0},{33,65},{48,16},{49,81},{64... | collective-permute-start | bytes 196616 | tf_op jit(solution)/shard_map/ppermute | solution.py:272
  127.3 13.9 %all-to-all-start.2 = ((bf16[8,64,256]{2,1,0:T(8,128)(2,1)}), bf16[8,64,256]{2,1,0:T(8,128)(2,1)S(1)}, u32[]{:S(2)}, u32[]{:S(2)}) async-start(bf16[8,64,256]{2,1,0:T(8,128)(2,1)} %shard_map.102), calls=%async_computation.2 | async-start | bytes 524288 | tf_op jit(solution)/shard_map/all_to_all | solution.py:251
  131.0 6.2 %collective-permute-start.11 = (bf16[4,64,128]{2,1,0:T(8,128)(2,1)S(1)}, bf16[4,64,128]{2,1,0:T(8,128)(2,1)S(1)}, u32[]{:S(2)}, u32[]{:S(2)}) collective-permute-start(bf16[4,64,128]{2,1,0:T(8,128)(2,1)S(1)} %pad_maximum_fusion.2), channel_id=1, source_target_pairs={{0,240},{1,17},{16,0},{17,33},{32,16},{33,49},{48,32},{49,65},{64,... | collective-permute-start | bytes 196616 | tf_op jit(solution)/shard_map/ppermute | solution.py:272
  133.5 9.6 %collective-permute-start.12 = (bf16[4,64,128]{2,1,0:T(8,128)(2,1)S(1)}, bf16[4,64,128]{2,1,0:T(8,128)(2,1)S(1)}, u32[]{:S(2)}, u32[]{:S(2)}) collective-permute-start(bf16[4,64,128]{2,1,0:T(8,128)(2,1)S(1)} %pad_maximum_fusion.2), channel_id=1, source_target_pairs={{0,16},{1,241},{16,32},{17,1},{32,48},{33,17},{48,64},{49,33},{64,... | collective-permute-start | bytes 196616 | tf_op jit(solution)/shard_map/ppermute | solution.py:272
  141.2 3.4 %collective-permute-start.6 = (bf16[8,64,256]{2,1,0:T(8,128)(2,1)S(1)}, bf16[8,64,256]{2,1,0:T(8,128)(2,1)S(1)}, u32[]{:S(2)}, u32[]{:S(2)}) collective-permute-start(bf16[8,64,256]{2,1,0:T(8,128)(2,1)S(1)} %all-to-all-done.2.mine_ref), channel_id=1, source_target_pairs={{0,1},{1,0},{2,3},{3,2},{4,5},{5,4},{6,7},{7,6},{8,9},{9,8},{10,11... | collective-permute-start | bytes 786440 | tf_op jit(solution)/shard_map/ppermute | solution.py:256
  145.8 21.5 %all-to-all-start.3 = ((bf16[8,256,128]{2,1,0:T(8,128)(2,1)}), bf16[8,256,128]{2,1,0:T(8,128)(2,1)S(1)}, u32[]{:S(2)}, u32[]{:S(2)}) async-start(bf16[8,256,128]{2,1,0:T(8,128)(2,1)} %get-tuple-element.47), calls=%async_computation.3 | async-start | bytes 1048576 | tf_op jit(solution)/shard_map/all_to_all | solution.py:251
  149.6 11.1 %collective-permute-start.14 = (bf16[4,192,128]{2,1,0:T(8,128)(2,1)S(1)}, bf16[4,192,128]{2,1,0:T(8,128)(2,1)S(1)}, u32[]{:S(2)}, u32[]{:S(2)}) collective-permute-start(bf16[4,192,128]{2,1,0:T(8,128)(2,1)S(1)} %pad_maximum_fusion), channel_id=1, source_target_pairs={{0,224},{1,33},{16,240},{17,49},{32,0},{33,65},{48,16},{49,81},{64... | collective-permute-start | bytes 589832 | tf_op jit(solution)/shard_map/ppermute | solution.py:272
  154.7 9.2 %collective-permute-start.15 = (bf16[4,192,128]{2,1,0:T(8,128)(2,1)S(1)}, bf16[4,192,128]{2,1,0:T(8,128)(2,1)S(1)}, u32[]{:S(2)}, u32[]{:S(2)}) collective-permute-start(bf16[4,192,128]{2,1,0:T(8,128)(2,1)S(1)} %pad_maximum_fusion), channel_id=1, source_target_pairs={{0,240},{1,17},{16,0},{17,33},{32,16},{33,49},{48,32},{49,65},{64,... | collective-permute-start | bytes 589832 | tf_op jit(solution)/shard_map/ppermute | solution.py:272
  156.7 12.6 %collective-permute-start.16 = (bf16[4,192,128]{2,1,0:T(8,128)(2,1)S(1)}, bf16[4,192,128]{2,1,0:T(8,128)(2,1)S(1)}, u32[]{:S(2)}, u32[]{:S(2)}) collective-permute-start(bf16[4,192,128]{2,1,0:T(8,128)(2,1)S(1)} %pad_maximum_fusion), channel_id=1, source_target_pairs={{0,16},{1,241},{16,32},{17,1},{32,48},{33,17},{48,64},{49,33},{64,... | collective-permute-start | bytes 589832 | tf_op jit(solution)/shard_map/ppermute | solution.py:272
  167.3 3.8 %collective-permute-start.13 = (bf16[8,256,128]{2,1,0:T(8,128)(2,1)S(1)}, bf16[8,256,128]{2,1,0:T(8,128)(2,1)S(1)}, u32[]{:S(2)}, u32[]{:S(2)}) collective-permute-start(bf16[8,256,128]{2,1,0:T(8,128)(2,1)S(1)} %all-to-all-done.3.mine_ref), channel_id=1, source_target_pairs={{0,1},{1,0},{2,3},{3,2},{4,5},{5,4},{6,7},{7,6},{8,9},{9,8},{10,11... | collective-permute-start | bytes 1572872 | tf_op jit(solution)/shard_map/ppermute | solution.py:256
  171.7 4.9 %collective-permute-start.17 = (bf16[64,128]{1,0:T(8,128)(2,1)S(1)}, bf16[64,128]{1,0:T(8,128)(2,1)S(1)}, u32[]{:S(2)}, u32[]{:S(2)}) collective-permute-start(bf16[64,128]{1,0:T(8,128)(2,1)S(1)} %get-tuple-element.53), channel_id=1, source_target_pairs={{0,16},{16,32},{32,48},{48,64},{64,80},{80,96},{96,112},{112,128},... | collective-permute-start | bytes 49160 | tf_op jit(solution)/shard_map/ppermute | solution.py:316
  212.3 3.4 %collective-permute-start.18 = (bf16[8,64,256]{2,1,0:T(8,128)(2,1)S(1)}, bf16[8,64,256]{2,1,0:T(8,128)(2,1)S(1)}, u32[]{:S(2)}, u32[]{:S(2)}) collective-permute-start(bf16[8,64,256]{2,1,0:T(8,128)(2,1)S(1)} %all_to_all.32.mine_ref), channel_id=1, source_target_pairs={{0,1},{1,0},{2,3},{3,2},{4,5},{5,4},{6,7},{7,6},{8,9},{9,8},{10,11... | collective-permute-start | bytes 786440 | tf_op jit(solution)/shard_map/ppermute | solution.py:256
  (5 other events, 22.0 us)

commit v8 on v7

--- a/solution.py
+++ b/solution.py
@@ -12,6 +12,7 @@
 EPS = 1e-06
 RATE_SCALE = 8.0
 LANES = 128
+HALO = 16
 NEAR = (-2, -1, 0, 1)
 
 
@@ -118,31 +119,43 @@
 
 
 def project_kernel(
-    slotted, hopped, mine_ref, theirs_ref, gain_ref, weight_ref, value_ref, gate_ref, tail_ref
+    slotted, hopped, mine_ref, theirs_ref, gain_ref, weight_ref, value_ref, gate_ref, edge_ref
 ):
-    chips, tok, width = mine_ref.shape
-    channels = value_ref.shape[0]
-    product = jnp.zeros((2 * channels, tok), jnp.float32)
-    squares = jnp.zeros((tok, width), jnp.float32)
+    chips, held_rows, width = mine_ref.shape
+    channels, tok = value_ref.shape
+    extra = held_rows - tok
     pieces = (mine_ref, theirs_ref)
-    for side in range(2):
-        for slot in range(chips):
-            block = piece_block(side, slot, chips, slotted)
-            held = weight_slot(block, weight_ref.shape[0], hopped)
-            wide = pieces[side][slot].astype(jnp.float32)
-            squares += wide * wide
-            scaled = (wide * gain_ref[block]).astype(jnp.bfloat16)
-            product += lax.dot_general(
-                weight_ref[held, : 2 * channels, :],
-                scaled,
-                (((1,), (1,)), ((), ())),
-                preferred_element_type=jnp.float32,
-            )
-    mean = jnp.sum(squares.T, axis=0, keepdims=True) * (1.0 / (2 * chips * width))
-    rows = (product * lax.rsqrt(mean + EPS)).astype(jnp.bfloat16)
+
+    def project(rows_of, count):
+        product = jnp.zeros((2 * channels, count), jnp.float32)
+        squares = jnp.zeros((count, width), jnp.float32)
+        for side in range(2):
+            for slot in range(chips):
+                block = piece_block(side, slot, chips, slotted)
+                held = weight_slot(block, weight_ref.shape[0], hopped)
+                wide = rows_of(pieces[side], slot).astype(jnp.float32)
+                squares += wide * wide
+                scaled = (wide * gain_ref[block]).astype(jnp.bfloat16)
+                product += lax.dot_general(
+                    weight_ref[held, : 2 * channels, :],
+                    scaled,
+                    (((1,), (1,)), ((), ())),
+                    preferred_element_type=jnp.float32,
+                )
+        mean = jnp.sum(squares.T, axis=0, keepdims=True) * (1.0 / (2 * chips * width))
+        return (product * lax.rsqrt(mean + EPS)).astype(jnp.bfloat16)
+
+    rows = project(lambda ref, slot: ref[slot, extra:, :], tok)
     value_ref[...] = rows[:channels]
     gate_ref[...] = rows[channels:]
-    tail_ref[...] = rows[:channels, tok - LANES :]
+    if extra:
+        blank = jnp.zeros((LANES - extra, width), jnp.bfloat16)
+        edge = project(
+            lambda ref, slot: jnp.concatenate([blank, ref[slot, :extra, :]], axis=0), LANES
+        )
+        edge_ref[...] = edge[:channels]
+    else:
+        edge_ref[...] = rows[:channels, tok - LANES :]
 
 
 def mix_kernel(mine_ref, theirs_ref, weight_ref, residual_ref, out_ref, *copies_ref):
@@ -162,7 +175,7 @@
         ref[...] = jnp.broadcast_to(mixed[None], ref.shape)
 
 
-def pack_kernel(value_ref, gate_ref, mix_ref, first_ref, later_ref, sems):
+def pack_kernel(value_ref, gate_ref, mix_ref, tokens_ref, first_ref, later_ref, last_ref, sems):
     layers, channels, _ = value_ref.shape
     shards = [ref.at[layer] for layer in range(layers) for ref in (value_ref, gate_ref, mix_ref)]
     moves = []
@@ -170,6 +183,9 @@
         rows_ref, at = (first_ref.at[0], k) if k < 2 else (later_ref, k - 2)
         target = rows_ref.at[pl.ds(at * channels, channels)]
         moves.append(pltpu.make_async_copy(shard_ref, target, sems.at[k]))
+    last = last_ref.shape[0]
+    source = tokens_ref.at[pl.ds(tokens_ref.shape[0] - last, last)]
+    moves.append(pltpu.make_async_copy(source, last_ref, sems.at[len(shards)]))
     for move in moves:
         move.start()
     for move in moves:
@@ -189,25 +205,25 @@
     )(*(pltpu.with_memory_space_constraint(a, pltpu.VMEM) for a in operands))
 
 
-def pack_call(value_proj, gate_proj, mix_proj, count):
+def pack_call(value_proj, gate_proj, mix_proj, tokens, count):
     layers, channels, width = value_proj.shape
     dtype = value_proj.dtype
     out = [
         pltpu.VMEM((count, 2 * channels, width), dtype),
         pltpu.VMEM(((3 * layers - 2) * channels, width), dtype),
+        pltpu.VMEM((HALO, tokens.shape[1]), tokens.dtype),
     ]
     return pl.pallas_call(
         pack_kernel,
         out_shape=out,
-        in_specs=[pl.BlockSpec(memory_space=pl.ANY)] * 3,
+        in_specs=[pl.BlockSpec(memory_space=pl.ANY)] * 4,
         out_specs=vmem(len(out)),
-        scratch_shapes=[pltpu.SemaphoreType.DMA((3 * layers,))],
+        scratch_shapes=[pltpu.SemaphoreType.DMA((3 * layers + 1,))],
         name="pack",
-    )(value_proj, gate_proj, mix_proj)
-
-
-def project_call(slotted, hopped, mine, theirs, gains, weights, channels):
-    _, tok, _ = mine.shape
+    )(value_proj, gate_proj, mix_proj, tokens)
+
+
+def project_call(slotted, hopped, mine, theirs, gains, weights, channels, tok):
     out = [pltpu.VMEM((channels, n), jnp.bfloat16) for n in (tok, tok, LANES)]
     kernel = functools.partial(project_kernel, slotted, hopped)
     return kernel_call(kernel, out, mine, theirs, gains, weights)
@@ -286,18 +302,22 @@
     decay_offset,
     mix_proj,
 ):
-    own_cols, channels = tokens.shape[1], value_proj.shape[1]
+    (tok_rows, own_cols), channels = tokens.shape, value_proj.shape[1]
     chips, cores, count = (lax.axis_size(name) for name in ("x", "core", "sp"))
 
     def swap(array):
         return shift(array, "core", 1)
 
-    far_tokens = far_hop(tokens, "x")
-    first, shard = pack_call(value_proj, gate_proj, mix_proj, count)
+    def to_next(array):
+        return lax.ppermute(array, "sp", [(i, i + 1) for i in range(count - 1)])
+
+    first, shard, last = pack_call(value_proj, gate_proj, mix_proj, tokens, count)
+    last = to_next(last)
     weights = exchange(first, "sp")
-    mine = near_hops(jnp.stack([tokens, far_tokens]), "x")
-    _, shard = lax.optimization_barrier((mine, shard))
+    held = jnp.concatenate([last, tokens], axis=0)
+    held = jnp.stack([held, far_hop(held, "x")])
     hop_one = far_hop(shard, "sp", -1)
+    mine = near_hops(held, "x")
     gains = [gain.reshape(chips * cores, 1, own_cols) for gain in norm_gain]
     gains[1] = copy_call(gains[1])
     gains[1] = copy_call(gains[1])
@@ -310,14 +330,15 @@
             mine = exchange(copies[0], "x")
             weights = later_weights
         theirs = swap(mine)
-        value_rows, gate_rows, tail = project_call(
-            layer == 0, layer > 0, mine, theirs, gains[layer], weights, channels
+        value_rows, gate_rows, edge = project_call(
+            layer == 0, layer > 0, mine, theirs, gains[layer], weights, channels, tok_rows
         )
-        before = lax.ppermute(tail, "sp", [(i, i + 1) for i in range(count - 1)])
+        if layer:
+            edge = to_next(edge)
         cum, state, msg = scan_call(
             layer,
             value_rows,
-            before,
+            edge,
             conv_taps,
             decay_param,
             recur_map,

time: 219 us -> 240 us (1.096)
  starting transfers between devices: 123 us -> 134 us
  waiting for transfers between devices: 27.5 us -> 38.2 us
    ppermute x2, waiting for transfers between devices: 2.85 us -> 14.5 us  [to_next(): return lax.ppermute(array, 'sp', [(i, i + 1) for i in range(count - 1)])]
    ppermute x8, starting transfers between devices: 33.9 us -> 44.3 us  [shift(): lax.ppermute(array, axis, [(i, (i + steps) % count) for i in range(count)])]
  transfers between devices with their start and end apart: 22 -> 22, of which waited for: 13 -> 12; matrix products, arithmetic and copies ran while one was open for 0% -> 0% of each run, Pallas kernels for 1% -> 1%
where the time goes in v8:
time: 240 us; the launch traced here: 238 us
  starting transfers between devices  134 us (56%)
  blocking collectives  55.7 us (23%)
  waiting for transfers between devices  38.2 us (16%)
  Pallas kernels  8.5 us (4%)
    all_to_all x3, blocking collectives, exchange(): return lax.all_to_all(copies, axis, split_axis=0, concat_axis=0, tiled=True)  55.7 us
    all_to_all x3, starting transfers between devices, exchange(): return lax.all_to_all(copies, axis, split_axis=0, concat_axis=0, tiled=True)  51.1 us
    ppermute x8, starting transfers between devices, shift(): lax.ppermute(array, axis, [(i, (i + steps) % count) for i in range(count)])  44.3 us
    ppermute x9, starting transfers between devices, hop(): return lax.ppermute(held, (axis, 'core'), pairs)  31.5 us
    ppermute x2, waiting for transfers between devices, to_next(): return lax.ppermute(array, 'sp', [(i, i + 1) for i in range(count - 1)])  14.5 us
    ppermute x9, waiting for transfers between devices, hop(): return lax.ppermute(held, (axis, 'core'), pairs)  9.02 us
    ppermute x8, waiting for transfers between devices, shift(): lax.ppermute(array, axis, [(i, (i + steps) % count) for i in range(count)])  7.32 us
    all_to_all x3, waiting for transfers between devices, exchange(): return lax.all_to_all(copies, axis, split_axis=0, concat_axis=0, tiled=True)  7.31 us
  transfers between devices with their start and end apart: 22, of which 12 were waited for; matrix products, arithmetic and copies ran while one was open for 0% of the time, Pallas kernels for 1%

profile of v8, /device:TPU:80, one launch (start us, length us, event | category | flops | bytes accessed | tf_op | source)
XLA Modules:
  0.0 238.0 jit_solution(1644750920062511208)
XLA Ops:
  1.8 43.8 %all-to-all-start = ((bf16[16,128,128]{2,1,0:T(8,128)(2,1)}), bf16[16,128,128]{2,1,0:T(8,128)(2,1)S(1)}, u32[]{:S(2)}, u32[]{:S(2)}) async-start(bf16[16,128,128]{2,1,0:T(8,128)(2,1)} %get-tuple-element.33), calls=%async_computation | async-start | bytes 1048576 | tf_op jit(solution)/shard_map/all_to_all | solution.py:267
  45.6 3.6 %collective-permute-start = (bf16[16,128]{1,0:T(8,128)(2,1)S(1)}, bf16[16,128]{1,0:T(8,128)(2,1)S(1)}, u32[]{:S(2)}, u32[]{:S(2)}) collective-permute-start(bf16[16,128]{1,0:T(8,128)(2,1)S(1)} %get-tuple-element.32), channel_id=1, source_target_pairs={{0,16},{16,32},{32,48},{48,64},{64,80},{80,96},{96,112},{112,128},... | collective-permute-start | bytes 12296 | tf_op jit(solution)/shard_map/ppermute | solution.py:312
  49.3 13.1 %collective-permute-done = bf16[16,128]{1,0:T(8,128)(2,1)S(1)} collective-permute-done((bf16[16,128]{1,0:T(8,128)(2,1)S(1)}, bf16[16,128]{1,0:T(8,128)(2,1)S(1)}, u32[]{:S(2)}, u32[]{:S(2)}) %collective-permute-start) | collective-permute-done | bytes 4128 | tf_op jit(solution)/shard_map/ppermute | solution.py:312
  62.4 8.0 %collective-permute-start.1 = (bf16[272,128]{1,0:T(8,128)(2,1)S(1)}, bf16[272,128]{1,0:T(8,128)(2,1)S(1)}, u32[]{:S(2)}, u32[]{:S(2)}) collective-permute-start(bf16[272,128]{1,0:T(8,128)(2,1)S(1)} %constant_dynamic-update-slice_fusion), channel_id=1, source_target_pairs={{0,8},{2,10},{4,12},{6,14},{8,0},{10,2},{12,4},{14,6},{1,9},{3,11}... | collective-permute-start | bytes 208904 | tf_op jit(solution)/shard_map/ppermute | solution.py:272
  70.4 2.6 %collective-permute-done.1 = bf16[272,128]{1,0:T(8,128)(2,1)S(1)} collective-permute-done((bf16[272,128]{1,0:T(8,128)(2,1)S(1)}, bf16[272,128]{1,0:T(8,128)(2,1)S(1)}, u32[]{:S(2)}, u32[]{:S(2)}) %collective-permute-start.1) | collective-permute-done | bytes 69664 | tf_op jit(solution)/shard_map/ppermute | solution.py:272
  72.9 6.1 %collective-permute-start.2 = (bf16[2,272,128]{2,1,0:T(8,128)(2,1)S(1)}, bf16[2,272,128]{2,1,0:T(8,128)(2,1)S(1)}, u32[]{:S(2)}, u32[]{:S(2)}) collective-permute-start(bf16[2,272,128]{2,1,0:T(8,128)(2,1)S(1)} %pad_maximum_fusion.1), channel_id=1, source_target_pairs={{0,12},{1,5},{2,14},{3,7},{4,0},{5,9},{6,2},{7,11},{8,4},{9,13},{1... | collective-permute-start | bytes 417800 | tf_op jit(solution)/shard_map/ppermute | solution.py:288
  79.0 3.3 %collective-permute-start.3 = (bf16[2,272,128]{2,1,0:T(8,128)(2,1)S(1)}, bf16[2,272,128]{2,1,0:T(8,128)(2,1)S(1)}, u32[]{:S(2)}, u32[]{:S(2)}) collective-permute-start(bf16[2,272,128]{2,1,0:T(8,128)(2,1)S(1)} %pad_maximum_fusion.1), channel_id=1, source_target_pairs={{0,14},{1,3},{2,0},{3,5},{4,2},{5,7},{6,4},{7,9},{8,6},{9,11},{10,... | collective-permute-start | bytes 417800 | tf_op jit(solution)/shard_map/ppermute | solution.py:288
  82.3 2.6 %collective-permute-start.4 = (bf16[2,272,128]{2,1,0:T(8,128)(2,1)S(1)}, bf16[2,272,128]{2,1,0:T(8,128)(2,1)S(1)}, u32[]{:S(2)}, u32[]{:S(2)}) collective-permute-start(bf16[2,272,128]{2,1,0:T(8,128)(2,1)S(1)} %pad_maximum_fusion.1), channel_id=1, source_target_pairs={{0,2},{1,15},{2,4},{3,1},{4,6},{5,3},{6,8},{7,5},{8,10},{9,7},{10,... | collective-permute-start | bytes 417800 | tf_op jit(solution)/shard_map/ppermute | solution.py:288
  86.2 4.3 %collective-permute-done.4 = bf16[2,272,128]{2,1,0:T(8,128)(2,1)S(1)} collective-permute-done((bf16[2,272,128]{2,1,0:T(8,128)(2,1)S(1)}, bf16[2,272,128]{2,1,0:T(8,128)(2,1)S(1)}, u32[]{:S(2)}, u32[]{:S(2)}) %collective-permute-start.4) | collective-permute-done | bytes 139296 | tf_op jit(solution)/shard_map/ppermute | solution.py:288
  92.5 15.0 %collective-permute-start.7 = (bf16[256,128]{1,0:T(8,128)(2,1)S(1)}, bf16[256,128]{1,0:T(8,128)(2,1)S(1)}, u32[]{:S(2)}, u32[]{:S(2)}) collective-permute-start(bf16[256,128]{1,0:T(8,128)(2,1)S(1)} %get-tuple-element.48), channel_id=1, source_target_pairs={{0,192},{16,208},{32,224},{48,240},{64,0},{80,16},{96,32},{112,48}... | collective-permute-start | bytes 196616 | tf_op jit(solution)/shard_map/ppermute | solution.py:272
  110.3 11.6 %collective-permute-start.8 = (bf16[256,128]{1,0:T(8,128)(2,1)S(1)}, bf16[256,128]{1,0:T(8,128)(2,1)S(1)}, u32[]{:S(2)}, u32[]{:S(2)}) collective-permute-start(bf16[256,128]{1,0:T(8,128)(2,1)S(1)} %get-tuple-element.48), channel_id=1, source_target_pairs={{0,64},{16,80},{32,96},{48,112},{64,128},{80,144},{96,160},{112,17... | collective-permute-start | bytes 196616 | tf_op jit(solution)/shard_map/ppermute | solution.py:272
  123.8 21.3 %all_to_all.30.msgs_ref = f32[16,1,128]{2,1,0:T(1,128)S(1)} all-to-all(f32[16,1,128]{2,1,0:T(1,128)S(1)} %get-tuple-element.36), channel_id=1, replica_groups=mesh['grp'=2,'sp'=16,'x'=8,'core'=2] {'sp'}, dimensions={0} | all-to-all | bytes 16384 | tf_op jit(solution)/shard_map/all_to_all | solution.py:267
  146.0 2.6 %collective-permute-start.10 = (bf16[4,64,128]{2,1,0:T(8,128)(2,1)S(1)}, bf16[4,64,128]{2,1,0:T(8,128)(2,1)S(1)}, u32[]{:S(2)}, u32[]{:S(2)}) collective-permute-start(bf16[4,64,128]{2,1,0:T(8,128)(2,1)S(1)} %pad_maximum_fusion.2), channel_id=1, source_target_pairs={{0,224},{1,33},{16,240},{17,49},{32,0},{33,65},{48,16},{49,81},{64... | collective-permute-start | bytes 196616 | tf_op jit(solution)/shard_map/ppermute | solution.py:288
  148.6 3.6 %all-to-all-start.2 = ((bf16[8,64,256]{2,1,0:T(8,128)(2,1)}), bf16[8,64,256]{2,1,0:T(8,128)(2,1)S(1)}, u32[]{:S(2)}, u32[]{:S(2)}) async-start(bf16[8,64,256]{2,1,0:T(8,128)(2,1)} %shard_map.102), calls=%async_computation.2 | async-start | bytes 524288 | tf_op jit(solution)/shard_map/all_to_all | solution.py:267
  154.7 3.4 %collective-permute-start.12 = (bf16[4,64,128]{2,1,0:T(8,128)(2,1)S(1)}, bf16[4,64,128]{2,1,0:T(8,128)(2,1)S(1)}, u32[]{:S(2)}, u32[]{:S(2)}) collective-permute-start(bf16[4,64,128]{2,1,0:T(8,128)(2,1)S(1)} %pad_maximum_fusion.2), channel_id=1, source_target_pairs={{0,16},{1,241},{16,32},{17,1},{32,48},{33,17},{48,64},{49,33},{64,... | collective-permute-start | bytes 196616 | tf_op jit(solution)/shard_map/ppermute | solution.py:288
  158.5 4.0 %all-to-all-done.2.mine_ref = bf16[8,64,256]{2,1,0:T(8,128)(2,1)S(1)} async-done(((bf16[8,64,256]{2,1,0:T(8,128)(2,1)}), bf16[8,64,256]{2,1,0:T(8,128)(2,1)S(1)}, u32[]{:S(2)}, u32[]{:S(2)}) %all-to-all-start.2) | async-done | bytes 262176 | tf_op jit(solution)/shard_map/all_to_all | solution.py:267
  167.1 3.7 %all-to-all-start.3 = ((bf16[8,256,128]{2,1,0:T(8,128)(2,1)}), bf16[8,256,128]{2,1,0:T(8,128)(2,1)S(1)}, u32[]{:S(2)}, u32[]{:S(2)}) async-start(bf16[8,256,128]{2,1,0:T(8,128)(2,1)} %get-tuple-element.47), calls=%async_computation.3 | async-start | bytes 1048576 | tf_op jit(solution)/shard_map/all_to_all | solution.py:267
  170.9 5.1 %collective-permute-start.14 = (bf16[4,192,128]{2,1,0:T(8,128)(2,1)S(1)}, bf16[4,192,128]{2,1,0:T(8,128)(2,1)S(1)}, u32[]{:S(2)}, u32[]{:S(2)}) collective-permute-start(bf16[4,192,128]{2,1,0:T(8,128)(2,1)S(1)} %pad_maximum_fusion), channel_id=1, source_target_pairs={{0,224},{1,33},{16,240},{17,49},{32,0},{33,65},{48,16},{49,81},{64... | collective-permute-start | bytes 589832 | tf_op jit(solution)/shard_map/ppermute | solution.py:288
  178.0 4.0 %collective-permute-start.16 = (bf16[4,192,128]{2,1,0:T(8,128)(2,1)S(1)}, bf16[4,192,128]{2,1,0:T(8,128)(2,1)S(1)}, u32[]{:S(2)}, u32[]{:S(2)}) collective-permute-start(bf16[4,192,128]{2,1,0:T(8,128)(2,1)S(1)} %pad_maximum_fusion), channel_id=1, source_target_pairs={{0,16},{1,241},{16,32},{17,1},{32,48},{33,17},{48,64},{49,33},{64,... | collective-permute-start | bytes 589832 | tf_op jit(solution)/shard_map/ppermute | solution.py:288
  182.0 3.3 %collective-permute-done.15 = bf16[4,192,128]{2,1,0:T(8,128)(2,1)S(1)} collective-permute-done((bf16[4,192,128]{2,1,0:T(8,128)(2,1)S(1)}, bf16[4,192,128]{2,1,0:T(8,128)(2,1)S(1)}, u32[]{:S(2)}, u32[]{:S(2)}) %collective-permute-start.15) | collective-permute-done | bytes 196640 | tf_op jit(solution)/shard_map/ppermute | solution.py:288
  185.3 3.3 %all-to-all-done.3.mine_ref = bf16[8,256,128]{2,1,0:T(8,128)(2,1)S(1)} async-done(((bf16[8,256,128]{2,1,0:T(8,128)(2,1)}), bf16[8,256,128]{2,1,0:T(8,128)(2,1)S(1)}, u32[]{:S(2)}, u32[]{:S(2)}) %all-to-all-start.3) | async-done | bytes 524320 | tf_op jit(solution)/shard_map/all_to_all | solution.py:267
  193.0 3.4 %collective-permute-start.17 = (bf16[64,128]{1,0:T(8,128)(2,1)S(1)}, bf16[64,128]{1,0:T(8,128)(2,1)S(1)}, u32[]{:S(2)}, u32[]{:S(2)}) collective-permute-start(bf16[64,128]{1,0:T(8,128)(2,1)S(1)} %get-tuple-element.53), channel_id=1, source_target_pairs={{0,16},{16,32},{32,48},{48,64},{64,80},{80,96},{96,112},{112,128},... | collective-permute-start | bytes 49160 | tf_op jit(solution)/shard_map/ppermute | solution.py:312
  198.9 19.3 %all_to_all.31.msgs_ref = f32[16,1,128]{2,1,0:T(1,128)S(1)} all-to-all(f32[16,1,128]{2,1,0:T(1,128)S(1)} %get-tuple-element.54), channel_id=1, replica_groups=mesh['grp'=2,'sp'=16,'x'=8,'core'=2] {'sp'}, dimensions={0} | all-to-all | bytes 16384 | tf_op jit(solution)/shard_map/all_to_all | solution.py:267
  218.4 15.2 %all_to_all.32.mine_ref = bf16[8,64,256]{2,1,0:T(8,128)(2,1)S(1)} all-to-all(bf16[8,64,256]{2,1,0:T(8,128)(2,1)S(1)} %shard_map.109), channel_id=1, replica_groups=mesh['grp'=2,'sp'=16,'x'=8,'core'=2] {'x'}, dimensions={0} | all-to-all | bytes 524288 | tf_op jit(solution)/shard_map/all_to_all | solution.py:267
  (80 shorter events, 31.4 us)
Async XLA Ops:
  1.8 60.6 %copy-start = (bf16[256,128]{1,0:T(8,128)(2,1)S(1)}, bf16[256,128]{1,0:T(8,128)(2,1)}, u32[]{:S(2)}) copy-start(bf16[256,128]{1,0:T(8,128)(2,1)} %residual_ref.1) | copy-start | bytes 196612
  1.8 105.8 %all-to-all-start = ((bf16[16,128,128]{2,1,0:T(8,128)(2,1)}), bf16[16,128,128]{2,1,0:T(8,128)(2,1)S(1)}, u32[]{:S(2)}, u32[]{:S(2)}) async-start(bf16[16,128,128]{2,1,0:T(8,128)(2,1)} %get-tuple-element.33), calls=%async_computation | async-start | bytes 1048576 | tf_op jit(solution)/shard_map/all_to_all | solution.py:267
  45.6 16.7 %collective-permute-start = (bf16[16,128]{1,0:T(8,128)(2,1)S(1)}, bf16[16,128]{1,0:T(8,128)(2,1)S(1)}, u32[]{:S(2)}, u32[]{:S(2)}) collective-permute-start(bf16[16,128]{1,0:T(8,128)(2,1)S(1)} %get-tuple-element.32), channel_id=1, source_target_pairs={{0,16},{16,32},{32,48},{48,64},{64,80},{80,96},{96,112},{112,128},... | collective-permute-start | bytes 12296 | tf_op jit(solution)/shard_map/ppermute | solution.py:312
  62.4 10.5 %collective-permute-start.1 = (bf16[272,128]{1,0:T(8,128)(2,1)S(1)}, bf16[272,128]{1,0:T(8,128)(2,1)S(1)}, u32[]{:S(2)}, u32[]{:S(2)}) collective-permute-start(bf16[272,128]{1,0:T(8,128)(2,1)S(1)} %constant_dynamic-update-slice_fusion), channel_id=1, source_target_pairs={{0,8},{2,10},{4,12},{6,14},{8,0},{10,2},{12,4},{14,6},{1,9},{3,11}... | collective-permute-start | bytes 208904 | tf_op jit(solution)/shard_map/ppermute | solution.py:272
  72.9 12.0 %collective-permute-start.2 = (bf16[2,272,128]{2,1,0:T(8,128)(2,1)S(1)}, bf16[2,272,128]{2,1,0:T(8,128)(2,1)S(1)}, u32[]{:S(2)}, u32[]{:S(2)}) collective-permute-start(bf16[2,272,128]{2,1,0:T(8,128)(2,1)S(1)} %pad_maximum_fusion.1), channel_id=1, source_target_pairs={{0,12},{1,5},{2,14},{3,7},{4,0},{5,9},{6,2},{7,11},{8,4},{9,13},{1... | collective-permute-start | bytes 417800 | tf_op jit(solution)/shard_map/ppermute | solution.py:288
  79.0 7.1 %collective-permute-start.3 = (bf16[2,272,128]{2,1,0:T(8,128)(2,1)S(1)}, bf16[2,272,128]{2,1,0:T(8,128)(2,1)S(1)}, u32[]{:S(2)}, u32[]{:S(2)}) collective-permute-start(bf16[2,272,128]{2,1,0:T(8,128)(2,1)S(1)} %pad_maximum_fusion.1), channel_id=1, source_target_pairs={{0,14},{1,3},{2,0},{3,5},{4,2},{5,7},{6,4},{7,9},{8,6},{9,11},{10,... | collective-permute-start | bytes 417800 | tf_op jit(solution)/shard_map/ppermute | solution.py:288
  82.3 8.2 %collective-permute-start.4 = (bf16[2,272,128]{2,1,0:T(8,128)(2,1)S(1)}, bf16[2,272,128]{2,1,0:T(8,128)(2,1)S(1)}, u32[]{:S(2)}, u32[]{:S(2)}) collective-permute-start(bf16[2,272,128]{2,1,0:T(8,128)(2,1)S(1)} %pad_maximum_fusion.1), channel_id=1, source_target_pairs={{0,2},{1,15},{2,4},{3,1},{4,6},{5,3},{6,8},{7,5},{8,10},{9,7},{10,... | collective-permute-start | bytes 417800 | tf_op jit(solution)/shard_map/ppermute | solution.py:288
  86.2 21.3 %copy-start.6 = (f32[2,2048]{1,0:T(2,128)S(1)}, f32[2,2048]{1,0:T(2,128)}, u32[]{:S(2)}) copy-start(f32[2,2048]{1,0:T(2,128)} %param.11) | copy-start | bytes 49156
  90.5 17.0 %collective-permute-start.5 = (bf16[8,272,128]{2,1,0:T(8,128)(2,1)S(1)}, bf16[8,272,128]{2,1,0:T(8,128)(2,1)S(1)}, u32[]{:S(2)}, u32[]{:S(2)}) collective-permute-start(bf16[8,272,128]{2,1,0:T(8,128)(2,1)S(1)} %constant_dynamic-update-slice_fusion.2.mine_ref), channel_id=1, source_target_pairs={{0,1},{1,0},{2,3},{3,2},{4,5},{5,4},{6,7},{7,6},{8,9},{9,8},{10,11... | collective-permute-start | bytes 1671176 | tf_op jit(solution)/shard_map/ppermute | solution.py:272
  92.5 17.8 %collective-permute-start.7 = (bf16[256,128]{1,0:T(8,128)(2,1)S(1)}, bf16[256,128]{1,0:T(8,128)(2,1)S(1)}, u32[]{:S(2)}, u32[]{:S(2)}) collective-permute-start(bf16[256,128]{1,0:T(8,128)(2,1)S(1)} %get-tuple-element.48), channel_id=1, source_target_pairs={{0,192},{16,208},{32,224},{48,240},{64,0},{80,16},{96,32},{112,48}... | collective-permute-start | bytes 196616 | tf_op jit(solution)/shard_map/ppermute | solution.py:272
  110.3 35.7 %collective-permute-start.8 = (bf16[256,128]{1,0:T(8,128)(2,1)S(1)}, bf16[256,128]{1,0:T(8,128)(2,1)S(1)}, u32[]{:S(2)}, u32[]{:S(2)}) collective-permute-start(bf16[256,128]{1,0:T(8,128)(2,1)S(1)} %get-tuple-element.48), channel_id=1, source_target_pairs={{0,64},{16,80},{32,96},{48,112},{64,128},{80,144},{96,160},{112,17... | collective-permute-start | bytes 196616 | tf_op jit(solution)/shard_map/ppermute | solution.py:272
  121.9 24.1 %collective-permute-start.9 = (bf16[256,128]{1,0:T(8,128)(2,1)S(1)}, bf16[256,128]{1,0:T(8,128)(2,1)S(1)}, u32[]{:S(2)}, u32[]{:S(2)}) collective-permute-start(bf16[256,128]{1,0:T(8,128)(2,1)S(1)} %collective-permute-done.7), channel_id=1, source_target_pairs={{0,192},{16,208},{32,224},{48,240},{64,0},{80,16},{96,32},{112,48}... | collective-permute-start | bytes 196616 | tf_op jit(solution)/shard_map/ppermute | solution.py:272
  146.0 12.1 %collective-permute-start.10 = (bf16[4,64,128]{2,1,0:T(8,128)(2,1)S(1)}, bf16[4,64,128]{2,1,0:T(8,128)(2,1)S(1)}, u32[]{:S(2)}, u32[]{:S(2)}) collective-permute-start(bf16[4,64,128]{2,1,0:T(8,128)(2,1)S(1)} %pad_maximum_fusion.2), channel_id=1, source_target_pairs={{0,224},{1,33},{16,240},{17,49},{32,0},{33,65},{48,16},{49,81},{64... | collective-permute-start | bytes 196616 | tf_op jit(solution)/shard_map/ppermute | solution.py:288
  148.6 13.9 %all-to-all-start.2 = ((bf16[8,64,256]{2,1,0:T(8,128)(2,1)}), bf16[8,64,256]{2,1,0:T(8,128)(2,1)S(1)}, u32[]{:S(2)}, u32[]{:S(2)}) async-start(bf16[8,64,256]{2,1,0:T(8,128)(2,1)} %shard_map.102), calls=%async_computation.2 | async-start | bytes 524288 | tf_op jit(solution)/shard_map/all_to_all | solution.py:267
  152.3 6.2 %collective-permute-start.11 = (bf16[4,64,128]{2,1,0:T(8,128)(2,1)S(1)}, bf16[4,64,128]{2,1,0:T(8,128)(2,1)S(1)}, u32[]{:S(2)}, u32[]{:S(2)}) collective-permute-start(bf16[4,64,128]{2,1,0:T(8,128)(2,1)S(1)} %pad_maximum_fusion.2), channel_id=1, source_target_pairs={{0,240},{1,17},{16,0},{17,33},{32,16},{33,49},{48,32},{49,65},{64,... | collective-permute-start | bytes 196616 | tf_op jit(solution)/shard_map/ppermute | solution.py:288
  154.7 9.7 %collective-permute-start.12 = (bf16[4,64,128]{2,1,0:T(8,128)(2,1)S(1)}, bf16[4,64,128]{2,1,0:T(8,128)(2,1)S(1)}, u32[]{:S(2)}, u32[]{:S(2)}) collective-permute-start(bf16[4,64,128]{2,1,0:T(8,128)(2,1)S(1)} %pad_maximum_fusion.2), channel_id=1, source_target_pairs={{0,16},{1,241},{16,32},{17,1},{32,48},{33,17},{48,64},{49,33},{64,... | collective-permute-start | bytes 196616 | tf_op jit(solution)/shard_map/ppermute | solution.py:288
  162.5 3.4 %collective-permute-start.6 = (bf16[8,64,256]{2,1,0:T(8,128)(2,1)S(1)}, bf16[8,64,256]{2,1,0:T(8,128)(2,1)S(1)}, u32[]{:S(2)}, u32[]{:S(2)}) collective-permute-start(bf16[8,64,256]{2,1,0:T(8,128)(2,1)S(1)} %all-to-all-done.2.mine_ref), channel_id=1, source_target_pairs={{0,1},{1,0},{2,3},{3,2},{4,5},{5,4},{6,7},{7,6},{8,9},{9,8},{10,11... | collective-permute-start | bytes 786440 | tf_op jit(solution)/shard_map/ppermute | solution.py:272
  167.1 21.5 %all-to-all-start.3 = ((bf16[8,256,128]{2,1,0:T(8,128)(2,1)}), bf16[8,256,128]{2,1,0:T(8,128)(2,1)S(1)}, u32[]{:S(2)}, u32[]{:S(2)}) async-start(bf16[8,256,128]{2,1,0:T(8,128)(2,1)} %get-tuple-element.47), calls=%async_computation.3 | async-start | bytes 1048576 | tf_op jit(solution)/shard_map/all_to_all | solution.py:267
  170.9 11.0 %collective-permute-start.14 = (bf16[4,192,128]{2,1,0:T(8,128)(2,1)S(1)}, bf16[4,192,128]{2,1,0:T(8,128)(2,1)S(1)}, u32[]{:S(2)}, u32[]{:S(2)}) collective-permute-start(bf16[4,192,128]{2,1,0:T(8,128)(2,1)S(1)} %pad_maximum_fusion), channel_id=1, source_target_pairs={{0,224},{1,33},{16,240},{17,49},{32,0},{33,65},{48,16},{49,81},{64... | collective-permute-start | bytes 589832 | tf_op jit(solution)/shard_map/ppermute | solution.py:288
  176.0 9.3 %collective-permute-start.15 = (bf16[4,192,128]{2,1,0:T(8,128)(2,1)S(1)}, bf16[4,192,128]{2,1,0:T(8,128)(2,1)S(1)}, u32[]{:S(2)}, u32[]{:S(2)}) collective-permute-start(bf16[4,192,128]{2,1,0:T(8,128)(2,1)S(1)} %pad_maximum_fusion), channel_id=1, source_target_pairs={{0,240},{1,17},{16,0},{17,33},{32,16},{33,49},{48,32},{49,65},{64,... | collective-permute-start | bytes 589832 | tf_op jit(solution)/shard_map/ppermute | solution.py:288
  178.0 12.6 %collective-permute-start.16 = (bf16[4,192,128]{2,1,0:T(8,128)(2,1)S(1)}, bf16[4,192,128]{2,1,0:T(8,128)(2,1)S(1)}, u32[]{:S(2)}, u32[]{:S(2)}) collective-permute-start(bf16[4,192,128]{2,1,0:T(8,128)(2,1)S(1)} %pad_maximum_fusion), channel_id=1, source_target_pairs={{0,16},{1,241},{16,32},{17,1},{32,48},{33,17},{48,64},{49,33},{64,... | collective-permute-start | bytes 589832 | tf_op jit(solution)/shard_map/ppermute | solution.py:288
  188.6 3.8 %collective-permute-start.13 = (bf16[8,256,128]{2,1,0:T(8,128)(2,1)S(1)}, bf16[8,256,128]{2,1,0:T(8,128)(2,1)S(1)}, u32[]{:S(2)}, u32[]{:S(2)}) collective-permute-start(bf16[8,256,128]{2,1,0:T(8,128)(2,1)S(1)} %all-to-all-done.3.mine_ref), channel_id=1, source_target_pairs={{0,1},{1,0},{2,3},{3,2},{4,5},{5,4},{6,7},{7,6},{8,9},{9,8},{10,11... | collective-permute-start | bytes 1572872 | tf_op jit(solution)/shard_map/ppermute | solution.py:272
  193.0 4.8 %collective-permute-start.17 = (bf16[64,128]{1,0:T(8,128)(2,1)S(1)}, bf16[64,128]{1,0:T(8,128)(2,1)S(1)}, u32[]{:S(2)}, u32[]{:S(2)}) collective-permute-start(bf16[64,128]{1,0:T(8,128)(2,1)S(1)} %get-tuple-element.53), channel_id=1, source_target_pairs={{0,16},{16,32},{32,48},{48,64},{64,80},{80,96},{96,112},{112,128},... | collective-permute-start | bytes 49160 | tf_op jit(solution)/shard_map/ppermute | solution.py:312
  233.6 3.4 %collective-permute-start.18 = (bf16[8,64,256]{2,1,0:T(8,128)(2,1)S(1)}, bf16[8,64,256]{2,1,0:T(8,128)(2,1)S(1)}, u32[]{:S(2)}, u32[]{:S(2)}) collective-permute-start(bf16[8,64,256]{2,1,0:T(8,128)(2,1)S(1)} %all_to_all.32.mine_ref), channel_id=1, source_target_pairs={{0,1},{1,0},{2,3},{3,2},{4,5},{5,4},{6,7},{7,6},{8,9},{9,8},{10,11... | collective-permute-start | bytes 786440 | tf_op jit(solution)/shard_map/ppermute | solution.py:272
  (5 other events, 4.3 us)

commit v9 on v6

--- a/solution.py
+++ b/solution.py
@@ -295,8 +295,11 @@
     first, shard = pack_call(value_proj, gate_proj, mix_proj, count)
     weights = exchange(first, "sp")
     held = jnp.stack([tokens, far_hop(tokens, "x")])
+    hop_one = far_hop(shard, "sp", -1)
+    hop_back = far_hop(shard, "sp")
     mine = near_hops(held, "x")
     gains = [gain.reshape(chips * cores, 1, own_cols) for gain in norm_gain]
+    gains[1] = copy_call(gains[1])
     gains[1] = copy_call(gains[1])
     gains[1] = copy_call(gains[1])
     gains[1] = copy_call(gains[1])
@@ -312,9 +315,6 @@
             layer == 0, layer > 0, mine, theirs, gains[layer], weights, channels
         )
         before = lax.ppermute(tail, "sp", [(i, i + 1) for i in range(count - 1)])
-        if more:
-            _, shard = lax.optimization_barrier((tail, shard))
-            hop_one = far_hop(shard, "sp", -1)
         cum, state, msg = scan_call(
             layer,
             value_rows,
@@ -328,8 +328,7 @@
         )
         msgs = exchange(msg, "sp")
         if more:
-            _, shard, hop_one = lax.optimization_barrier((msg, shard, hop_one))
-            hop_back = far_hop(shard, "sp")
+            _, hop_one = lax.optimization_barrier((msg, hop_one))
             hop_two = far_hop(hop_one, "sp", -1)
         sent = close_call(msgs, cum, state, gate_rows, chips)
         mine = exchange(sent, "x")

time: 221 us -> 214 us (0.968)
  waiting for transfers between devices: 30.1 us -> 24.8 us
  blocking collectives: 57.5 us -> 53.8 us
    all_to_all x3, blocking collectives: 57.5 us -> 53.8 us  [exchange(): return lax.all_to_all(copies, axis, split_axis=0, concat_axis=0, tiled=True)]
    ppermute x8, waiting for transfers between devices: 10.9 us -> 7.54 us  [shift(): lax.ppermute(array, axis, [(i, (i + steps) % count) for i in range(count)])]
    pallas_call x11 -> x12, Pallas kernels: 6.45 us -> 6.45 us  [kernel_call(): pl.pallas_call(kernel, out_shape=out_shape, in_specs=vmem(len(operands)),...]
  transfers between devices with their start and end apart: 22 -> 22, of which waited for: 15 -> 11; matrix products, arithmetic and copies ran while one was open for 0% -> 0% of each run, Pallas kernels for 1% -> 1%
where the time goes in v9:
time: 214 us; the launch traced here: 211 us
  starting transfers between devices  124 us (58%)
  blocking collectives  53.8 us (25%)
  waiting for transfers between devices  24.8 us (12%)
  Pallas kernels  8.2 us (4%)
    all_to_all x3, blocking collectives, exchange(): return lax.all_to_all(copies, axis, split_axis=0, concat_axis=0, tiled=True)  53.8 us
    all_to_all x3, starting transfers between devices, exchange(): return lax.all_to_all(copies, axis, split_axis=0, concat_axis=0, tiled=True)  51.2 us
    ppermute x8, starting transfers between devices, shift(): lax.ppermute(array, axis, [(i, (i + steps) % count) for i in range(count)])  34.7 us
    ppermute x9, starting transfers between devices, hop(): return lax.ppermute(held, (axis, 'core'), pairs)  31.8 us
    ppermute x9, waiting for transfers between devices, hop(): return lax.ppermute(held, (axis, 'core'), pairs)  8.44 us
    ppermute x8, waiting for transfers between devices, shift(): lax.ppermute(array, axis, [(i, (i + steps) % count) for i in range(count)])  7.54 us
    all_to_all x3, waiting for transfers between devices, exchange(): return lax.all_to_all(copies, axis, split_axis=0, concat_axis=0, tiled=True)  7.39 us
    pallas_call x12, Pallas kernels, kernel_call(): pl.pallas_call(kernel, out_shape=out_shape, in_specs=vmem(len(operands)),...  6.45 us
  transfers between devices with their start and end apart: 22, of which 11 were waited for; matrix products, arithmetic and copies ran while one was open for 0% of the time, Pallas kernels for 1%

profile of v9, /device:TPU:80, one launch (start us, length us, event | category | flops | bytes accessed | tf_op | source)
XLA Modules:
  0.0 211.4 jit_solution(3299027483823696103)
XLA Ops:
  1.8 43.8 %all-to-all-start = ((bf16[16,128,128]{2,1,0:T(8,128)(2,1)}), bf16[16,128,128]{2,1,0:T(8,128)(2,1)S(1)}, u32[]{:S(2)}, u32[]{:S(2)}) async-start(bf16[16,128,128]{2,1,0:T(8,128)(2,1)} %get-tuple-element.30), calls=%async_computation | async-start | bytes 1048576 | tf_op jit(solution)/shard_map/all_to_all | solution.py:251
  45.6 8.0 %collective-permute-start = (bf16[256,128]{1,0:T(8,128)(2,1)S(1)}, bf16[256,128]{1,0:T(8,128)(2,1)S(1)}, u32[]{:S(2)}, u32[]{:S(2)}) collective-permute-start(bf16[256,128]{1,0:T(8,128)(2,1)S(1)} %copy-done), channel_id=1, source_target_pairs={{0,8},{2,10},{4,12},{6,14},{8,0},{10,2},{12,4},{14,6},{1,9},{3,11}... | collective-permute-start | bytes 196616 | tf_op jit(solution)/shard_map/ppermute | solution.py:256
  53.6 2.8 %collective-permute-done = bf16[256,128]{1,0:T(8,128)(2,1)S(1)} collective-permute-done((bf16[256,128]{1,0:T(8,128)(2,1)S(1)}, bf16[256,128]{1,0:T(8,128)(2,1)S(1)}, u32[]{:S(2)}, u32[]{:S(2)}) %collective-permute-start) | collective-permute-done | bytes 65568 | tf_op jit(solution)/shard_map/ppermute | solution.py:256
  56.4 6.6 %collective-permute-start.1 = (bf16[2,256,128]{2,1,0:T(8,128)(2,1)S(1)}, bf16[2,256,128]{2,1,0:T(8,128)(2,1)S(1)}, u32[]{:S(2)}, u32[]{:S(2)}) collective-permute-start(bf16[2,256,128]{2,1,0:T(8,128)(2,1)S(1)} %pad_maximum_fusion.1), channel_id=1, source_target_pairs={{0,12},{1,5},{2,14},{3,7},{4,0},{5,9},{6,2},{7,11},{8,4},{9,13},{1... | collective-permute-start | bytes 393224 | tf_op jit(solution)/shard_map/ppermute | solution.py:272
  62.9 2.9 %collective-permute-start.2 = (bf16[2,256,128]{2,1,0:T(8,128)(2,1)S(1)}, bf16[2,256,128]{2,1,0:T(8,128)(2,1)S(1)}, u32[]{:S(2)}, u32[]{:S(2)}) collective-permute-start(bf16[2,256,128]{2,1,0:T(8,128)(2,1)S(1)} %pad_maximum_fusion.1), channel_id=1, source_target_pairs={{0,14},{1,3},{2,0},{3,5},{4,2},{5,7},{6,4},{7,9},{8,6},{9,11},{10,... | collective-permute-start | bytes 393224 | tf_op jit(solution)/shard_map/ppermute | solution.py:272
  65.8 3.0 %collective-permute-start.3 = (bf16[2,256,128]{2,1,0:T(8,128)(2,1)S(1)}, bf16[2,256,128]{2,1,0:T(8,128)(2,1)S(1)}, u32[]{:S(2)}, u32[]{:S(2)}) collective-permute-start(bf16[2,256,128]{2,1,0:T(8,128)(2,1)S(1)} %pad_maximum_fusion.1), channel_id=1, source_target_pairs={{0,2},{1,15},{2,4},{3,1},{4,6},{5,3},{6,8},{7,5},{8,10},{9,7},{10,... | collective-permute-start | bytes 393224 | tf_op jit(solution)/shard_map/ppermute | solution.py:272
  70.6 3.3 %collective-permute-done.3 = bf16[2,256,128]{2,1,0:T(8,128)(2,1)S(1)} collective-permute-done((bf16[2,256,128]{2,1,0:T(8,128)(2,1)S(1)}, bf16[2,256,128]{2,1,0:T(8,128)(2,1)S(1)}, u32[]{:S(2)}, u32[]{:S(2)}) %collective-permute-start.3) | collective-permute-done | bytes 131104 | tf_op jit(solution)/shard_map/ppermute | solution.py:272
  75.9 7.3 %collective-permute-start.8 = (bf16[256,128]{1,0:T(8,128)(2,1)S(1)}, bf16[256,128]{1,0:T(8,128)(2,1)S(1)}, u32[]{:S(2)}, u32[]{:S(2)}) collective-permute-start(bf16[256,128]{1,0:T(8,128)(2,1)S(1)} %get-tuple-element.44), channel_id=1, source_target_pairs={{0,192},{16,208},{32,224},{48,240},{64,0},{80,16},{96,32},{112,48}... | collective-permute-start | bytes 196616 | tf_op jit(solution)/shard_map/ppermute | solution.py:256
  83.8 2.5 %collective-permute-start.5 = (bf16[64,128]{1,0:T(8,128)(2,1)S(1)}, bf16[64,128]{1,0:T(8,128)(2,1)S(1)}, u32[]{:S(2)}, u32[]{:S(2)}) collective-permute-start(bf16[64,128]{1,0:T(8,128)(2,1)S(1)} %get-tuple-element.32), channel_id=1, source_target_pairs={{0,16},{16,32},{32,48},{48,64},{64,80},{80,96},{96,112},{112,128},... | collective-permute-start | bytes 49160 | tf_op jit(solution)/shard_map/ppermute | solution.py:317
  86.3 3.4 %collective-permute-start.7 = (bf16[256,128]{1,0:T(8,128)(2,1)S(1)}, bf16[256,128]{1,0:T(8,128)(2,1)S(1)}, u32[]{:S(2)}, u32[]{:S(2)}) collective-permute-start(bf16[256,128]{1,0:T(8,128)(2,1)S(1)} %get-tuple-element.44), channel_id=1, source_target_pairs={{0,64},{16,80},{32,96},{48,112},{64,128},{80,144},{96,160},{112,17... | collective-permute-start | bytes 196616 | tf_op jit(solution)/shard_map/ppermute | solution.py:256
  90.9 8.2 %collective-permute-start.9 = (bf16[256,128]{1,0:T(8,128)(2,1)S(1)}, bf16[256,128]{1,0:T(8,128)(2,1)S(1)}, u32[]{:S(2)}, u32[]{:S(2)}) collective-permute-start(bf16[256,128]{1,0:T(8,128)(2,1)S(1)} %collective-permute-done.8), channel_id=1, source_target_pairs={{0,192},{16,208},{32,224},{48,240},{64,0},{80,16},{96,32},{112,48}... | collective-permute-start | bytes 196616 | tf_op jit(solution)/shard_map/ppermute | solution.py:256
  99.2 19.3 %all_to_all.30.msgs_ref = f32[16,1,128]{2,1,0:T(1,128)S(1)} all-to-all(f32[16,1,128]{2,1,0:T(1,128)S(1)} %get-tuple-element.33), channel_id=1, replica_groups=mesh['grp'=2,'sp'=16,'x'=8,'core'=2] {'sp'}, dimensions={0} | all-to-all | bytes 16384 | tf_op jit(solution)/shard_map/all_to_all | solution.py:251
  121.9 3.6 %all-to-all-start.2 = ((bf16[8,64,256]{2,1,0:T(8,128)(2,1)}), bf16[8,64,256]{2,1,0:T(8,128)(2,1)S(1)}, u32[]{:S(2)}, u32[]{:S(2)}) async-start(bf16[8,64,256]{2,1,0:T(8,128)(2,1)} %shard_map.102), calls=%async_computation.2 | async-start | bytes 524288 | tf_op jit(solution)/shard_map/all_to_all | solution.py:251
  125.6 2.6 %collective-permute-start.11 = (bf16[4,64,128]{2,1,0:T(8,128)(2,1)S(1)}, bf16[4,64,128]{2,1,0:T(8,128)(2,1)S(1)}, u32[]{:S(2)}, u32[]{:S(2)}) collective-permute-start(bf16[4,64,128]{2,1,0:T(8,128)(2,1)S(1)} %pad_maximum_fusion.2), channel_id=1, source_target_pairs={{0,240},{1,17},{16,0},{17,33},{32,16},{33,49},{48,32},{49,65},{64,... | collective-permute-start | bytes 196616 | tf_op jit(solution)/shard_map/ppermute | solution.py:272
  128.1 3.3 %collective-permute-start.12 = (bf16[4,64,128]{2,1,0:T(8,128)(2,1)S(1)}, bf16[4,64,128]{2,1,0:T(8,128)(2,1)S(1)}, u32[]{:S(2)}, u32[]{:S(2)}) collective-permute-start(bf16[4,64,128]{2,1,0:T(8,128)(2,1)S(1)} %pad_maximum_fusion.2), channel_id=1, source_target_pairs={{0,16},{1,241},{16,32},{17,1},{32,48},{33,17},{48,64},{49,33},{64,... | collective-permute-start | bytes 196616 | tf_op jit(solution)/shard_map/ppermute | solution.py:272
  131.8 4.0 %all-to-all-done.2.mine_ref = bf16[8,64,256]{2,1,0:T(8,128)(2,1)S(1)} async-done(((bf16[8,64,256]{2,1,0:T(8,128)(2,1)}), bf16[8,64,256]{2,1,0:T(8,128)(2,1)S(1)}, u32[]{:S(2)}, u32[]{:S(2)}) %all-to-all-start.2) | async-done | bytes 262176 | tf_op jit(solution)/shard_map/all_to_all | solution.py:251
  140.4 3.7 %all-to-all-start.3 = ((bf16[8,256,128]{2,1,0:T(8,128)(2,1)}), bf16[8,256,128]{2,1,0:T(8,128)(2,1)S(1)}, u32[]{:S(2)}, u32[]{:S(2)}) async-start(bf16[8,256,128]{2,1,0:T(8,128)(2,1)} %get-tuple-element.43), calls=%async_computation.3 | async-start | bytes 1048576 | tf_op jit(solution)/shard_map/all_to_all | solution.py:251
  144.2 5.1 %collective-permute-start.14 = (bf16[4,192,128]{2,1,0:T(8,128)(2,1)S(1)}, bf16[4,192,128]{2,1,0:T(8,128)(2,1)S(1)}, u32[]{:S(2)}, u32[]{:S(2)}) collective-permute-start(bf16[4,192,128]{2,1,0:T(8,128)(2,1)S(1)} %pad_maximum_fusion), channel_id=1, source_target_pairs={{0,224},{1,33},{16,240},{17,49},{32,0},{33,65},{48,16},{49,81},{64... | collective-permute-start | bytes 589832 | tf_op jit(solution)/shard_map/ppermute | solution.py:272
  151.3 4.0 %collective-permute-start.16 = (bf16[4,192,128]{2,1,0:T(8,128)(2,1)S(1)}, bf16[4,192,128]{2,1,0:T(8,128)(2,1)S(1)}, u32[]{:S(2)}, u32[]{:S(2)}) collective-permute-start(bf16[4,192,128]{2,1,0:T(8,128)(2,1)S(1)} %pad_maximum_fusion), channel_id=1, source_target_pairs={{0,16},{1,241},{16,32},{17,1},{32,48},{33,17},{48,64},{49,33},{64,... | collective-permute-start | bytes 589832 | tf_op jit(solution)/shard_map/ppermute | solution.py:272
  155.3 3.2 %collective-permute-done.15 = bf16[4,192,128]{2,1,0:T(8,128)(2,1)S(1)} collective-permute-done((bf16[4,192,128]{2,1,0:T(8,128)(2,1)S(1)}, bf16[4,192,128]{2,1,0:T(8,128)(2,1)S(1)}, u32[]{:S(2)}, u32[]{:S(2)}) %collective-permute-start.15) | collective-permute-done | bytes 196640 | tf_op jit(solution)/shard_map/ppermute | solution.py:272
  158.6 3.4 %all-to-all-done.3.mine_ref = bf16[8,256,128]{2,1,0:T(8,128)(2,1)S(1)} async-done(((bf16[8,256,128]{2,1,0:T(8,128)(2,1)}), bf16[8,256,128]{2,1,0:T(8,128)(2,1)S(1)}, u32[]{:S(2)}, u32[]{:S(2)}) %all-to-all-start.3) | async-done | bytes 524320 | tf_op jit(solution)/shard_map/all_to_all | solution.py:251
  166.3 3.4 %collective-permute-start.17 = (bf16[64,128]{1,0:T(8,128)(2,1)S(1)}, bf16[64,128]{1,0:T(8,128)(2,1)S(1)}, u32[]{:S(2)}, u32[]{:S(2)}) collective-permute-start(bf16[64,128]{1,0:T(8,128)(2,1)S(1)} %get-tuple-element.49), channel_id=1, source_target_pairs={{0,16},{16,32},{32,48},{48,64},{64,80},{80,96},{96,112},{112,128},... | collective-permute-start | bytes 49160 | tf_op jit(solution)/shard_map/ppermute | solution.py:317
  172.3 19.3 %all_to_all.31.msgs_ref = f32[16,1,128]{2,1,0:T(1,128)S(1)} all-to-all(f32[16,1,128]{2,1,0:T(1,128)S(1)} %get-tuple-element.50), channel_id=1, replica_groups=mesh['grp'=2,'sp'=16,'x'=8,'core'=2] {'sp'}, dimensions={0} | all-to-all | bytes 16384 | tf_op jit(solution)/shard_map/all_to_all | solution.py:251
  191.7 15.2 %all_to_all.32.mine_ref = bf16[8,64,256]{2,1,0:T(8,128)(2,1)S(1)} all-to-all(bf16[8,64,256]{2,1,0:T(8,128)(2,1)S(1)} %shard_map.110), channel_id=1, replica_groups=mesh['grp'=2,'sp'=16,'x'=8,'core'=2] {'x'}, dimensions={0} | all-to-all | bytes 524288 | tf_op jit(solution)/shard_map/all_to_all | solution.py:251
  (79 shorter events, 28.9 us)
Async XLA Ops:
  1.8 43.8 %copy-start = (bf16[256,128]{1,0:T(8,128)(2,1)S(1)}, bf16[256,128]{1,0:T(8,128)(2,1)}, u32[]{:S(2)}) copy-start(bf16[256,128]{1,0:T(8,128)(2,1)} %residual_ref.1) | copy-start | bytes 196612
  1.8 81.5 %all-to-all-start = ((bf16[16,128,128]{2,1,0:T(8,128)(2,1)}), bf16[16,128,128]{2,1,0:T(8,128)(2,1)S(1)}, u32[]{:S(2)}, u32[]{:S(2)}) async-start(bf16[16,128,128]{2,1,0:T(8,128)(2,1)} %get-tuple-element.30), calls=%async_computation | async-start | bytes 1048576 | tf_op jit(solution)/shard_map/all_to_all | solution.py:251
  45.6 10.7 %collective-permute-start = (bf16[256,128]{1,0:T(8,128)(2,1)S(1)}, bf16[256,128]{1,0:T(8,128)(2,1)S(1)}, u32[]{:S(2)}, u32[]{:S(2)}) collective-permute-start(bf16[256,128]{1,0:T(8,128)(2,1)S(1)} %copy-done), channel_id=1, source_target_pairs={{0,8},{2,10},{4,12},{6,14},{8,0},{10,2},{12,4},{14,6},{1,9},{3,11}... | collective-permute-start | bytes 196616 | tf_op jit(solution)/shard_map/ppermute | solution.py:256
  56.4 12.5 %collective-permute-start.1 = (bf16[2,256,128]{2,1,0:T(8,128)(2,1)S(1)}, bf16[2,256,128]{2,1,0:T(8,128)(2,1)S(1)}, u32[]{:S(2)}, u32[]{:S(2)}) collective-permute-start(bf16[2,256,128]{2,1,0:T(8,128)(2,1)S(1)} %pad_maximum_fusion.1), channel_id=1, source_target_pairs={{0,12},{1,5},{2,14},{3,7},{4,0},{5,9},{6,2},{7,11},{8,4},{9,13},{1... | collective-permute-start | bytes 393224 | tf_op jit(solution)/shard_map/ppermute | solution.py:272
  62.9 7.6 %collective-permute-start.2 = (bf16[2,256,128]{2,1,0:T(8,128)(2,1)S(1)}, bf16[2,256,128]{2,1,0:T(8,128)(2,1)S(1)}, u32[]{:S(2)}, u32[]{:S(2)}) collective-permute-start(bf16[2,256,128]{2,1,0:T(8,128)(2,1)S(1)} %pad_maximum_fusion.1), channel_id=1, source_target_pairs={{0,14},{1,3},{2,0},{3,5},{4,2},{5,7},{6,4},{7,9},{8,6},{9,11},{10,... | collective-permute-start | bytes 393224 | tf_op jit(solution)/shard_map/ppermute | solution.py:272
  65.8 8.1 %collective-permute-start.3 = (bf16[2,256,128]{2,1,0:T(8,128)(2,1)S(1)}, bf16[2,256,128]{2,1,0:T(8,128)(2,1)S(1)}, u32[]{:S(2)}, u32[]{:S(2)}) collective-permute-start(bf16[2,256,128]{2,1,0:T(8,128)(2,1)S(1)} %pad_maximum_fusion.1), channel_id=1, source_target_pairs={{0,2},{1,15},{2,4},{3,1},{4,6},{5,3},{6,8},{7,5},{8,10},{9,7},{10,... | collective-permute-start | bytes 393224 | tf_op jit(solution)/shard_map/ppermute | solution.py:272
  70.6 12.6 %copy-start.6 = (f32[2,2048]{1,0:T(2,128)S(1)}, f32[2,2048]{1,0:T(2,128)}, u32[]{:S(2)}) copy-start(f32[2,2048]{1,0:T(2,128)} %param.11) | copy-start | bytes 49156
  73.9 9.3 %collective-permute-start.4 = (bf16[8,256,128]{2,1,0:T(8,128)(2,1)S(1)}, bf16[8,256,128]{2,1,0:T(8,128)(2,1)S(1)}, u32[]{:S(2)}, u32[]{:S(2)}) collective-permute-start(bf16[8,256,128]{2,1,0:T(8,128)(2,1)S(1)} %constant_dynamic-update-slice_fusion.mine_ref), channel_id=1, source_target_pairs={{0,1},{1,0},{2,3},{3,2},{4,5},{5,4},{6,7},{7,6},{8,9},{9,8},{10,11... | collective-permute-start | bytes 1572872 | tf_op jit(solution)/shard_map/ppermute | solution.py:256
  75.9 15.0 %collective-permute-start.8 = (bf16[256,128]{1,0:T(8,128)(2,1)S(1)}, bf16[256,128]{1,0:T(8,128)(2,1)S(1)}, u32[]{:S(2)}, u32[]{:S(2)}) collective-permute-start(bf16[256,128]{1,0:T(8,128)(2,1)S(1)} %get-tuple-element.44), channel_id=1, source_target_pairs={{0,192},{16,208},{32,224},{48,240},{64,0},{80,16},{96,32},{112,48}... | collective-permute-start | bytes 196616 | tf_op jit(solution)/shard_map/ppermute | solution.py:256
  83.8 5.9 %collective-permute-start.5 = (bf16[64,128]{1,0:T(8,128)(2,1)S(1)}, bf16[64,128]{1,0:T(8,128)(2,1)S(1)}, u32[]{:S(2)}, u32[]{:S(2)}) collective-permute-start(bf16[64,128]{1,0:T(8,128)(2,1)S(1)} %get-tuple-element.32), channel_id=1, source_target_pairs={{0,16},{16,32},{32,48},{48,64},{64,80},{80,96},{96,112},{112,128},... | collective-permute-start | bytes 49160 | tf_op jit(solution)/shard_map/ppermute | solution.py:317
  86.3 33.1 %collective-permute-start.7 = (bf16[256,128]{1,0:T(8,128)(2,1)S(1)}, bf16[256,128]{1,0:T(8,128)(2,1)S(1)}, u32[]{:S(2)}, u32[]{:S(2)}) collective-permute-start(bf16[256,128]{1,0:T(8,128)(2,1)S(1)} %get-tuple-element.44), channel_id=1, source_target_pairs={{0,64},{16,80},{32,96},{48,112},{64,128},{80,144},{96,160},{112,17... | collective-permute-start | bytes 196616 | tf_op jit(solution)/shard_map/ppermute | solution.py:256
  90.9 28.5 %collective-permute-start.9 = (bf16[256,128]{1,0:T(8,128)(2,1)S(1)}, bf16[256,128]{1,0:T(8,128)(2,1)S(1)}, u32[]{:S(2)}, u32[]{:S(2)}) collective-permute-start(bf16[256,128]{1,0:T(8,128)(2,1)S(1)} %collective-permute-done.8), channel_id=1, source_target_pairs={{0,192},{16,208},{32,224},{48,240},{64,0},{80,16},{96,32},{112,48}... | collective-permute-start | bytes 196616 | tf_op jit(solution)/shard_map/ppermute | solution.py:256
  119.5 12.0 %collective-permute-start.10 = (bf16[4,64,128]{2,1,0:T(8,128)(2,1)S(1)}, bf16[4,64,128]{2,1,0:T(8,128)(2,1)S(1)}, u32[]{:S(2)}, u32[]{:S(2)}) collective-permute-start(bf16[4,64,128]{2,1,0:T(8,128)(2,1)S(1)} %pad_maximum_fusion.2), channel_id=1, source_target_pairs={{0,224},{1,33},{16,240},{17,49},{32,0},{33,65},{48,16},{49,81},{64... | collective-permute-start | bytes 196616 | tf_op jit(solution)/shard_map/ppermute | solution.py:272
  121.9 13.9 %all-to-all-start.2 = ((bf16[8,64,256]{2,1,0:T(8,128)(2,1)}), bf16[8,64,256]{2,1,0:T(8,128)(2,1)S(1)}, u32[]{:S(2)}, u32[]{:S(2)}) async-start(bf16[8,64,256]{2,1,0:T(8,128)(2,1)} %shard_map.102), calls=%async_computation.2 | async-start | bytes 524288 | tf_op jit(solution)/shard_map/all_to_all | solution.py:251
  125.6 6.2 %collective-permute-start.11 = (bf16[4,64,128]{2,1,0:T(8,128)(2,1)S(1)}, bf16[4,64,128]{2,1,0:T(8,128)(2,1)S(1)}, u32[]{:S(2)}, u32[]{:S(2)}) collective-permute-start(bf16[4,64,128]{2,1,0:T(8,128)(2,1)S(1)} %pad_maximum_fusion.2), channel_id=1, source_target_pairs={{0,240},{1,17},{16,0},{17,33},{32,16},{33,49},{48,32},{49,65},{64,... | collective-permute-start | bytes 196616 | tf_op jit(solution)/shard_map/ppermute | solution.py:272
  128.1 9.6 %collective-permute-start.12 = (bf16[4,64,128]{2,1,0:T(8,128)(2,1)S(1)}, bf16[4,64,128]{2,1,0:T(8,128)(2,1)S(1)}, u32[]{:S(2)}, u32[]{:S(2)}) collective-permute-start(bf16[4,64,128]{2,1,0:T(8,128)(2,1)S(1)} %pad_maximum_fusion.2), channel_id=1, source_target_pairs={{0,16},{1,241},{16,32},{17,1},{32,48},{33,17},{48,64},{49,33},{64,... | collective-permute-start | bytes 196616 | tf_op jit(solution)/shard_map/ppermute | solution.py:272
  135.8 3.4 %collective-permute-start.6 = (bf16[8,64,256]{2,1,0:T(8,128)(2,1)S(1)}, bf16[8,64,256]{2,1,0:T(8,128)(2,1)S(1)}, u32[]{:S(2)}, u32[]{:S(2)}) collective-permute-start(bf16[8,64,256]{2,1,0:T(8,128)(2,1)S(1)} %all-to-all-done.2.mine_ref), channel_id=1, source_target_pairs={{0,1},{1,0},{2,3},{3,2},{4,5},{5,4},{6,7},{7,6},{8,9},{9,8},{10,11... | collective-permute-start | bytes 786440 | tf_op jit(solution)/shard_map/ppermute | solution.py:256
  140.4 21.5 %all-to-all-start.3 = ((bf16[8,256,128]{2,1,0:T(8,128)(2,1)}), bf16[8,256,128]{2,1,0:T(8,128)(2,1)S(1)}, u32[]{:S(2)}, u32[]{:S(2)}) async-start(bf16[8,256,128]{2,1,0:T(8,128)(2,1)} %get-tuple-element.43), calls=%async_computation.3 | async-start | bytes 1048576 | tf_op jit(solution)/shard_map/all_to_all | solution.py:251
  144.2 11.0 %collective-permute-start.14 = (bf16[4,192,128]{2,1,0:T(8,128)(2,1)S(1)}, bf16[4,192,128]{2,1,0:T(8,128)(2,1)S(1)}, u32[]{:S(2)}, u32[]{:S(2)}) collective-permute-start(bf16[4,192,128]{2,1,0:T(8,128)(2,1)S(1)} %pad_maximum_fusion), channel_id=1, source_target_pairs={{0,224},{1,33},{16,240},{17,49},{32,0},{33,65},{48,16},{49,81},{64... | collective-permute-start | bytes 589832 | tf_op jit(solution)/shard_map/ppermute | solution.py:272
  149.3 9.2 %collective-permute-start.15 = (bf16[4,192,128]{2,1,0:T(8,128)(2,1)S(1)}, bf16[4,192,128]{2,1,0:T(8,128)(2,1)S(1)}, u32[]{:S(2)}, u32[]{:S(2)}) collective-permute-start(bf16[4,192,128]{2,1,0:T(8,128)(2,1)S(1)} %pad_maximum_fusion), channel_id=1, source_target_pairs={{0,240},{1,17},{16,0},{17,33},{32,16},{33,49},{48,32},{49,65},{64,... | collective-permute-start | bytes 589832 | tf_op jit(solution)/shard_map/ppermute | solution.py:272
  151.3 12.6 %collective-permute-start.16 = (bf16[4,192,128]{2,1,0:T(8,128)(2,1)S(1)}, bf16[4,192,128]{2,1,0:T(8,128)(2,1)S(1)}, u32[]{:S(2)}, u32[]{:S(2)}) collective-permute-start(bf16[4,192,128]{2,1,0:T(8,128)(2,1)S(1)} %pad_maximum_fusion), channel_id=1, source_target_pairs={{0,16},{1,241},{16,32},{17,1},{32,48},{33,17},{48,64},{49,33},{64,... | collective-permute-start | bytes 589832 | tf_op jit(solution)/shard_map/ppermute | solution.py:272
  162.0 3.8 %collective-permute-start.13 = (bf16[8,256,128]{2,1,0:T(8,128)(2,1)S(1)}, bf16[8,256,128]{2,1,0:T(8,128)(2,1)S(1)}, u32[]{:S(2)}, u32[]{:S(2)}) collective-permute-start(bf16[8,256,128]{2,1,0:T(8,128)(2,1)S(1)} %all-to-all-done.3.mine_ref), channel_id=1, source_target_pairs={{0,1},{1,0},{2,3},{3,2},{4,5},{5,4},{6,7},{7,6},{8,9},{9,8},{10,11... | collective-permute-start | bytes 1572872 | tf_op jit(solution)/shard_map/ppermute | solution.py:256
  166.3 4.9 %collective-permute-start.17 = (bf16[64,128]{1,0:T(8,128)(2,1)S(1)}, bf16[64,128]{1,0:T(8,128)(2,1)S(1)}, u32[]{:S(2)}, u32[]{:S(2)}) collective-permute-start(bf16[64,128]{1,0:T(8,128)(2,1)S(1)} %get-tuple-element.49), channel_id=1, source_target_pairs={{0,16},{16,32},{32,48},{48,64},{64,80},{80,96},{96,112},{112,128},... | collective-permute-start | bytes 49160 | tf_op jit(solution)/shard_map/ppermute | solution.py:317
  207.0 3.4 %collective-permute-start.18 = (bf16[8,64,256]{2,1,0:T(8,128)(2,1)S(1)}, bf16[8,64,256]{2,1,0:T(8,128)(2,1)S(1)}, u32[]{:S(2)}, u32[]{:S(2)}) collective-permute-start(bf16[8,64,256]{2,1,0:T(8,128)(2,1)S(1)} %all_to_all.32.mine_ref), channel_id=1, source_target_pairs={{0,1},{1,0},{2,3},{3,2},{4,5},{5,4},{6,7},{7,6},{8,9},{9,8},{10,11... | collective-permute-start | bytes 786440 | tf_op jit(solution)/shard_map/ppermute | solution.py:256
  (5 other events, 32.0 us)

commit v10 on v8

--- a/solution.py
+++ b/solution.py
@@ -317,11 +317,16 @@
     held = jnp.concatenate([last, tokens], axis=0)
     held = jnp.stack([held, far_hop(held, "x")])
     hop_one = far_hop(shard, "sp", -1)
+    hop_back = far_hop(shard, "sp")
     mine = near_hops(held, "x")
     gains = [gain.reshape(chips * cores, 1, own_cols) for gain in norm_gain]
     gains[1] = copy_call(gains[1])
     gains[1] = copy_call(gains[1])
     gains[1] = copy_call(gains[1])
+    gains[1] = copy_call(gains[1])
+
+    gains[1] = copy_call(gains[1])
+    decay_param = copy_call(decay_param)
 
     residual = tokens
     for layer in range(LAYERS):
@@ -348,8 +353,7 @@
         )
         msgs = exchange(msg, "sp")
         if more:
-            _, shard, hop_one = lax.optimization_barrier((msg, shard, hop_one))
-            hop_back = far_hop(shard, "sp")
+            _, hop_one = lax.optimization_barrier((msg, hop_one))
             hop_two = far_hop(hop_one, "sp", -1)
         sent = close_call(msgs, cum, state, gate_rows, chips)
         mine = exchange(sent, "x")

time: 240 us -> 236 us (0.983)
  starting transfers between devices: 134 us -> 130 us
    ppermute x8, starting transfers between devices: 44.3 us -> 40.6 us  [shift(): lax.ppermute(array, axis, [(i, (i + steps) % count) for i in range(count)])]
    pallas_call x11 -> x14, Pallas kernels: 6.74 us -> 6.73 us  [kernel_call(): pl.pallas_call(kernel, out_shape=out_shape, in_specs=vmem(len(operands)),...]
where the time goes in v10:
time: 236 us; the launch traced here: 234 us
  starting transfers between devices  130 us (55%)
  blocking collectives  55.9 us (24%)
  waiting for transfers between devices  38 us (16%)
  Pallas kernels  8.47 us (4%)
    all_to_all x3, blocking collectives, exchange(): return lax.all_to_all(copies, axis, split_axis=0, concat_axis=0, tiled=True)  55.9 us
    all_to_all x3, starting transfers between devices, exchange(): return lax.all_to_all(copies, axis, split_axis=0, concat_axis=0, tiled=True)  51.2 us
    ppermute x8, starting transfers between devices, shift(): lax.ppermute(array, axis, [(i, (i + steps) % count) for i in range(count)])  40.6 us
    ppermute x9, starting transfers between devices, hop(): return lax.ppermute(held, (axis, 'core'), pairs)  31.6 us
    ppermute x2, waiting for transfers between devices, to_next(): return lax.ppermute(array, 'sp', [(i, i + 1) for i in range(count - 1)])  14.5 us
    ppermute x9, waiting for transfers between devices, hop(): return lax.ppermute(held, (axis, 'core'), pairs)  8.95 us
    ppermute x8, waiting for transfers between devices, shift(): lax.ppermute(array, axis, [(i, (i + steps) % count) for i in range(count)])  7.31 us
    all_to_all x3, waiting for transfers between devices, exchange(): return lax.all_to_all(copies, axis, split_axis=0, concat_axis=0, tiled=True)  7.18 us
  transfers between devices with their start and end apart: 22, of which 12 were waited for; matrix products, arithmetic and copies ran while one was open for 0% of the time, Pallas kernels for 1%

profile of v10, /device:TPU:80, one launch (start us, length us, event | category | flops | bytes accessed | tf_op | source)
XLA Modules:
  0.0 233.8 jit_solution(14757861520514382979)
XLA Ops:
  1.8 43.8 %all-to-all-start = ((bf16[16,128,128]{2,1,0:T(8,128)(2,1)}), bf16[16,128,128]{2,1,0:T(8,128)(2,1)S(1)}, u32[]{:S(2)}, u32[]{:S(2)}) async-start(bf16[16,128,128]{2,1,0:T(8,128)(2,1)} %get-tuple-element.32), calls=%async_computation | async-start | bytes 1048576 | tf_op jit(solution)/shard_map/all_to_all | solution.py:267
  45.6 3.6 %collective-permute-start = (bf16[16,128]{1,0:T(8,128)(2,1)S(1)}, bf16[16,128]{1,0:T(8,128)(2,1)S(1)}, u32[]{:S(2)}, u32[]{:S(2)}) collective-permute-start(bf16[16,128]{1,0:T(8,128)(2,1)S(1)} %get-tuple-element.31), channel_id=1, source_target_pairs={{0,16},{16,32},{32,48},{48,64},{64,80},{80,96},{96,112},{112,128},... | collective-permute-start | bytes 12296 | tf_op jit(solution)/shard_map/ppermute | solution.py:312
  49.2 13.1 %collective-permute-done = bf16[16,128]{1,0:T(8,128)(2,1)S(1)} collective-permute-done((bf16[16,128]{1,0:T(8,128)(2,1)S(1)}, bf16[16,128]{1,0:T(8,128)(2,1)S(1)}, u32[]{:S(2)}, u32[]{:S(2)}) %collective-permute-start) | collective-permute-done | bytes 4128 | tf_op jit(solution)/shard_map/ppermute | solution.py:312
  62.4 8.0 %collective-permute-start.1 = (bf16[272,128]{1,0:T(8,128)(2,1)S(1)}, bf16[272,128]{1,0:T(8,128)(2,1)S(1)}, u32[]{:S(2)}, u32[]{:S(2)}) collective-permute-start(bf16[272,128]{1,0:T(8,128)(2,1)S(1)} %constant_dynamic-update-slice_fusion), channel_id=1, source_target_pairs={{0,8},{2,10},{4,12},{6,14},{8,0},{10,2},{12,4},{14,6},{1,9},{3,11}... | collective-permute-start | bytes 208904 | tf_op jit(solution)/shard_map/ppermute | solution.py:272
  70.3 2.6 %collective-permute-done.1 = bf16[272,128]{1,0:T(8,128)(2,1)S(1)} collective-permute-done((bf16[272,128]{1,0:T(8,128)(2,1)S(1)}, bf16[272,128]{1,0:T(8,128)(2,1)S(1)}, u32[]{:S(2)}, u32[]{:S(2)}) %collective-permute-start.1) | collective-permute-done | bytes 69664 | tf_op jit(solution)/shard_map/ppermute | solution.py:272
  72.9 6.1 %collective-permute-start.2 = (bf16[2,272,128]{2,1,0:T(8,128)(2,1)S(1)}, bf16[2,272,128]{2,1,0:T(8,128)(2,1)S(1)}, u32[]{:S(2)}, u32[]{:S(2)}) collective-permute-start(bf16[2,272,128]{2,1,0:T(8,128)(2,1)S(1)} %pad_maximum_fusion.1), channel_id=1, source_target_pairs={{0,12},{1,5},{2,14},{3,7},{4,0},{5,9},{6,2},{7,11},{8,4},{9,13},{1... | collective-permute-start | bytes 417800 | tf_op jit(solution)/shard_map/ppermute | solution.py:288
  79.0 3.3 %collective-permute-start.3 = (bf16[2,272,128]{2,1,0:T(8,128)(2,1)S(1)}, bf16[2,272,128]{2,1,0:T(8,128)(2,1)S(1)}, u32[]{:S(2)}, u32[]{:S(2)}) collective-permute-start(bf16[2,272,128]{2,1,0:T(8,128)(2,1)S(1)} %pad_maximum_fusion.1), channel_id=1, source_target_pairs={{0,14},{1,3},{2,0},{3,5},{4,2},{5,7},{6,4},{7,9},{8,6},{9,11},{10,... | collective-permute-start | bytes 417800 | tf_op jit(solution)/shard_map/ppermute | solution.py:288
  82.3 2.6 %collective-permute-start.4 = (bf16[2,272,128]{2,1,0:T(8,128)(2,1)S(1)}, bf16[2,272,128]{2,1,0:T(8,128)(2,1)S(1)}, u32[]{:S(2)}, u32[]{:S(2)}) collective-permute-start(bf16[2,272,128]{2,1,0:T(8,128)(2,1)S(1)} %pad_maximum_fusion.1), channel_id=1, source_target_pairs={{0,2},{1,15},{2,4},{3,1},{4,6},{5,3},{6,8},{7,5},{8,10},{9,7},{10,... | collective-permute-start | bytes 417800 | tf_op jit(solution)/shard_map/ppermute | solution.py:288
  86.2 4.3 %collective-permute-done.4 = bf16[2,272,128]{2,1,0:T(8,128)(2,1)S(1)} collective-permute-done((bf16[2,272,128]{2,1,0:T(8,128)(2,1)S(1)}, bf16[2,272,128]{2,1,0:T(8,128)(2,1)S(1)}, u32[]{:S(2)}, u32[]{:S(2)}) %collective-permute-start.4) | collective-permute-done | bytes 139296 | tf_op jit(solution)/shard_map/ppermute | solution.py:288
  92.5 15.0 %collective-permute-start.8 = (bf16[256,128]{1,0:T(8,128)(2,1)S(1)}, bf16[256,128]{1,0:T(8,128)(2,1)S(1)}, u32[]{:S(2)}, u32[]{:S(2)}) collective-permute-start(bf16[256,128]{1,0:T(8,128)(2,1)S(1)} %get-tuple-element.46), channel_id=1, source_target_pairs={{0,192},{16,208},{32,224},{48,240},{64,0},{80,16},{96,32},{112,48}... | collective-permute-start | bytes 196616 | tf_op jit(solution)/shard_map/ppermute | solution.py:272
  111.6 7.9 %collective-permute-start.9 = (bf16[256,128]{1,0:T(8,128)(2,1)S(1)}, bf16[256,128]{1,0:T(8,128)(2,1)S(1)}, u32[]{:S(2)}, u32[]{:S(2)}) collective-permute-start(bf16[256,128]{1,0:T(8,128)(2,1)S(1)} %collective-permute-done.8), channel_id=1, source_target_pairs={{0,192},{16,208},{32,224},{48,240},{64,0},{80,16},{96,32},{112,48}... | collective-permute-start | bytes 196616 | tf_op jit(solution)/shard_map/ppermute | solution.py:272
  119.5 21.4 %all_to_all.30.msgs_ref = f32[16,1,128]{2,1,0:T(1,128)S(1)} all-to-all(f32[16,1,128]{2,1,0:T(1,128)S(1)} %get-tuple-element.35), channel_id=1, replica_groups=mesh['grp'=2,'sp'=16,'x'=8,'core'=2] {'sp'}, dimensions={0} | all-to-all | bytes 16384 | tf_op jit(solution)/shard_map/all_to_all | solution.py:267
  141.8 2.6 %collective-permute-start.10 = (bf16[4,64,128]{2,1,0:T(8,128)(2,1)S(1)}, bf16[4,64,128]{2,1,0:T(8,128)(2,1)S(1)}, u32[]{:S(2)}, u32[]{:S(2)}) collective-permute-start(bf16[4,64,128]{2,1,0:T(8,128)(2,1)S(1)} %pad_maximum_fusion.2), channel_id=1, source_target_pairs={{0,224},{1,33},{16,240},{17,49},{32,0},{33,65},{48,16},{49,81},{64... | collective-permute-start | bytes 196616 | tf_op jit(solution)/shard_map/ppermute | solution.py:288
  144.4 3.6 %all-to-all-start.2 = ((bf16[8,64,256]{2,1,0:T(8,128)(2,1)}), bf16[8,64,256]{2,1,0:T(8,128)(2,1)S(1)}, u32[]{:S(2)}, u32[]{:S(2)}) async-start(bf16[8,64,256]{2,1,0:T(8,128)(2,1)} %shard_map.103), calls=%async_computation.2 | async-start | bytes 524288 | tf_op jit(solution)/shard_map/all_to_all | solution.py:267
  150.5 3.4 %collective-permute-start.12 = (bf16[4,64,128]{2,1,0:T(8,128)(2,1)S(1)}, bf16[4,64,128]{2,1,0:T(8,128)(2,1)S(1)}, u32[]{:S(2)}, u32[]{:S(2)}) collective-permute-start(bf16[4,64,128]{2,1,0:T(8,128)(2,1)S(1)} %pad_maximum_fusion.2), channel_id=1, source_target_pairs={{0,16},{1,241},{16,32},{17,1},{32,48},{33,17},{48,64},{49,33},{64,... | collective-permute-start | bytes 196616 | tf_op jit(solution)/shard_map/ppermute | solution.py:288
  154.3 4.0 %all-to-all-done.2.mine_ref = bf16[8,64,256]{2,1,0:T(8,128)(2,1)S(1)} async-done(((bf16[8,64,256]{2,1,0:T(8,128)(2,1)}), bf16[8,64,256]{2,1,0:T(8,128)(2,1)S(1)}, u32[]{:S(2)}, u32[]{:S(2)}) %all-to-all-start.2) | async-done | bytes 262176 | tf_op jit(solution)/shard_map/all_to_all | solution.py:267
  162.9 3.7 %all-to-all-start.3 = ((bf16[8,256,128]{2,1,0:T(8,128)(2,1)}), bf16[8,256,128]{2,1,0:T(8,128)(2,1)S(1)}, u32[]{:S(2)}, u32[]{:S(2)}) async-start(bf16[8,256,128]{2,1,0:T(8,128)(2,1)} %get-tuple-element.45), calls=%async_computation.3 | async-start | bytes 1048576 | tf_op jit(solution)/shard_map/all_to_all | solution.py:267
  166.7 5.2 %collective-permute-start.14 = (bf16[4,192,128]{2,1,0:T(8,128)(2,1)S(1)}, bf16[4,192,128]{2,1,0:T(8,128)(2,1)S(1)}, u32[]{:S(2)}, u32[]{:S(2)}) collective-permute-start(bf16[4,192,128]{2,1,0:T(8,128)(2,1)S(1)} %pad_maximum_fusion), channel_id=1, source_target_pairs={{0,224},{1,33},{16,240},{17,49},{32,0},{33,65},{48,16},{49,81},{64... | collective-permute-start | bytes 589832 | tf_op jit(solution)/shard_map/ppermute | solution.py:288
  173.9 4.0 %collective-permute-start.16 = (bf16[4,192,128]{2,1,0:T(8,128)(2,1)S(1)}, bf16[4,192,128]{2,1,0:T(8,128)(2,1)S(1)}, u32[]{:S(2)}, u32[]{:S(2)}) collective-permute-start(bf16[4,192,128]{2,1,0:T(8,128)(2,1)S(1)} %pad_maximum_fusion), channel_id=1, source_target_pairs={{0,16},{1,241},{16,32},{17,1},{32,48},{33,17},{48,64},{49,33},{64,... | collective-permute-start | bytes 589832 | tf_op jit(solution)/shard_map/ppermute | solution.py:288
  177.9 3.2 %collective-permute-done.15 = bf16[4,192,128]{2,1,0:T(8,128)(2,1)S(1)} collective-permute-done((bf16[4,192,128]{2,1,0:T(8,128)(2,1)S(1)}, bf16[4,192,128]{2,1,0:T(8,128)(2,1)S(1)}, u32[]{:S(2)}, u32[]{:S(2)}) %collective-permute-start.15) | collective-permute-done | bytes 196640 | tf_op jit(solution)/shard_map/ppermute | solution.py:288
  181.2 3.2 %all-to-all-done.3.mine_ref = bf16[8,256,128]{2,1,0:T(8,128)(2,1)S(1)} async-done(((bf16[8,256,128]{2,1,0:T(8,128)(2,1)}), bf16[8,256,128]{2,1,0:T(8,128)(2,1)S(1)}, u32[]{:S(2)}, u32[]{:S(2)}) %all-to-all-start.3) | async-done | bytes 524320 | tf_op jit(solution)/shard_map/all_to_all | solution.py:267
  188.7 3.4 %collective-permute-start.17 = (bf16[64,128]{1,0:T(8,128)(2,1)S(1)}, bf16[64,128]{1,0:T(8,128)(2,1)S(1)}, u32[]{:S(2)}, u32[]{:S(2)}) collective-permute-start(bf16[64,128]{1,0:T(8,128)(2,1)S(1)} %get-tuple-element.51), channel_id=1, source_target_pairs={{0,16},{16,32},{32,48},{48,64},{64,80},{80,96},{96,112},{112,128},... | collective-permute-start | bytes 49160 | tf_op jit(solution)/shard_map/ppermute | solution.py:312
  194.7 19.3 %all_to_all.31.msgs_ref = f32[16,1,128]{2,1,0:T(1,128)S(1)} all-to-all(f32[16,1,128]{2,1,0:T(1,128)S(1)} %get-tuple-element.52), channel_id=1, replica_groups=mesh['grp'=2,'sp'=16,'x'=8,'core'=2] {'sp'}, dimensions={0} | all-to-all | bytes 16384 | tf_op jit(solution)/shard_map/all_to_all | solution.py:267
  214.1 15.2 %all_to_all.32.mine_ref = bf16[8,64,256]{2,1,0:T(8,128)(2,1)S(1)} all-to-all(bf16[8,64,256]{2,1,0:T(8,128)(2,1)S(1)} %shard_map.112), channel_id=1, replica_groups=mesh['grp'=2,'sp'=16,'x'=8,'core'=2] {'x'}, dimensions={0} | all-to-all | bytes 524288 | tf_op jit(solution)/shard_map/all_to_all | solution.py:267
  (85 shorter events, 30.7 us)
Async XLA Ops:
  1.7 60.6 %copy-start = (bf16[256,128]{1,0:T(8,128)(2,1)S(1)}, bf16[256,128]{1,0:T(8,128)(2,1)}, u32[]{:S(2)}) copy-start(bf16[256,128]{1,0:T(8,128)(2,1)} %residual_ref.1) | copy-start | bytes 196612
  1.8 107.8 %all-to-all-start = ((bf16[16,128,128]{2,1,0:T(8,128)(2,1)}), bf16[16,128,128]{2,1,0:T(8,128)(2,1)S(1)}, u32[]{:S(2)}, u32[]{:S(2)}) async-start(bf16[16,128,128]{2,1,0:T(8,128)(2,1)} %get-tuple-element.32), calls=%async_computation | async-start | bytes 1048576 | tf_op jit(solution)/shard_map/all_to_all | solution.py:267
  45.6 16.7 %collective-permute-start = (bf16[16,128]{1,0:T(8,128)(2,1)S(1)}, bf16[16,128]{1,0:T(8,128)(2,1)S(1)}, u32[]{:S(2)}, u32[]{:S(2)}) collective-permute-start(bf16[16,128]{1,0:T(8,128)(2,1)S(1)} %get-tuple-element.31), channel_id=1, source_target_pairs={{0,16},{16,32},{32,48},{48,64},{64,80},{80,96},{96,112},{112,128},... | collective-permute-start | bytes 12296 | tf_op jit(solution)/shard_map/ppermute | solution.py:312
  62.4 10.5 %collective-permute-start.1 = (bf16[272,128]{1,0:T(8,128)(2,1)S(1)}, bf16[272,128]{1,0:T(8,128)(2,1)S(1)}, u32[]{:S(2)}, u32[]{:S(2)}) collective-permute-start(bf16[272,128]{1,0:T(8,128)(2,1)S(1)} %constant_dynamic-update-slice_fusion), channel_id=1, source_target_pairs={{0,8},{2,10},{4,12},{6,14},{8,0},{10,2},{12,4},{14,6},{1,9},{3,11}... | collective-permute-start | bytes 208904 | tf_op jit(solution)/shard_map/ppermute | solution.py:272
  72.9 12.0 %collective-permute-start.2 = (bf16[2,272,128]{2,1,0:T(8,128)(2,1)S(1)}, bf16[2,272,128]{2,1,0:T(8,128)(2,1)S(1)}, u32[]{:S(2)}, u32[]{:S(2)}) collective-permute-start(bf16[2,272,128]{2,1,0:T(8,128)(2,1)S(1)} %pad_maximum_fusion.1), channel_id=1, source_target_pairs={{0,12},{1,5},{2,14},{3,7},{4,0},{5,9},{6,2},{7,11},{8,4},{9,13},{1... | collective-permute-start | bytes 417800 | tf_op jit(solution)/shard_map/ppermute | solution.py:288
  79.0 7.1 %collective-permute-start.3 = (bf16[2,272,128]{2,1,0:T(8,128)(2,1)S(1)}, bf16[2,272,128]{2,1,0:T(8,128)(2,1)S(1)}, u32[]{:S(2)}, u32[]{:S(2)}) collective-permute-start(bf16[2,272,128]{2,1,0:T(8,128)(2,1)S(1)} %pad_maximum_fusion.1), channel_id=1, source_target_pairs={{0,14},{1,3},{2,0},{3,5},{4,2},{5,7},{6,4},{7,9},{8,6},{9,11},{10,... | collective-permute-start | bytes 417800 | tf_op jit(solution)/shard_map/ppermute | solution.py:288
  82.3 8.2 %collective-permute-start.4 = (bf16[2,272,128]{2,1,0:T(8,128)(2,1)S(1)}, bf16[2,272,128]{2,1,0:T(8,128)(2,1)S(1)}, u32[]{:S(2)}, u32[]{:S(2)}) collective-permute-start(bf16[2,272,128]{2,1,0:T(8,128)(2,1)S(1)} %pad_maximum_fusion.1), channel_id=1, source_target_pairs={{0,2},{1,15},{2,4},{3,1},{4,6},{5,3},{6,8},{7,5},{8,10},{9,7},{10,... | collective-permute-start | bytes 417800 | tf_op jit(solution)/shard_map/ppermute | solution.py:288
  86.2 23.3 %copy-start.7 = (f32[2,2048]{1,0:T(2,128)S(1)}, f32[2,2048]{1,0:T(2,128)}, u32[]{:S(2)}) copy-start(f32[2,2048]{1,0:T(2,128)} %param.11) | copy-start | bytes 49156
  90.5 19.0 %collective-permute-start.5 = (bf16[8,272,128]{2,1,0:T(8,128)(2,1)S(1)}, bf16[8,272,128]{2,1,0:T(8,128)(2,1)S(1)}, u32[]{:S(2)}, u32[]{:S(2)}) collective-permute-start(bf16[8,272,128]{2,1,0:T(8,128)(2,1)S(1)} %constant_dynamic-update-slice_fusion.2.mine_ref), channel_id=1, source_target_pairs={{0,1},{1,0},{2,3},{3,2},{4,5},{5,4},{6,7},{7,6},{8,9},{9,8},{10,11... | collective-permute-start | bytes 1671176 | tf_op jit(solution)/shard_map/ppermute | solution.py:272
  92.5 19.1 %collective-permute-start.8 = (bf16[256,128]{1,0:T(8,128)(2,1)S(1)}, bf16[256,128]{1,0:T(8,128)(2,1)S(1)}, u32[]{:S(2)}, u32[]{:S(2)}) collective-permute-start(bf16[256,128]{1,0:T(8,128)(2,1)S(1)} %get-tuple-element.46), channel_id=1, source_target_pairs={{0,192},{16,208},{32,224},{48,240},{64,0},{80,16},{96,32},{112,48}... | collective-permute-start | bytes 196616 | tf_op jit(solution)/shard_map/ppermute | solution.py:272
  107.5 34.3 %collective-permute-start.7 = (bf16[256,128]{1,0:T(8,128)(2,1)S(1)}, bf16[256,128]{1,0:T(8,128)(2,1)S(1)}, u32[]{:S(2)}, u32[]{:S(2)}) collective-permute-start(bf16[256,128]{1,0:T(8,128)(2,1)S(1)} %get-tuple-element.46), channel_id=1, source_target_pairs={{0,64},{16,80},{32,96},{48,112},{64,128},{80,144},{96,160},{112,17... | collective-permute-start | bytes 196616 | tf_op jit(solution)/shard_map/ppermute | solution.py:272
  111.6 30.2 %collective-permute-start.9 = (bf16[256,128]{1,0:T(8,128)(2,1)S(1)}, bf16[256,128]{1,0:T(8,128)(2,1)S(1)}, u32[]{:S(2)}, u32[]{:S(2)}) collective-permute-start(bf16[256,128]{1,0:T(8,128)(2,1)S(1)} %collective-permute-done.8), channel_id=1, source_target_pairs={{0,192},{16,208},{32,224},{48,240},{64,0},{80,16},{96,32},{112,48}... | collective-permute-start | bytes 196616 | tf_op jit(solution)/shard_map/ppermute | solution.py:272
  141.8 12.1 %collective-permute-start.10 = (bf16[4,64,128]{2,1,0:T(8,128)(2,1)S(1)}, bf16[4,64,128]{2,1,0:T(8,128)(2,1)S(1)}, u32[]{:S(2)}, u32[]{:S(2)}) collective-permute-start(bf16[4,64,128]{2,1,0:T(8,128)(2,1)S(1)} %pad_maximum_fusion.2), channel_id=1, source_target_pairs={{0,224},{1,33},{16,240},{17,49},{32,0},{33,65},{48,16},{49,81},{64... | collective-permute-start | bytes 196616 | tf_op jit(solution)/shard_map/ppermute | solution.py:288
  144.4 13.9 %all-to-all-start.2 = ((bf16[8,64,256]{2,1,0:T(8,128)(2,1)}), bf16[8,64,256]{2,1,0:T(8,128)(2,1)S(1)}, u32[]{:S(2)}, u32[]{:S(2)}) async-start(bf16[8,64,256]{2,1,0:T(8,128)(2,1)} %shard_map.103), calls=%async_computation.2 | async-start | bytes 524288 | tf_op jit(solution)/shard_map/all_to_all | solution.py:267
  148.1 6.2 %collective-permute-start.11 = (bf16[4,64,128]{2,1,0:T(8,128)(2,1)S(1)}, bf16[4,64,128]{2,1,0:T(8,128)(2,1)S(1)}, u32[]{:S(2)}, u32[]{:S(2)}) collective-permute-start(bf16[4,64,128]{2,1,0:T(8,128)(2,1)S(1)} %pad_maximum_fusion.2), channel_id=1, source_target_pairs={{0,240},{1,17},{16,0},{17,33},{32,16},{33,49},{48,32},{49,65},{64,... | collective-permute-start | bytes 196616 | tf_op jit(solution)/shard_map/ppermute | solution.py:288
  150.5 9.7 %collective-permute-start.12 = (bf16[4,64,128]{2,1,0:T(8,128)(2,1)S(1)}, bf16[4,64,128]{2,1,0:T(8,128)(2,1)S(1)}, u32[]{:S(2)}, u32[]{:S(2)}) collective-permute-start(bf16[4,64,128]{2,1,0:T(8,128)(2,1)S(1)} %pad_maximum_fusion.2), channel_id=1, source_target_pairs={{0,16},{1,241},{16,32},{17,1},{32,48},{33,17},{48,64},{49,33},{64,... | collective-permute-start | bytes 196616 | tf_op jit(solution)/shard_map/ppermute | solution.py:288
  158.3 3.4 %collective-permute-start.6 = (bf16[8,64,256]{2,1,0:T(8,128)(2,1)S(1)}, bf16[8,64,256]{2,1,0:T(8,128)(2,1)S(1)}, u32[]{:S(2)}, u32[]{:S(2)}) collective-permute-start(bf16[8,64,256]{2,1,0:T(8,128)(2,1)S(1)} %all-to-all-done.2.mine_ref), channel_id=1, source_target_pairs={{0,1},{1,0},{2,3},{3,2},{4,5},{5,4},{6,7},{7,6},{8,9},{9,8},{10,11... | collective-permute-start | bytes 786440 | tf_op jit(solution)/shard_map/ppermute | solution.py:272
  162.9 21.5 %all-to-all-start.3 = ((bf16[8,256,128]{2,1,0:T(8,128)(2,1)}), bf16[8,256,128]{2,1,0:T(8,128)(2,1)S(1)}, u32[]{:S(2)}, u32[]{:S(2)}) async-start(bf16[8,256,128]{2,1,0:T(8,128)(2,1)} %get-tuple-element.45), calls=%async_computation.3 | async-start | bytes 1048576 | tf_op jit(solution)/shard_map/all_to_all | solution.py:267
  166.7 11.2 %collective-permute-start.14 = (bf16[4,192,128]{2,1,0:T(8,128)(2,1)S(1)}, bf16[4,192,128]{2,1,0:T(8,128)(2,1)S(1)}, u32[]{:S(2)}, u32[]{:S(2)}) collective-permute-start(bf16[4,192,128]{2,1,0:T(8,128)(2,1)S(1)} %pad_maximum_fusion), channel_id=1, source_target_pairs={{0,224},{1,33},{16,240},{17,49},{32,0},{33,65},{48,16},{49,81},{64... | collective-permute-start | bytes 589832 | tf_op jit(solution)/shard_map/ppermute | solution.py:288
  171.9 9.2 %collective-permute-start.15 = (bf16[4,192,128]{2,1,0:T(8,128)(2,1)S(1)}, bf16[4,192,128]{2,1,0:T(8,128)(2,1)S(1)}, u32[]{:S(2)}, u32[]{:S(2)}) collective-permute-start(bf16[4,192,128]{2,1,0:T(8,128)(2,1)S(1)} %pad_maximum_fusion), channel_id=1, source_target_pairs={{0,240},{1,17},{16,0},{17,33},{32,16},{33,49},{48,32},{49,65},{64,... | collective-permute-start | bytes 589832 | tf_op jit(solution)/shard_map/ppermute | solution.py:288
  173.9 12.5 %collective-permute-start.16 = (bf16[4,192,128]{2,1,0:T(8,128)(2,1)S(1)}, bf16[4,192,128]{2,1,0:T(8,128)(2,1)S(1)}, u32[]{:S(2)}, u32[]{:S(2)}) collective-permute-start(bf16[4,192,128]{2,1,0:T(8,128)(2,1)S(1)} %pad_maximum_fusion), channel_id=1, source_target_pairs={{0,16},{1,241},{16,32},{17,1},{32,48},{33,17},{48,64},{49,33},{64,... | collective-permute-start | bytes 589832 | tf_op jit(solution)/shard_map/ppermute | solution.py:288
  184.4 3.8 %collective-permute-start.13 = (bf16[8,256,128]{2,1,0:T(8,128)(2,1)S(1)}, bf16[8,256,128]{2,1,0:T(8,128)(2,1)S(1)}, u32[]{:S(2)}, u32[]{:S(2)}) collective-permute-start(bf16[8,256,128]{2,1,0:T(8,128)(2,1)S(1)} %all-to-all-done.3.mine_ref), channel_id=1, source_target_pairs={{0,1},{1,0},{2,3},{3,2},{4,5},{5,4},{6,7},{7,6},{8,9},{9,8},{10,11... | collective-permute-start | bytes 1572872 | tf_op jit(solution)/shard_map/ppermute | solution.py:272
  188.7 4.8 %collective-permute-start.17 = (bf16[64,128]{1,0:T(8,128)(2,1)S(1)}, bf16[64,128]{1,0:T(8,128)(2,1)S(1)}, u32[]{:S(2)}, u32[]{:S(2)}) collective-permute-start(bf16[64,128]{1,0:T(8,128)(2,1)S(1)} %get-tuple-element.51), channel_id=1, source_target_pairs={{0,16},{16,32},{32,48},{48,64},{64,80},{80,96},{96,112},{112,128},... | collective-permute-start | bytes 49160 | tf_op jit(solution)/shard_map/ppermute | solution.py:312
  229.4 3.4 %collective-permute-start.18 = (bf16[8,64,256]{2,1,0:T(8,128)(2,1)S(1)}, bf16[8,64,256]{2,1,0:T(8,128)(2,1)S(1)}, u32[]{:S(2)}, u32[]{:S(2)}) collective-permute-start(bf16[8,64,256]{2,1,0:T(8,128)(2,1)S(1)} %all_to_all.32.mine_ref), channel_id=1, source_target_pairs={{0,1},{1,0},{2,3},{3,2},{4,5},{5,4},{6,7},{7,6},{8,9},{9,8},{10,11... | collective-permute-start | bytes 786440 | tf_op jit(solution)/shard_map/ppermute | solution.py:272
  (6 other events, 27.7 us)
